TPU v7x, 32 devices: a whole 2x2x4 slice. The times are simulated.
32 devices in a mesh: ep: 8 (over z, x), tp: 4 (over y, core).
Axes of the slice: x: 2, y: 2, z: 4, core: 2. Of those that a mesh axis runs over, the one named last changes fastest.
Arguments:
- query_rows: bfloat16 [3072, 1024], P('ep', 'tp'), may hold values from -8 to 8
- key_rows: bfloat16 [3072, 256], P('ep'), may hold values from -8 to 8
- value_rows: bfloat16 [3072, 256], P('ep'), may hold values from -6 to 6
- query_gain: float32 [64], replicated, may hold values from 0.3 to 6
- key_gain: float32 [64], replicated, may hold values from 0.3 to 6
- out_weight: bfloat16 [1024, 2048], P('tp'), may hold values from -0.1875 to 0.1875
- mixer_gain: float32 [2048], replicated, may hold values from 0.1 to 1.9
- expert_input: bfloat16 [2048, 2048], P('ep'), may hold values from -6 to 6
- expert_ids: int32 [2048, 2], P('ep'), may hold values from 0 to 7, all different within a row; in each aligned block of 256 rows (0 to 255, 256 to 511, ...) at most 96 rows name the same one
- gate_score: float32 [2048, 2], P('ep'), may hold values from 0.05 to 1
- expert_gain: float32 [2048], replicated, may hold values from 0.1 to 1.9
- gate_weight: bfloat16 [8, 2048, 4096], P('ep', None, 'tp'), may hold values from -0.125 to 0.125
- up_weight: bfloat16 [8, 2048, 4096], P('ep', None, 'tp'), may hold values from -0.125 to 0.125
- down_weight: bfloat16 [8, 4096, 2048], P('ep', 'tp'), may hold values from -0.09375 to 0.09375
- shared_gate: bfloat16 [2048, 2048], P(None, 'tp'), may hold values from -0.125 to 0.125
- shared_up: bfloat16 [2048, 2048], P(None, 'tp'), may hold values from -0.125 to 0.125
- shared_down: bfloat16 [2048, 2048], P('tp'), may hold values from -0.125 to 0.125
Outputs:
- mixer_out: bfloat16 [3072, 2048], P('ep')
- expert_out: bfloat16 [2048, 2048], P('ep', 'tp')
Inputs may be any that keep to these rules, and one draw needn't show every extreme that they name: `expert_ids`: each row names 2 different experts. In each aligned block of 256 rows (the rows of one device) no expert is named by more than 96 rows, a bound that some block reaches.
All inputs are finite; a program needn't handle non-finite values.
Results may differ from a plain program's by a relative error of at most 0.02.
The roundings to bfloat16 on the way count: a program that leaves them out, or rounds other values in their place, can miss the bound.
Values may be sent and summed in bfloat16 or wider, within the bound.
No kernel may reach another device: no remote copies, remote signals or barrier semaphores. Data moves between devices by JAX's collectives and lax.ppermute only.
A program may use at most 128 MiB of HBM per device.

v0:
```python
import math

import jax
import jax.numpy as jnp
from jax import lax
from jax.sharding import PartitionSpec as P

HEADS = 16
KV_HEADS = 4
HEAD_DIM = 64
GRID_W = 64


EPSILON = 1e-06
ROUTED_SCALE = 2.5


def rotary_angles(position):
    grid_row = (position // GRID_W).astype(jnp.float32)
    grid_col = (position % GRID_W).astype(jnp.float32)
    quarter = HEAD_DIM // 4
    inverse = 10000.0 ** (-jnp.arange(quarter, dtype=jnp.float32) / quarter)
    return jnp.concatenate([grid_row[:, None] * inverse, grid_col[:, None] * inverse], axis=1)


def normalize_rotate(heads_in, gain_vector, angles):
    widened = heads_in.astype(jnp.float32)
    scaled = widened * lax.rsqrt(jnp.mean(widened * widened, axis=-1, keepdims=True) + EPSILON)
    scaled = scaled * gain_vector
    half_dim = scaled.shape[-1] // 2
    front_half = scaled[..., :half_dim]
    back_half = scaled[..., half_dim:]
    cosine_table = jnp.cos(angles)[:, None, :]
    sine_table = jnp.sin(angles)[:, None, :]
    turned = jnp.concatenate(
        [
            front_half * cosine_table - back_half * sine_table,
            front_half * sine_table + back_half * cosine_table,
        ],
        axis=-1,
    )
    return turned.astype(jnp.bfloat16)


def mixer_half(query_rows, key_rows, value_rows, query_gain, key_gain, out_weight, mixer_gain):
    local_rows = query_rows.shape[0]
    lane_heads = query_rows.shape[1] // HEAD_DIM
    group = HEADS // KV_HEADS
    lane_kv = max(1, lane_heads // group)
    local_group = lane_heads // lane_kv
    first_kv = lax.axis_index("tp") * lane_heads // group
    offset = lax.axis_index("ep") * local_rows
    angles = rotary_angles(offset + jnp.arange(local_rows, dtype=jnp.int32))
    query_rot = normalize_rotate(
        query_rows.reshape(local_rows, lane_heads, HEAD_DIM), query_gain, angles
    )
    query_grouped = query_rot.reshape(local_rows, lane_kv, local_group, HEAD_DIM)
    key_cols = lax.dynamic_slice_in_dim(key_rows, first_kv * HEAD_DIM, lane_kv * HEAD_DIM, 1)
    value_cols = lax.dynamic_slice_in_dim(value_rows, first_kv * HEAD_DIM, lane_kv * HEAD_DIM, 1)
    key_rot = normalize_rotate(key_cols.reshape(local_rows, lane_kv, HEAD_DIM), key_gain, angles)
    stacked = jnp.concatenate([key_rot.reshape(local_rows, lane_kv * HEAD_DIM), value_cols], axis=1)
    scale_factor = HEAD_DIM ** (-0.5)
    key_width = lane_kv * HEAD_DIM

    def step_block(state, block_rows):
        row_peak, row_total, accum = state
        block_keys = block_rows[:, :key_width].reshape(block_rows.shape[0], lane_kv, HEAD_DIM)
        block_values = block_rows[:, key_width:].reshape(block_rows.shape[0], lane_kv, HEAD_DIM)
        scores = (
            jnp.einsum(
                "qkgd,skd->kgqs", query_grouped, block_keys, preferred_element_type=jnp.float32
            )
            * scale_factor
        )
        new_peak = jnp.maximum(row_peak, jnp.max(scores, axis=3))
        shrink = jnp.exp(row_peak - new_peak)
        exponent = jnp.exp(scores - new_peak[..., None])
        row_total = row_total * shrink + jnp.sum(exponent, axis=3)
        accum = accum * shrink[..., None] + jnp.einsum(
            "kgqs,skd->kgqd",
            exponent.astype(jnp.bfloat16),
            block_values,
            preferred_element_type=jnp.float32,
        )
        return ((new_peak, row_total, accum), None)

    start_state = (
        jnp.full((lane_kv, local_group, local_rows), -jnp.inf, jnp.float32),
        jnp.zeros((lane_kv, local_group, local_rows), jnp.float32),
        jnp.zeros((lane_kv, local_group, local_rows, HEAD_DIM), jnp.float32),
    )
    carry = start_state
    piece = lax.all_gather(stacked, "ep", axis=0, tiled=True)
    shard_count = piece.shape[0] // local_rows
    per_block = math.gcd(shard_count, max(1, 2048 // local_rows))
    block_rows = per_block * local_rows
    blocks = piece.reshape(piece.shape[0] // block_rows, block_rows, piece.shape[1])
    carry, unused = lax.scan(step_block, carry, blocks)
    row_peak, row_total, accum = carry
    attended = (accum / row_total[..., None]).astype(jnp.bfloat16)
    lane_weight = out_weight.reshape(lane_kv, local_group, HEAD_DIM, out_weight.shape[1])
    partial_value = jnp.einsum(
        "kgqd,kgde->qe", attended, lane_weight, preferred_element_type=jnp.float32
    )
    mixer_sum = lax.psum(partial_value.astype(jnp.bfloat16), "tp").astype(jnp.float32)
    mixer_scale = lax.rsqrt(jnp.mean(mixer_sum * mixer_sum, axis=1, keepdims=True) + EPSILON)
    return (mixer_sum * mixer_scale * mixer_gain).astype(jnp.bfloat16)


def expert_half(
    expert_input,
    expert_ids,
    gate_score,
    expert_gain,
    gate_weight,
    up_weight,
    down_weight,
    shared_gate,
    shared_up,
    shared_down,
):
    local_rows, top_count = expert_ids.shape
    local_experts = gate_weight.shape[0]
    ep_size = lax.axis_size("ep")
    experts_all = local_experts * ep_size
    capacity = 3 * local_rows * top_count // (2 * experts_all)
    model_width = expert_input.shape[1]
    lane_cols = model_width // lax.axis_size("tp")
    slots_total = ep_size * capacity
    widened = expert_input.astype(jnp.float32)
    normed = (
        widened
        * lax.rsqrt(jnp.mean(widened * widened, axis=1, keepdims=True) + EPSILON)
        * expert_gain
    ).astype(jnp.bfloat16)
    route_weight = gate_score / jnp.sum(gate_score, axis=1, keepdims=True) * ROUTED_SCALE
    pair_ids = expert_ids.reshape(local_rows * top_count)
    onehot = (pair_ids[:, None] == jnp.arange(experts_all, dtype=jnp.int32)).astype(jnp.int32)
    ranks = jnp.sum(
        (jnp.cumsum(onehot, axis=0, dtype=jnp.int32) - 1) * onehot, axis=1, dtype=jnp.int32
    )
    slot_index = pair_ids * capacity + ranks
    row_numbers = jnp.arange(local_rows * top_count, dtype=jnp.int32) // top_count
    sources = jnp.full((experts_all * capacity,), -1, jnp.int32).at[slot_index].set(row_numbers)
    filled = (sources >= 0)[:, None]
    safe_rows = jnp.maximum(sources, 0)
    nothing = jnp.zeros((), jnp.bfloat16)
    lane_start = lax.axis_index("tp") * lane_cols
    own_cols = lax.dynamic_slice_in_dim(normed, lane_start, lane_cols, 1)
    outgoing = jnp.where(filled, own_cols[safe_rows], nothing).reshape(
        experts_all, capacity, lane_cols
    )
    arrived = lax.all_to_all(outgoing, "ep", split_axis=0, concat_axis=0, tiled=True)
    arranged = arrived.reshape(ep_size, local_experts, capacity, lane_cols).transpose(1, 0, 2, 3)
    arranged = arranged.reshape(local_experts, slots_total, lane_cols)
    piece = lax.all_gather(arranged, "tp", axis=2, tiled=True)
    gate_value = jnp.einsum("esd,edf->esf", piece, gate_weight, preferred_element_type=jnp.float32)
    up_value = jnp.einsum("esd,edf->esf", piece, up_weight, preferred_element_type=jnp.float32)
    hidden = (jax.nn.silu(gate_value) * up_value).astype(jnp.bfloat16)
    down_part = jnp.einsum("esf,efd->esd", hidden, down_weight, preferred_element_type=jnp.float32)
    down_rows = down_part.reshape(local_experts, ep_size, capacity, model_width).transpose(
        1, 0, 2, 3
    )
    down_rows = down_rows.reshape(experts_all * capacity, model_width)
    shared_gate_value = jnp.dot(normed, shared_gate, preferred_element_type=jnp.float32)
    shared_up_value = jnp.dot(normed, shared_up, preferred_element_type=jnp.float32)
    shared_hidden = (jax.nn.silu(shared_gate_value) * shared_up_value).astype(jnp.bfloat16)
    shared_part = jnp.dot(shared_hidden, shared_down, preferred_element_type=jnp.float32)
    terms = jnp.concatenate([down_rows, shared_part], axis=0)
    summed = lax.psum_scatter(
        terms.astype(jnp.bfloat16), "tp", scatter_dimension=1, tiled=True
    ).astype(jnp.float32)
    routed_slots = (
        summed[: experts_all * capacity]
        .astype(jnp.bfloat16)
        .reshape(experts_all, capacity, lane_cols)
    )
    shared_cols = summed[experts_all * capacity :]
    returned = lax.all_to_all(routed_slots, "ep", split_axis=0, concat_axis=0, tiled=True)
    picked = returned.reshape(experts_all * capacity, lane_cols)[slot_index]
    picked = picked.reshape(local_rows, top_count, lane_cols)
    routed = jnp.sum(picked.astype(jnp.float32) * route_weight[:, :, None], axis=1)
    return (routed + shared_cols).astype(jnp.bfloat16)


def body(
    query_rows,
    key_rows,
    value_rows,
    query_gain,
    key_gain,
    out_weight,
    mixer_gain,
    expert_input,
    expert_ids,
    gate_score,
    expert_gain,
    gate_weight,
    up_weight,
    down_weight,
    shared_gate,
    shared_up,
    shared_down,
):
    mixer_out = mixer_half(
        query_rows, key_rows, value_rows, query_gain, key_gain, out_weight, mixer_gain
    )
    expert_out = expert_half(
        expert_input,
        expert_ids,
        gate_score,
        expert_gain,
        gate_weight,
        up_weight,
        down_weight,
        shared_gate,
        shared_up,
        shared_down,
    )
    return (mixer_out, expert_out)


def solution(mesh):
    in_specs = (
        P("ep", "tp"),
        P("ep", None),
        P("ep", None),
        P(),
        P(),
        P("tp", None),
        P(),
        P("ep", None),
        P("ep", None),
        P("ep", None),
        P(),
        P("ep", None, "tp"),
        P("ep", None, "tp"),
        P("ep", "tp", None),
        P(None, "tp"),
        P(None, "tp"),
        P("tp", None),
    )
    out_specs = (P("ep", None), P("ep", "tp"))
    return jax.shard_map(body, mesh=mesh, in_specs=in_specs, out_specs=out_specs, check_vma=False)
```

profile of v0, /device:TPU:0, one launch (start us, length us, event | category | flops | bytes accessed | tf_op | source)
XLA Modules:
  0.0 218.4 jit_solution(9273533455983463291)
XLA Ops:
  11.0 2.4 %scatter_custom_fusion = s32[768]{0:T(1024)S(1)} fusion(s32[512]{0:T(512)S(1)} %bitcast.141, s32[512]{0:T(512)S(1)} %add_select_fusion, s32[]{:T(128)} %constant.116.clone.1), kind=kCustom, calls=%fused_computation.114 | custom fusion | bytes 3076 | tf_op jit(solution)/shard_map/scatter | solution.py:144
  17.1 2.7 %gather_fusion = bf16[768,512]{1,0:T(8,128)(2,1)S(1)} fusion(bf16[256,512]{1,0:T(8,128)(2,1)S(1)} %constant_dynamic-slice_fusion.1, s32[1024]{0:T(1024)S(1)} %pad_clamp_fusion.1), kind=kCustom, calls=%fused_computation | custom fusion | bytes 1575936 | tf_op jit(solution)/shard_map/gather | solution.py:150
  20.0 27.3 %all_to_all.10 = bf16[8,96,512]{2,1,0:T(8,128)(2,1)} all-to-all(bf16[8,96,512]{2,1,0:T(8,128)(2,1)S(1)} %broadcast_select_fusion), channel_id=1, replica_groups=mesh['ep'=8,'tp'=4] {'ep'}, dimensions={0} | all-to-all | bytes 1572864 | tf_op jit(solution)/shard_map/all_to_all | solution.py:153
  50.8 3.1 %fusion.67 = f32[256,512]{1,0:T(8,128)} fusion(bf16[256,2048]{1,0:T(8,128)(2,1)S(1)} %copy-done.5, bf16[2048,512]{1,0:T(8,128)(2,1)} %param.33), kind=kOutput, calls=%fused_computation.131 | convolution fusion | flops 536870912 | bytes 3670016 | tf_op jit(solution)/shard_map/dot_general | solution.py:165
  53.9 34.3 %all_gather.6 = bf16[3072,128]{1,0:T(8,128)(2,1)} all-gather(bf16[384,128]{1,0:T(8,128)(2,1)S(1)} %pad_maximum_fusion.2), channel_id=1, replica_groups=mesh['ep'=8,'tp'=4] {'ep'}, dimensions={0}, use_global_device_ids=true | all-gather | bytes 884736 | tf_op jit(solution)/shard_map/all_gather | solution.py:93
  88.1 4.3 %convolution_convert_fusion = bf16[256,2048]{1,0:T(8,128)(2,1)} fusion(bf16[512,2048]{1,0:T(8,128)(2,1)S(1)} %copy-done, bf16[256,2048]{1,0:T(8,128)(2,1)} %copy-done.4, bf16[2048,512]{1,0:T(8,128)(2,1)} %param.34, f32[256,512]{1,0:T(8,128)} %fusion.67), kind=kOutput, calls=%fused_computation.44 | convolution fusion | flops 1075052544 | bytes 6815744 | tf_op jit(solution)/shard_map/dot_general | solution.py:168
  92.5 6.3 %fusion.16 = f32[768,1024]{1,0:T(8,128)S(1)} fusion(bf16[1,2048,1024]{2,1,0:T(8,128)(2,1)} %param.30, bf16[1,768,2048]{2,1,0:T(8,128)(2,1)} %all-gather.2.cloned.1.call-done), kind=kOutput, calls=%fused_computation.30 | convolution fusion | flops 3221225472 | bytes 10485760 | tf_op jit(solution)/shard_map/esd,edf->esf/dot_general | solution.py:157
  98.8 3.6 %multiply_convert_fusion = bf16[768,1024]{1,0:T(8,128)(2,1)S(1)} fusion(f32[768,1024]{1,0:T(8,128)S(1)} %fusion.16, bf16[1,2048,1024]{2,1,0:T(8,128)(2,1)S(1)} %copy-done.12, bf16[1,768,2048]{2,1,0:T(8,128)(2,1)S(1)} %copy-done.14), kind=kOutput, calls=%fused_computation.41 | convolution fusion | flops 3225944064 | bytes 12058624 | tf_op jit(solution)/shard_map/esd,edf->esf/dot_general | solution.py:158
  102.4 3.6 %fusion.18 = bf16[768,2048]{1,0:T(8,128)(2,1)S(1)} fusion(bf16[768,1024]{1,0:T(8,128)(2,1)S(1)} %multiply_convert_fusion, bf16[1,1024,2048]{2,1,0:T(8,128)(2,1)S(1)} %copy-done.13), kind=kOutput, calls=%fused_computation.34 | convolution fusion | flops 3222798336 | bytes 8912896 | tf_op jit(solution)/shard_map/esf,efd->esd/dot_general | solution.py:160
  106.1 2.2 %pad_maximum_fusion = bf16[1024,2048]{1,0:T(8,128)(2,1)} fusion(bf16[256,2048]{1,0:T(8,128)(2,1)S(1)} %copy-done.6, bf16[768,2048]{1,0:T(8,128)(2,1)S(1)} %fusion.18), kind=kLoop, calls=%fused_computation.25 | loop fusion | flops 8388608 | bytes 8388608 | tf_op jit(solution)/shard_map/concatenate | solution.py:169
  108.4 47.6 %while.15 = (s32[]{:T(128)}, f32[1,4,384]{2,1,0:T(4,128)S(1)}, f32[1,4,384]{2,1,0:T(4,128)S(1)}, f32[1,4,384,64]{2,3,1,0:T(8,128)S(1)}, bf16[8,384,128]{2,1,0:T(...) while((s32[]{:T(128)}, f32[1,4,384]{2,1,0:T(4,128)S(1)}, ...), condition=%wide.region_5.6_spmd.clone, body=%wide.region_2.5_spmd.clone.sunk | while | flops 156017664 | bytes 18088064 | solution.py:98
  111.3 2.8 %fusion.82 = f32[1,4,384,64]{2,3,1,0:T(8,128)S(1)} fusion(f32[384,384,4]{1,0,2:T(8,128)} %get-tuple-element.151, f32[4,384]{1,0:T(4,128)S(1)} %bitcast.134, f32[1,4,384,64]{2,3,1,0:T(8,128)S(1)} %get-tuple-element.164, f32[4,384]{1,0:T(4,128)S(1)} %get-tuple-element.152, pred[]{:T(512)S(6)} %compare.18, bf16[384,128]{0,1:T(8,128)(2,1)S(1)} %bitcast.133), kind=kOutput, calls=%fused_computation.9.clone.1 | convolution fusion | flops 77561856 | bytes 3207169 | tf_op jit(solution)/shard_map/while/body/eval_jaxpr/kgqs,skd->kgqd/dot_general | solution.py:79
  117.8 2.5 %fusion.82 = f32[1,4,384,64]{2,3,1,0:T(8,128)S(1)} fusion(f32[384,384,4]{1,0,2:T(8,128)} %get-tuple-element.151, f32[4,384]{1,0:T(4,128)S(1)} %bitcast.134, f32[1,4,384,64]{2,3,1,0:T(8,128)S(1)} %get-tuple-element.164, f32[4,384]{1,0:T(4,128)S(1)} %get-tuple-element.152, pred[]{:T(512)S(6)} %compare.18, bf16[384,128]{0,1:T(8,128)(2,1)S(1)} %bitcast.133), kind=kOutput, calls=%fused_computation.9.clone.1 | convolution fusion | flops 77561856 | bytes 3207169 | tf_op jit(solution)/shard_map/while/body/eval_jaxpr/kgqs,skd->kgqd/dot_general | solution.py:79
  123.7 2.4 %fusion.82 = f32[1,4,384,64]{2,3,1,0:T(8,128)S(1)} fusion(f32[384,384,4]{1,0,2:T(8,128)} %get-tuple-element.151, f32[4,384]{1,0:T(4,128)S(1)} %bitcast.134, f32[1,4,384,64]{2,3,1,0:T(8,128)S(1)} %get-tuple-element.164, f32[4,384]{1,0:T(4,128)S(1)} %get-tuple-element.152, pred[]{:T(512)S(6)} %compare.18, bf16[384,128]{0,1:T(8,128)(2,1)S(1)} %bitcast.133), kind=kOutput, calls=%fused_computation.9.clone.1 | convolution fusion | flops 77561856 | bytes 3207169 | tf_op jit(solution)/shard_map/while/body/eval_jaxpr/kgqs,skd->kgqd/dot_general | solution.py:79
  129.8 2.4 %fusion.82 = f32[1,4,384,64]{2,3,1,0:T(8,128)S(1)} fusion(f32[384,384,4]{1,0,2:T(8,128)} %get-tuple-element.151, f32[4,384]{1,0:T(4,128)S(1)} %bitcast.134, f32[1,4,384,64]{2,3,1,0:T(8,128)S(1)} %get-tuple-element.164, f32[4,384]{1,0:T(4,128)S(1)} %get-tuple-element.152, pred[]{:T(512)S(6)} %compare.18, bf16[384,128]{0,1:T(8,128)(2,1)S(1)} %bitcast.133), kind=kOutput, calls=%fused_computation.9.clone.1 | convolution fusion | flops 77561856 | bytes 3207169 | tf_op jit(solution)/shard_map/while/body/eval_jaxpr/kgqs,skd->kgqd/dot_general | solution.py:79
  135.6 2.4 %fusion.82 = f32[1,4,384,64]{2,3,1,0:T(8,128)S(1)} fusion(f32[384,384,4]{1,0,2:T(8,128)} %get-tuple-element.151, f32[4,384]{1,0:T(4,128)S(1)} %bitcast.134, f32[1,4,384,64]{2,3,1,0:T(8,128)S(1)} %get-tuple-element.164, f32[4,384]{1,0:T(4,128)S(1)} %get-tuple-element.152, pred[]{:T(512)S(6)} %compare.18, bf16[384,128]{0,1:T(8,128)(2,1)S(1)} %bitcast.133), kind=kOutput, calls=%fused_computation.9.clone.1 | convolution fusion | flops 77561856 | bytes 3207169 | tf_op jit(solution)/shard_map/while/body/eval_jaxpr/kgqs,skd->kgqd/dot_general | solution.py:79
  141.4 2.4 %fusion.82 = f32[1,4,384,64]{2,3,1,0:T(8,128)S(1)} fusion(f32[384,384,4]{1,0,2:T(8,128)} %get-tuple-element.151, f32[4,384]{1,0:T(4,128)S(1)} %bitcast.134, f32[1,4,384,64]{2,3,1,0:T(8,128)S(1)} %get-tuple-element.164, f32[4,384]{1,0:T(4,128)S(1)} %get-tuple-element.152, pred[]{:T(512)S(6)} %compare.18, bf16[384,128]{0,1:T(8,128)(2,1)S(1)} %bitcast.133), kind=kOutput, calls=%fused_computation.9.clone.1 | convolution fusion | flops 77561856 | bytes 3207169 | tf_op jit(solution)/shard_map/while/body/eval_jaxpr/kgqs,skd->kgqd/dot_general | solution.py:79
  147.2 2.4 %fusion.82 = f32[1,4,384,64]{2,3,1,0:T(8,128)S(1)} fusion(f32[384,384,4]{1,0,2:T(8,128)} %get-tuple-element.151, f32[4,384]{1,0:T(4,128)S(1)} %bitcast.134, f32[1,4,384,64]{2,3,1,0:T(8,128)S(1)} %get-tuple-element.164, f32[4,384]{1,0:T(4,128)S(1)} %get-tuple-element.152, pred[]{:T(512)S(6)} %compare.18, bf16[384,128]{0,1:T(8,128)(2,1)S(1)} %bitcast.133), kind=kOutput, calls=%fused_computation.9.clone.1 | convolution fusion | flops 77561856 | bytes 3207169 | tf_op jit(solution)/shard_map/while/body/eval_jaxpr/kgqs,skd->kgqd/dot_general | solution.py:79
  153.1 2.4 %fusion.82 = f32[1,4,384,64]{2,3,1,0:T(8,128)S(1)} fusion(f32[384,384,4]{1,0,2:T(8,128)} %get-tuple-element.151, f32[4,384]{1,0:T(4,128)S(1)} %bitcast.134, f32[1,4,384,64]{2,3,1,0:T(8,128)S(1)} %get-tuple-element.164, f32[4,384]{1,0:T(4,128)S(1)} %get-tuple-element.152, pred[]{:T(512)S(6)} %compare.18, bf16[384,128]{0,1:T(8,128)(2,1)S(1)} %bitcast.133), kind=kOutput, calls=%fused_computation.9.clone.1 | convolution fusion | flops 77561856 | bytes 3207169 | tf_op jit(solution)/shard_map/while/body/eval_jaxpr/kgqs,skd->kgqd/dot_general | solution.py:79
  155.9 3.0 %bitcast_convert_fusion = bf16[384,2048]{1,0:T(8,128)(2,1)} fusion(bf16[4,64,2048]{2,1,0:T(8,128)(2,1)} %bitcast.144, f32[1,4,384,64]{2,3,1,0:T(8,128)S(1)} %get-tuple-element.35, f32[4,384]{1,0:T(4,128)S(1)} %bitcast.140), kind=kOutput, calls=%fused_computation.40 | convolution fusion | flops 403636224 | bytes 3020800 | tf_op jit(solution)/shard_map/kgqd,kgde->qe/dot_general | solution.py:102
  159.0 2.1 slice.56
  161.0 3.8 %all-to-all-start.1 = ((bf16[8,96,512]{2,1,0:T(8,128)(2,1)}), bf16[8,96,512]{2,1,0:T(8,128)(2,1)S(1)}, u32[]{:S(2)}, u32[]{:S(2)}) async-start(bf16[8,96,512]{2,1,0:T(8,128)(2,1)} %bitcast.137), calls=%async_computation.2 | async-start | bytes 1572864 | tf_op jit(solution)/shard_map/all_to_all | solution.py:179
  165.0 35.9 %all-reduce.2.cloned.1.call-done = bf16[384,2048]{1,0:T(8,128)(2,1)} async-done(((bf16[384,2048]{1,0:T(8,128)(2,1)}), bf16[384,2048]{1,0:T(8,128)(2,1)}) %all-reduce.2.cloned.1.call-update) | async-done | bytes 1572880 | tf_op jit(solution)/shard_map/psum | solution.py:105
  204.5 2.6 %gather_fusion.1 = bf16[512,512]{1,0:T(8,128)(2,1)} fusion(bf16[768,512]{1,0:T(8,128)(2,1)S(1)} %bitcast.131, s32[1024]{0:T(1024)S(1)} %pad_clamp_fusion), kind=kCustom, calls=%fused_computation.1 | custom fusion | bytes 1050624 | tf_op jit(solution)/shard_map/gather | solution.py:180
  (164 shorter events, 46.9 us)
Async XLA Ops:
  7.2 81.0 %copy-start = (bf16[512,2048]{1,0:T(8,128)(2,1)S(1)}, bf16[512,2048]{1,0:T(8,128)(2,1)}, u32[]{:S(2)}) copy-start(bf16[512,2048]{1,0:T(8,128)(2,1)} %param.35) | copy-start | bytes 6291460
  7.2 8.0 %copy-start.3 = (bf16[256,2048]{1,0:T(8,128)(2,1)S(1)}, bf16[256,2048]{1,0:T(8,128)(2,1)}, u32[]{:S(2)}) copy-start(bf16[256,2048]{1,0:T(8,128)(2,1)} %param.26) | copy-start | bytes 3145732
  7.2 85.3 %all-gather.2.cloned.1.call-start = ((), (), s32[]{:S(2)}) async-start(), calls=%async_computation.4 | async-start | bytes 3932160 | tf_op jit(solution)/shard_map/all_gather | solution.py:156
  19.8 29.0 %copy-start.10 = (f32[64]{0:T(128)S(1)}, f32[64]{0:T(128)}, u32[]{:S(2)}) copy-start(f32[64]{0:T(128)} %param.23) | copy-start | bytes 772
  19.8 29.5 %copy-start.7 = (bf16[384,256]{1,0:T(8,128)(2,1)S(1)}, bf16[384,256]{1,0:T(8,128)(2,1)}, u32[]{:S(2)}) copy-start(bf16[384,256]{1,0:T(8,128)(2,1)} %param.19) | copy-start | bytes 589828
  20.0 29.9 %copy-start.11 = (f32[64]{0:T(128)S(1)}, f32[64]{0:T(128)}, u32[]{:S(2)}) copy-start(f32[64]{0:T(128)} %param.22) | copy-start | bytes 772
  47.4 111.6 %reduce-scatter.2.cloned.1.call-start = ((), (), s32[]{:S(2)}) async-start(), calls=%async_computation.5 | async-start | bytes 5242880 | tf_op jit(solution)/shard_map/reduce_scatter | solution.py:170
  92.5 6.3 %copy-start.12 = (bf16[1,2048,1024]{2,1,0:T(8,128)(2,1)S(1)}, bf16[1,2048,1024]{2,1,0:T(8,128)(2,1)}, u32[]{:S(2)}) copy-start(bf16[1,2048,1024]{2,1,0:T(8,128)(2,1)} %param.31) | copy-start | bytes 12582916
  92.5 6.3 %copy-start.14 = (bf16[1,768,2048]{2,1,0:T(8,128)(2,1)S(1)}, bf16[1,768,2048]{2,1,0:T(8,128)(2,1)}, u32[]{:S(2)}) copy-start(bf16[1,768,2048]{2,1,0:T(8,128)(2,1)} %all-gather.2.cloned.1.call-done) | copy-start | bytes 9437188
  98.8 3.6 %copy-start.13 = (bf16[1,1024,2048]{2,1,0:T(8,128)(2,1)S(1)}, bf16[1,1024,2048]{2,1,0:T(8,128)(2,1)}, u32[]{:S(2)}) copy-start(bf16[1,1024,2048]{2,1,0:T(8,128)(2,1)} %param.32) | copy-start | bytes 12582916
  102.4 3.6 %copy-start.6 = (bf16[256,2048]{1,0:T(8,128)(2,1)S(1)}, bf16[256,2048]{1,0:T(8,128)(2,1)}, u32[]{:S(2)}) copy-start(bf16[256,2048]{1,0:T(8,128)(2,1)} %convolution_convert_fusion) | copy-start | bytes 3145732
  108.3 92.6 %all-reduce.2.cloned.1.call-start = ((), (), s32[]{:S(2)}) async-start(), calls=%async_computation.3 | async-start | bytes 3145728 | tf_op jit(solution)/shard_map/psum | solution.py:105
  111.3 3.1 %copy-start.1 = (f32[384,384,4]{1,0,2:T(8,128)S(1)}, f32[384,384,4]{1,0,2:T(8,128)}, u32[]{:S(2)}) copy-start(f32[384,384,4]{1,0,2:T(8,128)} %get-tuple-element.151) | copy-start | bytes 7077892 | tf_op jit(solution)/shard_map/while
  117.8 2.5 %copy-start.1 = (f32[384,384,4]{1,0,2:T(8,128)S(1)}, f32[384,384,4]{1,0,2:T(8,128)}, u32[]{:S(2)}) copy-start(f32[384,384,4]{1,0,2:T(8,128)} %get-tuple-element.151) | copy-start | bytes 7077892 | tf_op jit(solution)/shard_map/while
  123.7 2.6 %copy-start.1 = (f32[384,384,4]{1,0,2:T(8,128)S(1)}, f32[384,384,4]{1,0,2:T(8,128)}, u32[]{:S(2)}) copy-start(f32[384,384,4]{1,0,2:T(8,128)} %get-tuple-element.151) | copy-start | bytes 7077892 | tf_op jit(solution)/shard_map/while
  129.7 2.4 %copy-start.1 = (f32[384,384,4]{1,0,2:T(8,128)S(1)}, f32[384,384,4]{1,0,2:T(8,128)}, u32[]{:S(2)}) copy-start(f32[384,384,4]{1,0,2:T(8,128)} %get-tuple-element.151) | copy-start | bytes 7077892 | tf_op jit(solution)/shard_map/while
  135.6 2.4 %copy-start.1 = (f32[384,384,4]{1,0,2:T(8,128)S(1)}, f32[384,384,4]{1,0,2:T(8,128)}, u32[]{:S(2)}) copy-start(f32[384,384,4]{1,0,2:T(8,128)} %get-tuple-element.151) | copy-start | bytes 7077892 | tf_op jit(solution)/shard_map/while
  141.4 2.4 %copy-start.1 = (f32[384,384,4]{1,0,2:T(8,128)S(1)}, f32[384,384,4]{1,0,2:T(8,128)}, u32[]{:S(2)}) copy-start(f32[384,384,4]{1,0,2:T(8,128)} %get-tuple-element.151) | copy-start | bytes 7077892 | tf_op jit(solution)/shard_map/while
  147.2 2.4 %copy-start.1 = (f32[384,384,4]{1,0,2:T(8,128)S(1)}, f32[384,384,4]{1,0,2:T(8,128)}, u32[]{:S(2)}) copy-start(f32[384,384,4]{1,0,2:T(8,128)} %get-tuple-element.151) | copy-start | bytes 7077892 | tf_op jit(solution)/shard_map/while
  153.1 2.4 %copy-start.1 = (f32[384,384,4]{1,0,2:T(8,128)S(1)}, f32[384,384,4]{1,0,2:T(8,128)}, u32[]{:S(2)}) copy-start(f32[384,384,4]{1,0,2:T(8,128)} %get-tuple-element.151) | copy-start | bytes 7077892 | tf_op jit(solution)/shard_map/while
  158.9 5.9 %copy-start.9 = (f32[256,2]{0,1:T(2,128)S(1)}, f32[256,2]{0,1:T(2,128)}, u32[]{:S(2)}) copy-start(f32[256,2]{0,1:T(2,128)} %param.28) | copy-start | bytes 6148
  158.9 43.9 %copy-start.8 = (f32[2048]{0:T(1024)S(1)}, f32[2048]{0:T(1024)}, u32[]{:S(2)}) copy-start(f32[2048]{0:T(1024)} %param.25) | copy-start | bytes 24580
  161.0 43.4 %all-to-all-start.1 = ((bf16[8,96,512]{2,1,0:T(8,128)(2,1)}), bf16[8,96,512]{2,1,0:T(8,128)(2,1)S(1)}, u32[]{:S(2)}, u32[]{:S(2)}) async-start(bf16[8,96,512]{2,1,0:T(8,128)(2,1)} %bitcast.137), calls=%async_computation.2 | async-start | bytes 1572864 | tf_op jit(solution)/shard_map/all_to_all | solution.py:179
  200.9 1.9 copy-start.2
  (2 other events, 2.2 us)
Sparse Core Ops, SparseCore 0:
  47.5 27.5 all-gather.1
  108.4 43.3 reduce-scatter.1
  159.1 41.8 all-reduce.1
where the time goes:
time: 219 us; the launch traced here: 218 us
  blocking collectives  61.6 us (28%)
  matrix products  58.9 us (27%)
  waiting for transfers between devices  36 us (16%)
  local copies, waits for them, and re-layouts  25.5 us (12%)
  other arithmetic  17.9 us (8%)
  between operations  14.2 us (6%)
  starting transfers between devices  3.9 us (2%)
    psum x1, waiting for transfers between devices, mixer_half(): lax.psum(partial_value.astype(jnp.bfloat16), 'tp').astype(jnp.float32)  35.9 us
    all_gather x1, blocking collectives, mixer_half(): piece = lax.all_gather(stacked, 'ep', axis=0, tiled=True)  34.3 us
    all_to_all x1, blocking collectives, expert_half(): lax.all_to_all(outgoing, 'ep', split_axis=0, concat_axis=0, tiled=True)  27.3 us
    dot_general x8, matrix products, step_block(): jnp.einsum('kgqs,skd->kgqd', exponent.astype(jnp.bfloat16), block_values,...  19.6 us
    dot_general x8, matrix products, step_block(): jnp.einsum('qkgd,skd->kgqs', query_grouped, block_keys, preferred_element...  15.3 us
    dynamic_slice x16, local copies, waits for them, and re-layouts, mixer_half(): carry, unused = lax.scan(step_block, carry, blocks)  8.26 us
    dot_general x1, matrix products, expert_half(): jnp.einsum('esd,edf->esf', piece, gate_weight, preferred_element_type=jnp...  6.28 us
  transfers between devices with their start and end apart: 4, of which 1 were waited for; matrix products, arithmetic and copies ran while one was open for 30% of the time, Pallas kernels for 0%

commit v1 on v0

v1 whole, which is shorter than its diff:
```python
import functools
import math

import jax
import jax.numpy as jnp
from jax import lax
from jax.experimental import pallas as pl
from jax.experimental.pallas import tpu as pltpu
from jax.sharding import PartitionSpec as P

HEADS = 16
KV_HEADS = 4
HEAD_DIM = 64
GRID_W = 64
EPSILON = 1e-06
ROUTED_SCALE = 2.5
LOG2E = 1.4426950408889634
BF = jnp.bfloat16
F32 = jnp.float32
VMEM = pl.BlockSpec(memory_space=pltpu.VMEM)
SMEM = pl.BlockSpec(memory_space=pltpu.SMEM)


def params(mib):
    return pltpu.CompilerParams(vmem_limit_bytes=mib * 1024 * 1024)


def cost(flops, bytes_accessed, exps=0):
    return pl.CostEstimate(
        flops=int(flops), bytes_accessed=int(bytes_accessed), transcendentals=int(exps)
    )


def dot(a, b, dims=((1,), (0,))):
    return lax.dot_general(a, b, (dims, ((), ())), preferred_element_type=F32)


def rotary_table(offset, local_rows):
    grid_rows = local_rows // GRID_W
    quarter = HEAD_DIM // 4
    inverse = 10000.0 ** (-jnp.arange(quarter, dtype=F32) / quarter)
    inverse = jnp.tile(inverse, 128 // quarter)[None, :]
    rows = (offset // GRID_W + jnp.arange(grid_rows, dtype=jnp.int32)).astype(F32)
    cols = jnp.arange(GRID_W, dtype=jnp.int32).astype(F32)
    angle = jnp.concatenate([rows, cols])[:, None] * inverse
    sign = jnp.where(jnp.arange(128) % HEAD_DIM < HEAD_DIM // 2, -1.0, 1.0).astype(F32)[None, :]
    return jnp.concatenate([jnp.cos(angle), jnp.sin(angle) * sign], axis=0)


def rotate_block(x, gain, table_ref, grid_rows, g):
    lane = lax.broadcasted_iota(jnp.int32, x.shape, 1)
    squares = x * x
    first = lane < HEAD_DIM
    sum_a = jnp.sum(jnp.where(first, squares, 0.0), axis=1, keepdims=True)
    sum_b = jnp.sum(jnp.where(first, 0.0, squares), axis=1, keepdims=True)
    mean = jnp.where(first, sum_a, sum_b) * (1.0 / HEAD_DIM)
    y = x * lax.rsqrt(mean + EPSILON) * gain
    by_row = lane % 32 < 16
    height = grid_rows + GRID_W
    cosine = jnp.where(by_row, table_ref[g : g + 1, :], table_ref[grid_rows:height, :])
    sine = jnp.where(
        by_row,
        table_ref[height + g : height + g + 1, :],
        table_ref[height + grid_rows : 2 * height, :],
    )
    swapped = jnp.where(lane % HEAD_DIM < 32, pltpu.roll(y, 96, 1), pltpu.roll(y, 32, 1))
    return y * cosine + swapped * sine


def key_kernel(grid_rows, parity_ref, key_ref, value_ref, gain_ref, table_ref, out_ref):
    odd = parity_ref[1] == 1
    lane = lax.broadcasted_iota(jnp.int32, (GRID_W, 128), 1)
    for g in range(grid_rows):
        rows = slice(g * GRID_W, (g + 1) * GRID_W)
        keys = key_ref[rows, :].astype(F32)
        values = value_ref[rows, :].astype(F32)
        turned = rotate_block(keys, gain_ref[...], table_ref, grid_rows, g)
        turned = jnp.where(odd, pltpu.roll(turned, 64, 1), turned)
        values = jnp.where(odd, values, pltpu.roll(values, 64, 1))
        out_ref[rows, :] = jnp.where(lane < HEAD_DIM, turned, values).astype(BF)


def prepare_keys(key_rows, value_rows, gain, table, kv_index):
    local_rows = key_rows.shape[0]
    grid_rows = local_rows // GRID_W
    place = jnp.stack([kv_index // 2, kv_index % 2]).astype(jnp.int32)
    return pl.pallas_call(
        functools.partial(key_kernel, grid_rows),
        grid_spec=pltpu.PrefetchScalarGridSpec(
            num_scalar_prefetch=1,
            grid=(1,),
            in_specs=[
                pl.BlockSpec((local_rows, 128), lambda i, s: (0, s[0])),
                pl.BlockSpec((local_rows, 128), lambda i, s: (0, s[0])),
                pl.BlockSpec((1, 128), lambda i, s: (0, 0)),
                pl.BlockSpec(table.shape, lambda i, s: (0, 0)),
            ],
            out_specs=pl.BlockSpec((local_rows, 128), lambda i, s: (0, 0)),
        ),
        out_shape=jax.ShapeDtypeStruct((local_rows, 128), BF),
        cost_estimate=cost(1e6, 3e5),
        name="keys",
    )(place, key_rows, value_rows, gain, table)


def attention_kernel(
    heads, halves, tile, chunk, side_ref, q_ref, *rest
):
    n_kv = len(rest) - 9
    kv_refs = rest[:n_kv]
    gain_ref, table_ref, w_ref, send_ref, keep_ref, qs_ref, s_ref, o_ref, att_ref = rest[n_kv:]
    local_rows = q_ref.shape[0]
    grid_rows = local_rows // GRID_W
    lane = lax.broadcasted_iota(jnp.int32, (GRID_W, 128), 1)
    for pair in range(q_ref.shape[1] // 128):
        for g in range(grid_rows):
            x = q_ref[g * GRID_W : (g + 1) * GRID_W, pair * 128 : (pair + 1) * 128].astype(F32)
            turned = rotate_block(x, gain_ref[...], table_ref, grid_rows, g)
            turned = turned.astype(BF).astype(F32) * HEAD_DIM ** (-0.5)
            for k in range(2):
                head = pair * 2 + k
                if head < heads:
                    own = turned if k == 0 else pltpu.roll(turned, 64, 1)
                    start = head * local_rows + g * GRID_W
                    qs_ref[start : start + GRID_W, :] = jnp.where(lane < HEAD_DIM, own, 0.0).astype(BF)
    pieces = []
    column = 0
    for ref in kv_refs:
        for b in range(ref.shape[0]):
            for start in range(0, ref.shape[1], chunk):
                pieces.append((ref, b, start, column))
                column += chunk

    def one_tile(i, unused):
        begin = pl.multiple_of(i * tile, tile)
        q = qs_ref[pl.ds(begin, tile), :]
        peak = None
        for ref, b, start, at in pieces:
            s = dot(q, ref[b, start : start + chunk, :], ((1,), (1,)))
            s_ref[:, at : at + chunk] = s
            for c in range(0, chunk, 128):
                part = s[:, c : c + 128]
                peak = part if peak is None else jnp.maximum(peak, part)
        peak = jnp.max(peak, axis=1, keepdims=True)
        total = jnp.zeros((tile, 128), F32)
        accum = jnp.zeros((tile, 128), F32)
        for ref, b, start, at in pieces:
            e = jnp.exp2((s_ref[:, at : at + chunk] - peak) * LOG2E)
            for c in range(0, chunk, 128):
                total = total + e[:, c : c + 128]
            accum = accum + dot(e.astype(BF), ref[b, start : start + chunk, :])
        o_ref[pl.ds(begin, tile), :] = accum / jnp.sum(total, axis=1, keepdims=True)
        return unused

    lax.fori_loop(0, heads * local_rows // tile, one_tile, 0)
    wide = lax.broadcasted_iota(jnp.int32, (local_rows, 128), 1)
    for pair in range(q_ref.shape[1] // 128):
        head = pair * 2
        low = pltpu.roll(o_ref[head * local_rows : (head + 1) * local_rows, :], 64, 1)
        high = (
            o_ref[(head + 1) * local_rows : (head + 2) * local_rows, :]
            if head + 1 < heads
            else jnp.zeros((local_rows, 128), F32)
        )
        att_ref[:, pair * 128 : (pair + 1) * 128] = jnp.where(wide < HEAD_DIM, low, high).astype(BF)
    share = local_rows // (2 * halves)
    side = side_ref[0]
    for y in range(halves):
        for core, out in ((1 - side, send_ref), (side, keep_ref)):
            begin = pl.multiple_of((2 * y + core) * share, 8)
            out[y] = dot(att_ref[pl.ds(begin, share), :], w_ref[...]).astype(BF)


def attention(query_rows, kv_list, gain, table, out_weight, side, halves):
    local_rows, width = query_rows.shape
    heads = width // HEAD_DIM
    if width % 128:
        query_rows = jnp.pad(query_rows, ((0, 0), (0, 64)))
        out_weight = jnp.pad(out_weight, ((0, 64), (0, 0)))
    keys = sum(k.shape[0] * k.shape[1] for k in kv_list)
    tile = 128
    chunk = 384
    share = local_rows // (2 * halves)
    model = out_weight.shape[1]
    shape = jax.ShapeDtypeStruct((halves, share, model), BF)
    return pl.pallas_call(
        functools.partial(attention_kernel, heads, halves, tile, chunk),
        in_specs=[SMEM] + [VMEM] * (len(kv_list) + 4),
        out_specs=[VMEM, VMEM],
        out_shape=[shape, shape],
        scratch_shapes=[
            pltpu.VMEM((heads * local_rows, 128), BF),
            pltpu.VMEM((tile, keys), F32),
            pltpu.VMEM((heads * local_rows, 128), F32),
            pltpu.VMEM((local_rows, query_rows.shape[1]), BF),
        ],
        compiler_params=params(48),
        cost_estimate=cost(8e9, 4e6, heads * local_rows * keys),
        name="attention",
    )(side, query_rows, *kv_list, gain, table, out_weight)


def route_kernel(experts, cap, lane_ref, ids_ref, idst_ref, x_ref, gain_ref, *outs):
    normed_ref, slot_ref = outs[:2]
    chunk_refs = outs[2:]
    rows, top = ids_ref.shape
    x = x_ref[...].astype(F32)
    mean = jnp.mean(x * x, axis=1, keepdims=True)
    normed_ref[...] = (x * lax.rsqrt(mean + EPSILON) * gain_ref[...]).astype(BF)
    names = lax.broadcasted_iota(jnp.int32, (rows, experts), 1)
    hits = [ids_ref[:, k : k + 1] == names for k in range(top)]
    named = functools.reduce(jnp.logical_or, hits)
    r0 = lax.broadcasted_iota(jnp.int32, (rows, rows), 0)
    r1 = lax.broadcasted_iota(jnp.int32, (rows, rows), 1)
    below = jnp.where(r1 < r0, 1.0, 0.0).astype(BF)
    above = jnp.where(r0 < r1, 1.0, 0.0).astype(BF)
    count = dot(below, jnp.where(named, 1.0, 0.0).astype(BF))
    columns = []
    for k in range(top):
        rank = jnp.sum(jnp.where(hits[k], count, 0.0), axis=1, keepdims=True)
        columns.append(ids_ref[:, k : k + 1] * cap + rank.astype(jnp.int32))
    for k in range(top):
        slot_ref[:, k : k + 1] = columns[k]
    namest = lax.broadcasted_iota(jnp.int32, (experts, rows), 0)
    namedt = functools.reduce(
        jnp.logical_or, [idst_ref[k : k + 1, :] == namest for k in range(top)]
    )
    countt = dot(jnp.where(namedt, 1.0, 0.0).astype(BF), above).astype(jnp.int32)
    place = jnp.where(namedt, countt, -1)
    width = chunk_refs[0].shape[2]
    own = normed_ref[:, pl.ds(pl.multiple_of(lane_ref[0] * width, 128), width)]
    size = cap // len(chunk_refs)
    slots = lax.broadcasted_iota(jnp.int32, (cap, rows), 0)
    for e in range(experts):
        pick = jnp.where(place[e : e + 1, :] == slots, 1.0, 0.0).astype(BF)
        moved = dot(pick, own).astype(BF)
        for h, ref in enumerate(chunk_refs):
            ref[e] = moved[h * size : (h + 1) * size, :]


def route(expert_ids, expert_input, gain, lane, experts, cap, chunks, width):
    rows, top = expert_ids.shape
    model = expert_input.shape[1]
    return pl.pallas_call(
        functools.partial(route_kernel, experts, cap),
        in_specs=[SMEM] + [VMEM] * 4,
        out_specs=[VMEM] * (2 + chunks),
        out_shape=[
            jax.ShapeDtypeStruct((rows, model), BF),
            jax.ShapeDtypeStruct((rows, top), jnp.int32),
        ]
        + [jax.ShapeDtypeStruct((experts, cap // chunks, width), BF)] * chunks,
        compiler_params=params(32),
        cost_estimate=cost(1e9, 4e6),
        name="route",
    )(lane, expert_ids, expert_ids.T, expert_input, gain)


def mlp_kernel(n_x, halves, place_ref, *refs):
    x_refs = refs[:n_x]
    gate_ref, up_ref, down_ref, send_ref, keep_ref, x_scr, acc_ref = refs[n_x:]
    step = pl.program_id(0)
    rows = x_scr.shape[0]

    @pl.when(step == 0)
    def assemble():
        at = 0
        for ref in x_refs:
            for b in range(ref.shape[0]):
                width = ref.shape[2]
                begin = pl.multiple_of(place_ref[1 + at] * width, 128)
                x_scr[:, pl.ds(begin, width)] = ref[b]
                at += 1

    x = x_scr[...]
    gate = dot(x, gate_ref[0])
    up = dot(x, up_ref[0])
    hidden = (gate / (1.0 + jnp.exp(-gate)) * up).astype(BF)
    part = dot(hidden, down_ref[0])

    @pl.when(step == 0)
    def first():
        acc_ref[...] = part

    @pl.when(step > 0)
    def later():
        acc_ref[...] += part

    @pl.when(step == pl.num_programs(0) - 1)
    def finish():
        side = place_ref[0]
        width = send_ref.shape[2]
        for y in range(halves):
            for core, out in ((1 - side, send_ref), (side, keep_ref)):
                begin = pl.multiple_of((2 * y + core) * width, 128)
                out[y] = acc_ref[:, pl.ds(begin, width)].astype(BF)


def mlp(x_list, gate, up, down, place, halves):
    rows = x_list[0].shape[1]
    model, hidden = gate.shape[1:]
    block = min(256, hidden)
    width = model // (2 * halves)
    shape = jax.ShapeDtypeStruct((halves, rows, width), BF)

    def full(a):
        return pl.BlockSpec(a.shape, lambda i, s: (0, 0, 0))

    return pl.pallas_call(
        functools.partial(mlp_kernel, len(x_list), halves),
        grid_spec=pltpu.PrefetchScalarGridSpec(
            num_scalar_prefetch=1,
            grid=(hidden // block,),
            in_specs=[full(a) for a in x_list]
            + [
                pl.BlockSpec((1, model, block), lambda i, s: (0, 0, i)),
                pl.BlockSpec((1, model, block), lambda i, s: (0, 0, i)),
                pl.BlockSpec((1, block, model), lambda i, s: (0, i, 0)),
            ],
            out_specs=[pl.BlockSpec(shape.shape, lambda i, s: (0, 0, 0))] * 2,
            scratch_shapes=[pltpu.VMEM((rows, model), BF), pltpu.VMEM((rows, model), F32)],
        ),
        out_shape=[shape, shape],
        compiler_params=params(48),
        cost_estimate=cost(6 * rows * model * hidden, 6 * model * hidden),
        name="mlp",
    )(place, *x_list, gate, up, down)


def combine_kernel(cap, chunks, slot_ref, score_ref, *refs):
    chunk_refs = refs[:chunks]
    shared_a, shared_b, out_ref = refs[chunks:]
    rows, top = slot_ref.shape
    experts, size, width = chunk_refs[0].shape
    scores = score_ref[...]
    weight = scores / jnp.sum(scores, axis=1, keepdims=True) * ROUTED_SCALE
    n = lax.broadcasted_iota(jnp.int32, (rows, experts * size), 1)
    routed = None
    for k in range(top):
        slot = slot_ref[:, k : k + 1]
        expert = slot // cap
        inside = slot - expert * cap
        picked = None
        for h, ref in enumerate(chunk_refs):
            fits = (inside >= h * size) & (inside < (h + 1) * size)
            at = jnp.where(fits, expert * size + inside - h * size, -1)
            pick = jnp.where(n == at, 1.0, 0.0).astype(BF)
            got = dot(pick, ref[...].reshape(experts * size, width))
            picked = got if picked is None else picked + got
        term = picked * weight[:, k : k + 1]
        routed = term if routed is None else routed + term
    shared = shared_a[...] + shared_b[...].astype(F32)
    out_ref[...] = (routed + shared).astype(BF)


def combine(slot, gate_score, chunk_list, shared_a, shared_b, cap):
    rows = slot.shape[0]
    width = chunk_list[0].shape[2]
    return pl.pallas_call(
        functools.partial(combine_kernel, cap, len(chunk_list)),
        in_specs=[VMEM] * (4 + len(chunk_list)),
        out_specs=VMEM,
        out_shape=jax.ShapeDtypeStruct((rows, width), BF),
        compiler_params=params(32),
        cost_estimate=cost(8e8, 2e6),
        name="combine",
    )(slot, gate_score, *chunk_list, shared_a, shared_b)


def core_swap(x):
    n = lax.axis_size("tp")
    return lax.ppermute(x, "tp", [(i, i ^ 1) for i in range(n)])


def chip_shift(x, step):
    n = lax.axis_size("tp")
    return lax.ppermute(x, "tp", [(i, (i + 2 * step) % n) for i in range(n)])


def scatter_chips(keep, received, chip, halves):
    total = lax.dynamic_index_in_dim(keep, chip, 0, False).astype(F32)
    total = total + lax.dynamic_index_in_dim(received, chip, 0, False).astype(F32)
    arrived = []
    for step in range(1, halves):
        to = (chip + step) % halves
        term = lax.dynamic_index_in_dim(keep, to, 0, False).astype(F32)
        term = term + lax.dynamic_index_in_dim(received, to, 0, False).astype(F32)
        arrived.append(chip_shift(term.astype(BF), step))
    for a in arrived[:-1]:
        total = total + a.astype(F32)
    return total, arrived[-1]


def gather_chips(x, halves):
    return [x[None]] + [chip_shift(x, step)[None] for step in range(1, halves)]


def ep_gather(x, axis_z, axis_x):
    n = lax.axis_size("ep")
    own = [x]
    for step in range(1, axis_z):
        own.append(lax.ppermute(x, "ep", [(i, (i + step * axis_x) % n) for i in range(n)]))
    stacked = jnp.stack(own)
    groups = [stacked]
    for step in range(1, axis_x):
        perm = [(i, i // axis_x * axis_x + (i + step) % axis_x) for i in range(n)]
        groups.append(lax.ppermute(stacked, "ep", perm))
    return groups


def body(
    x_size,
    query_rows,
    key_rows,
    value_rows,
    query_gain,
    key_gain,
    out_weight,
    mixer_gain,
    expert_input,
    expert_ids,
    gate_score,
    expert_gain,
    gate_weight,
    up_weight,
    down_weight,
    shared_gate,
    shared_up,
    shared_down,
):
    ep, tp = lax.axis_size("ep"), lax.axis_size("tp")
    halves = tp // 2
    lane = lax.axis_index("tp")
    chip, side = lane // 2, lane % 2
    local_rows = query_rows.shape[0]
    heads = query_rows.shape[1] // HEAD_DIM
    assert tp % 2 == 0 and heads <= HEADS // KV_HEADS and gate_weight.shape[0] == 1
    rows, top = expert_ids.shape
    model = expert_input.shape[1]
    width = model // tp
    cap = 3 * rows * top // (2 * ep)
    chunks = 2

    table = rotary_table(lax.axis_index("ep") * local_rows, local_rows)
    key_gain2 = jnp.tile(key_gain, 2)[None, :]
    query_gain2 = jnp.tile(query_gain, 2)[None, :]
    kv_index = lane * heads * KV_HEADS // HEADS
    kv = prepare_keys(key_rows, value_rows, key_gain2, table, kv_index)
    kv_list = ep_gather(kv, ep // x_size, x_size)

    lane_s = lane[None].astype(jnp.int32)
    side_s = side[None].astype(jnp.int32)
    normed, slot, *outgoing = route(
        expert_ids, expert_input, expert_gain[None, :], lane_s, ep, cap, chunks, width
    )
    arrived = [lax.all_to_all(o, "ep", 0, 0, tiled=True) for o in outgoing]

    identity = jnp.concatenate([side_s, jnp.zeros((1,), jnp.int32)])
    sh_send, sh_keep = mlp(
        [normed[None]], shared_gate[None], shared_up[None], shared_down[None], identity, halves
    )
    sh_total, sh_last = scatter_chips(sh_keep, core_swap(sh_send), chip, halves)

    send, keep = attention(
        query_rows, kv_list, query_gain2, table, out_weight, side_s, halves
    )

    chips = [(chip - step) % halves for step in range(halves)]
    place = jnp.stack(
        [side] + [2 * c + side for c in chips] + [2 * c + 1 - side for c in chips]
    ).astype(jnp.int32)
    returned = []
    for a in arrived:
        x = a.reshape(ep * (cap // chunks), width)
        mine = gather_chips(x, halves)
        mine = jnp.concatenate(mine, axis=0)
        other = core_swap(mine)
        d_send, d_keep = mlp([mine, other], gate_weight, up_weight, down_weight, place, halves)
        total, last = scatter_chips(d_keep, core_swap(d_send), chip, halves)
        result = (total + last.astype(F32)).astype(BF).reshape(ep, cap // chunks, width)
        returned.append(lax.all_to_all(result, "ep", 0, 0, tiled=True))

    total, last = scatter_chips(keep, core_swap(send), chip, halves)
    mixer_sum = total + last.astype(F32)
    scale = lax.rsqrt(jnp.mean(mixer_sum * mixer_sum, axis=1, keepdims=True) + EPSILON)
    mixed = (mixer_sum * scale * mixer_gain).astype(BF)
    mine = jnp.concatenate(gather_chips(mixed, halves), axis=0)
    other = core_swap(mine)
    pieces = jnp.where(side == 0, jnp.stack([mine, other], 1), jnp.stack([other, mine], 1))
    back = (chip - jnp.arange(halves)) % halves
    mixer_out = pieces[back].reshape(local_rows, model)

    expert_out = combine(slot, gate_score, returned, sh_total, sh_last, cap)
    return (mixer_out, expert_out)


def solution(mesh):
    in_specs = (
        P("ep", "tp"),
        P("ep", None),
        P("ep", None),
        P(),
        P(),
        P("tp", None),
        P(),
        P("ep", None),
        P("ep", None),
        P("ep", None),
        P(),
        P("ep", None, "tp"),
        P("ep", None, "tp"),
        P("ep", "tp", None),
        P(None, "tp"),
        P(None, "tp"),
        P("tp", None),
    )
    out_specs = (P("ep", None), P("ep", "tp"))
    ep = mesh.shape["ep"]
    x_size = 2 ** (int(math.log2(ep)) // 2)
    return jax.shard_map(
        functools.partial(body, x_size),
        mesh=mesh,
        in_specs=in_specs,
        out_specs=out_specs,
        check_vma=False,
    )
```

time: 219 us -> 154 us (0.70)
  blocking collectives: 61.6 us -> 0 us
  matrix products: 58.9 us -> 0 us
  Pallas kernels: 0 us -> 47.8 us
  starting transfers between devices: 3.9 us -> 44.2 us
  local copies, waits for them, and re-layouts: 25.5 us -> 10.1 us
  between operations: 14.2 us -> 0.93 us
  waiting for transfers between devices: 36 us -> 32.7 us
    dot_general x22 -> x0, matrix products: 58.9 us -> none  [the longest x8 19.6 us: step_block(): jnp.einsum('kgqs,skd->kgqd', exponent.astype(jnp.bfloat16), block_values,...]
    pallas_call x0 -> x7, Pallas kernels: none -> 47.8 us  [the longest x3 25.4 us: mlp(): pl.pallas_call(functools.partial(mlp_kernel, len(x_list), halves), grid_s...]
    psum x1 -> x0, waiting for transfers between devices: 35.9 us -> none  [mixer_half(): lax.psum(partial_value.astype(jnp.bfloat16), 'tp').astype(jnp.float32)]
    all_gather x1 -> x0, blocking collectives: 34.3 us -> none  [mixer_half(): piece = lax.all_gather(stacked, 'ep', axis=0, tiled=True)]
    ppermute x0 -> x18, waiting for transfers between devices: none -> 31.2 us  [the longest x7 20 us: chip_shift(): return lax.ppermute(x, 'tp', [(i, (i + 2 * step) % n) for i in range(n)])]
    all_to_all x1 -> x0, blocking collectives: 27.3 us -> none  [expert_half(): lax.all_to_all(outgoing, 'ep', split_axis=0, concat_axis=0, tiled=True)]
    all_to_all x1 -> x4, starting transfers between devices: 3.78 us -> 25.4 us  [the longest x2 13.9 us: body(): returned.append(lax.all_to_all(result, 'ep', 0, 0, tiled=True))]
    ppermute x0 -> x18, starting transfers between devices: none -> 18.8 us  [the longest x7 9.72 us: chip_shift(): return lax.ppermute(x, 'tp', [(i, (i + 2 * step) % n) for i in range(n)])]
  transfers between devices with their start and end apart: 4 -> 22, of which waited for: 1 -> 7; matrix products, arithmetic and copies ran while one was open for 30% -> 14% of each run, Pallas kernels for 0% -> 29%
where the time goes in v1:
time: 154 us; the launch traced here: 153 us
  Pallas kernels  47.8 us (31%)
  starting transfers between devices  44.2 us (29%)
  waiting for transfers between devices  32.7 us (21%)
  other arithmetic  17.8 us (12%)
  local copies, waits for them, and re-layouts  10.1 us (7%)
    pallas_call x3, Pallas kernels, mlp(): pl.pallas_call(functools.partial(mlp_kernel, len(x_list), halves), grid_s...  25.4 us
    ppermute x7, waiting for transfers between devices, chip_shift(): return lax.ppermute(x, 'tp', [(i, (i + 2 * step) % n) for i in range(n)])  20 us
    pallas_call x1, Pallas kernels, attention(): pl.pallas_call(functools.partial(attention_kernel, heads, halves, tile, c...  15.7 us
    all_to_all x2, starting transfers between devices, body(): returned.append(lax.all_to_all(result, 'ep', 0, 0, tiled=True))  13.9 us
    all_to_all x2, starting transfers between devices, body(): arrived = [lax.all_to_all(o, 'ep', 0, 0, tiled=True) for o in outgoing]  11.5 us
    ppermute x7, starting transfers between devices, chip_shift(): return lax.ppermute(x, 'tp', [(i, (i + 2 * step) % n) for i in range(n)])  9.72 us
    ppermute x3, waiting for transfers between devices, ep_gather(): lax.ppermute(x, 'ep', [(i, (i + step * axis_x) % n) for i in range(n)])  7.77 us
    unnamed x34, local copies, waits for them, and re-layouts  5.98 us
  transfers between devices with their start and end apart: 22, of which 7 were waited for; matrix products, arithmetic and copies ran while one was open for 14% of the time, Pallas kernels for 29%

profile of v1, /device:TPU:0, one launch (start us, length us, event | category | flops | bytes accessed | tf_op | source)
XLA Modules:
  0.0 153.3 jit_solution(4107445279687788519)
XLA Ops:
  4.1 2.0 %route.1 = (bf16[256,2048]{1,0:T(8,128)(2,1)S(1)}, s32[256,2]{1,0:T(8,128)S(1)}, bf16[8,48,512]{2,1,0:T(8,128)(2,1)}, bf16[8,48,512]{2,1,0:T(8,128)(2,1)}) custom-call(s32[1]{0:T(128)} %bitcast.15.lane_ref, s32[256,2]{1,0:T(8,128)S(1)} %copy.19.ids_ref, s32[2,256]{1,0:T(2,128)S(1)} %bitcast.60, bf16[256,2048]{1,0:T(8,128)(2,1)S(1)} %copy-done.3, ...), custom_call_target="tpu_custom_call" | custom-call | flops 1000000000 | bytes 4000000 | tf_op jit(solution)/shard_map/route/pallas_call | solution.py:244
  6.7 7.4 %all-to-all-start.2 = ((bf16[8,48,512]{2,1,0:T(8,128)(2,1)}), bf16[8,48,512]{2,1,0:T(8,128)(2,1)}, u32[]{:S(2)}, u32[]{:S(2)}) async-start(bf16[8,48,512]{2,1,0:T(8,128)(2,1)} %get-tuple-element.20), calls=%async_computation.2 | async-start | bytes 786432 | tf_op jit(solution)/shard_map/all_to_all | solution.py:456
  16.4 3.1 %keys.1 = bf16[384,128]{1,0:T(8,128)(2,1)} custom-call(s32[2]{0:T(128)} %pad_add_fusion.parity_ref, bf16[384,256]{1,0:T(8,128)(2,1)} %key_ref.1, bf16[384,256]{1,0:T(8,128)(2,1)} %value_ref.1, f32[1,128]{1,0:T(1,128)} %broadcast_in_dim_tile.7.gain_ref, f32[140,128]{1,0:T(8,128)} %pad_maximum_fusion.4.table_ref.rest_3_), custom_call_target="tpu_custom_call" | custom-call | flops 1000000 | bytes 300000 | tf_op jit(solution)/shard_map/keys/pallas_call | solution.py:87
  19.6 2.0 %collective-permute-start = (bf16[384,128]{1,0:T(8,128)(2,1)}, bf16[384,128]{1,0:T(8,128)(2,1)S(1)}, u32[]{:S(2)}, u32[]{:S(2)}) collective-permute-start(bf16[384,128]{1,0:T(8,128)(2,1)} %keys.1), channel_id=1, source_target_pairs={{0,8},{4,12},{8,16},{12,20},{16,24},{20,28},{24,0},{28,4},{1,9},{5... | collective-permute-start | bytes 294920 | tf_op jit(solution)/shard_map/ppermute | solution.py:402
  21.6 2.4 %collective-permute-start.1 = (bf16[384,128]{1,0:T(8,128)(2,1)}, bf16[384,128]{1,0:T(8,128)(2,1)S(1)}, u32[]{:S(2)}, u32[]{:S(2)}) collective-permute-start(bf16[384,128]{1,0:T(8,128)(2,1)} %keys.1), channel_id=1, source_target_pairs={{0,16},{4,20},{8,24},{12,28},{16,0},{20,4},{24,8},{28,12},{1,17},{... | collective-permute-start | bytes 294920 | tf_op jit(solution)/shard_map/ppermute | solution.py:402
  25.4 2.3 %collective-permute-done = bf16[384,128]{1,0:T(8,128)(2,1)S(1)} collective-permute-done((bf16[384,128]{1,0:T(8,128)(2,1)}, bf16[384,128]{1,0:T(8,128)(2,1)S(1)}, u32[]{:S(2)}, u32[]{:S(2)}) %collective-permute-start) | collective-permute-done | bytes 98336 | tf_op jit(solution)/shard_map/ppermute | solution.py:402
  27.7 5.5 %collective-permute-done.1 = bf16[384,128]{1,0:T(8,128)(2,1)S(1)} collective-permute-done((bf16[384,128]{1,0:T(8,128)(2,1)}, bf16[384,128]{1,0:T(8,128)(2,1)S(1)}, u32[]{:S(2)}, u32[]{:S(2)}) %collective-permute-start.1) | collective-permute-done | bytes 98336 | tf_op jit(solution)/shard_map/ppermute | solution.py:402
  35.7 4.1 %all-to-all-start = ((bf16[8,48,512]{2,1,0:T(8,128)(2,1)}), bf16[8,48,512]{2,1,0:T(8,128)(2,1)}, u32[]{:S(2)}, u32[]{:S(2)}) async-start(bf16[8,48,512]{2,1,0:T(8,128)(2,1)} %get-tuple-element.17), calls=%async_computation | async-start | bytes 786432 | tf_op jit(solution)/shard_map/all_to_all | solution.py:456
  39.8 1.6 %collective-permute-start.12 = (bf16[384,512]{1,0:T(8,128)(2,1)}, bf16[384,512]{1,0:T(8,128)(2,1)S(1)}, u32[]{:S(2)}, u32[]{:S(2)}) collective-permute-start(bf16[384,512]{1,0:T(8,128)(2,1)} %bitcast.29), channel_id=1, source_target_pairs={{0,2},{1,3},{2,0},{3,1},{4,6},{5,7},{6,4},{7,5},{8,10},{9,11},{10,... | collective-permute-start | bytes 1179656 | tf_op jit(solution)/shard_map/ppermute | solution.py:377
  41.4 3.4 %collective-permute-done.3.rest_1_ = bf16[4,384,128]{2,1,0:T(8,128)(2,1)S(1)} collective-permute-done((bf16[4,384,128]{2,1,0:T(8,128)(2,1)S(1)}, bf16[4,384,128]{2,1,0:T(8,128)(2,1)S(1)}, u32[]{:S(2)}, u32[]{:S(2)}) %collective-permute-start.3) | collective-permute-done | bytes 393248 | tf_op jit(solution)/shard_map/ppermute | solution.py:407
  46.5 15.7 %attention.1 = (bf16[2,96,2048]{2,1,0:T(8,128)(2,1)}, bf16[2,96,2048]{2,1,0:T(8,128)(2,1)S(1)}) custom-call(s32[1]{0:T(128)} %bitcast.side_ref, bf16[384,256]{1,0:T(8,128)(2,1)S(1)} %copy-done.7, bf16[4,384,128]{2,1,0:T(8,128)(2,1)S(1)} %pad_maximum_fusion.3.rest_0_, bf16[4,384,128]{2,1,0:T(8,128)(2,1)S(1)} %copy-done.6, ...), custom_call_target="tpu_custom_call" | custom-call | flops 8000000000 | bytes 4000000 | tf_op jit(solution)/shard_map/attention/pallas_call | solution.py:186
  65.5 9.8 %collective-permute-done.8 = bf16[384,512]{1,0:T(8,128)(2,1)} collective-permute-done((bf16[384,512]{1,0:T(8,128)(2,1)}, bf16[384,512]{1,0:T(8,128)(2,1)}, u32[]{:S(2)}, u32[]{:S(2)}) %collective-permute-start.8) | collective-permute-done | bytes 393248 | tf_op jit(solution)/shard_map/ppermute | solution.py:377
  77.7 1.6 %collective-permute-start.5 = (bf16[96,2048]{1,0:T(8,128)(2,1)S(1)}, bf16[96,2048]{1,0:T(8,128)(2,1)S(1)}, u32[]{:S(2)}, u32[]{:S(2)}) collective-permute-start(bf16[96,2048]{1,0:T(8,128)(2,1)S(1)} %fusion.2), channel_id=1, source_target_pairs={{0,2},{1,3},{2,0},{3,1},{4,6},{5,7},{6,4},{7,5},{8,10},{9,11},{10,... | collective-permute-start | bytes 1179656 | tf_op jit(solution)/shard_map/ppermute | solution.py:377
  79.3 9.8 %mlp.4 = (bf16[2,384,512]{2,1,0:T(8,128)(2,1)S(1)}, bf16[2,384,512]{2,1,0:T(8,128)(2,1)S(1)}) custom-call(s32[5]{0:T(128)S(1)} %stack.70.place_ref, bf16[2,384,512]{2,1,0:T(8,128)(2,1)S(1)} %pad_maximum_fusion.2.refs_0_, bf16[2,384,512]{2,1,0:T(8,128)(2,1)S(1)} %collective-permute-done.13.refs_1_, bf16[1,2048,1024]{2,1,0:T(8,128)(2,1)} %refs_2_.3, ...), custom_call_target="tpu_custom_call" | custom-call | flops 4831838208 | bytes 12582912 | tf_op jit(solution)/shard_map/mlp/pallas_call | solution.py:309
  90.7 10.7 %mlp.3 = (bf16[2,384,512]{2,1,0:T(8,128)(2,1)}, bf16[2,384,512]{2,1,0:T(8,128)(2,1)S(1)}) custom-call(s32[5]{0:T(128)S(1)} %stack.70.place_ref, bf16[2,384,512]{2,1,0:T(8,128)(2,1)S(1)} %pad_maximum_fusion.1.refs_0_, bf16[2,384,512]{2,1,0:T(8,128)(2,1)S(1)} %collective-permute-done.9.refs_1_, bf16[1,2048,1024]{2,1,0:T(8,128)(2,1)} %refs_2_.3, ...), custom_call_target="tpu_custom_call" | custom-call | flops 4831838208 | bytes 12582912 | tf_op jit(solution)/shard_map/mlp/pallas_call | solution.py:309
  105.3 8.6 %collective-permute-done.15 = bf16[384,512]{1,0:T(8,128)(2,1)S(1)} collective-permute-done((bf16[384,512]{1,0:T(8,128)(2,1)S(1)}, bf16[384,512]{1,0:T(8,128)(2,1)S(1)}, u32[]{:S(2)}, u32[]{:S(2)}) %collective-permute-start.15) | collective-permute-done | bytes 393248 | tf_op jit(solution)/shard_map/ppermute | solution.py:377
  114.8 8.0 %all-to-all-start.3 = ((bf16[8,48,512]{2,1,0:T(8,128)(2,1)}), bf16[8,48,512]{2,1,0:T(8,128)(2,1)S(1)}, u32[]{:S(2)}, u32[]{:S(2)}) async-start(bf16[8,48,512]{2,1,0:T(8,128)(2,1)} %bitcast.33), calls=%async_computation.3 | async-start | bytes 786432 | tf_op jit(solution)/shard_map/all_to_all | solution.py:481
  126.5 4.9 %mlp.5 = (bf16[2,256,512]{2,1,0:T(8,128)(2,1)S(1)}, bf16[2,256,512]{2,1,0:T(8,128)(2,1)S(1)}) custom-call(s32[2]{0:T(128)S(1)} %pad_add_fusion.1.place_ref, bf16[1,256,2048]{2,1,0:T(8,128)(2,1)S(1)} %bitcast.59, bf16[1,2048,512]{2,1,0:T(8,128)(2,1)S(1)} %bitcast.58, bf16[1,2048,512]{2,1,0:T(8,128)(2,1)} %bitcast.62, bf16[1,512,2048]{2,1,0:T(8,128)(2,1)} %bitcast.63), custom_call_target="tpu_custom_call" | custom-call | flops 1610612736 | bytes 6291456 | tf_op jit(solution)/shard_map/mlp/pallas_call | solution.py:309
  133.4 1.9 %fusion.1 = bf16[384,512]{1,0:T(8,128)(2,1)} fusion(bf16[384,512]{1,0:T(8,128)(2,1)S(1)} %collective-permute-done.11, bf16[2,384,512]{2,1,0:T(8,128)(2,1)} %collective-permute-done.10, s32[]{:T(128)S(6)} %select_n.123, bf16[2,384,512]{2,1,0:T(8,128)(2,1)S(1)} %get-tuple-element.18), kind=kLoop, calls=%fused_computation.8 | loop fusion | flops 1179648 | bytes 1572868 | tf_op jit(solution)/shard_map/convert_element_type | solution.py:480
  135.3 5.8 %all-to-all-start.1 = ((bf16[8,48,512]{2,1,0:T(8,128)(2,1)}), bf16[8,48,512]{2,1,0:T(8,128)(2,1)S(1)}, u32[]{:S(2)}, u32[]{:S(2)}) async-start(bf16[8,48,512]{2,1,0:T(8,128)(2,1)} %bitcast.27), calls=%async_computation.1 | async-start | bytes 786432 | tf_op jit(solution)/shard_map/all_to_all | solution.py:481
  142.5 1.7 %collective-permute-start.17 = (bf16[256,512]{1,0:T(8,128)(2,1)S(1)}, bf16[256,512]{1,0:T(8,128)(2,1)S(1)}, u32[]{:S(2)}, u32[]{:S(2)}) collective-permute-start(bf16[256,512]{1,0:T(8,128)(2,1)S(1)} %get-tuple-element.26), channel_id=1, source_target_pairs={{0,2},{1,3},{2,0},{3,1},{4,6},{5,7},{6,4},{7,5},{8,10},{9,11},{10,... | collective-permute-start | bytes 786440 | tf_op jit(solution)/shard_map/ppermute | solution.py:377
  144.3 2.8 %maximum_select_fusion = bf16[2,2,96,2048]{3,2,0,1:T(8,128)(2,1)} fusion(bf16[2,1,96,2048]{3,2,0,1:T(8,128)(2,1)} %bitcast.12, bf16[2,1,96,2048]{3,2,0,1:T(8,128)(2,1)S(1)} %copy-done.11, pred[]{:T(512)S(6)} %eq.16), kind=kLoop, calls=%fused_computation.1 | loop fusion | flops 2359296 | bytes 3145729 | tf_op jit(solution)/shard_map/jit(_where)/select_n | solution.py:489
  147.1 3.2 %gather_fusion = bf16[2,2,96,2048]{3,2,1,0:T(8,128)(2,1)} fusion(bf16[2,2,96,2048]{3,2,0,1:T(8,128)(2,1)} %maximum_select_fusion, s32[1024]{0:T(1024)S(1)} %pad_clamp_fusion), kind=kCustom, calls=%fused_computation | custom fusion | bytes 3145736 | tf_op jit(solution)/shard_map/gather | solution.py:491
  151.8 1.5 %combine.1 = bf16[256,512]{1,0:T(8,128)(2,1)} custom-call(s32[256,2]{1,0:T(8,128)S(1)} %copy-done.10, f32[256,2]{1,0:T(8,128)S(1)} %copy.20.score_ref, bf16[8,48,512]{2,1,0:T(8,128)(2,1)S(1)} %all-to-all-done.1.refs_0_, bf16[8,48,512]{2,1,0:T(8,128)(2,1)S(1)} %all-to-all-done.3.refs_1_, f32[256,512]{1,0:T(8,128)S(1)} %get-tuple-element.27.refs_2_, ...), custom_call_target="tpu_custom_call" | custom-call | flops 800000000 | bytes 2000000 | tf_op jit(solution)/shard_map/combine/pallas_call | solution.py:359
  (94 shorter events, 32.5 us)
Async XLA Ops:
  6.7 38.8 %copy-start.4 = (bf16[256,2048]{1,0:T(8,128)(2,1)S(1)}, bf16[256,2048]{1,0:T(8,128)(2,1)}, u32[]{:S(2)}) copy-start(bf16[256,2048]{1,0:T(8,128)(2,1)} %rest_4_.1) | copy-start | bytes 3145732
  6.7 38.8 %copy-start.7 = (bf16[384,256]{1,0:T(8,128)(2,1)S(1)}, bf16[384,256]{1,0:T(8,128)(2,1)}, u32[]{:S(2)}) copy-start(bf16[384,256]{1,0:T(8,128)(2,1)} %q_ref.1) | copy-start | bytes 589828
  6.7 29.0 %all-to-all-start.2 = ((bf16[8,48,512]{2,1,0:T(8,128)(2,1)}), bf16[8,48,512]{2,1,0:T(8,128)(2,1)}, u32[]{:S(2)}, u32[]{:S(2)}) async-start(bf16[8,48,512]{2,1,0:T(8,128)(2,1)} %get-tuple-element.20), calls=%async_computation.2 | async-start | bytes 786432 | tf_op jit(solution)/shard_map/all_to_all | solution.py:456
  19.6 8.1 %collective-permute-start = (bf16[384,128]{1,0:T(8,128)(2,1)}, bf16[384,128]{1,0:T(8,128)(2,1)S(1)}, u32[]{:S(2)}, u32[]{:S(2)}) collective-permute-start(bf16[384,128]{1,0:T(8,128)(2,1)} %keys.1), channel_id=1, source_target_pairs={{0,8},{4,12},{8,16},{12,20},{16,24},{20,28},{24,0},{28,4},{1,9},{5... | collective-permute-start | bytes 294920 | tf_op jit(solution)/shard_map/ppermute | solution.py:402
  21.6 11.6 %collective-permute-start.1 = (bf16[384,128]{1,0:T(8,128)(2,1)}, bf16[384,128]{1,0:T(8,128)(2,1)S(1)}, u32[]{:S(2)}, u32[]{:S(2)}) collective-permute-start(bf16[384,128]{1,0:T(8,128)(2,1)} %keys.1), channel_id=1, source_target_pairs={{0,16},{4,20},{8,24},{12,28},{16,0},{20,4},{24,8},{28,12},{1,17},{... | collective-permute-start | bytes 294920 | tf_op jit(solution)/shard_map/ppermute | solution.py:402
  23.9 9.2 %collective-permute-start.2 = (bf16[384,128]{1,0:T(8,128)(2,1)}, bf16[384,128]{1,0:T(8,128)(2,1)S(1)}, u32[]{:S(2)}, u32[]{:S(2)}) collective-permute-start(bf16[384,128]{1,0:T(8,128)(2,1)} %keys.1), channel_id=1, source_target_pairs={{0,24},{4,28},{8,0},{12,4},{16,8},{20,12},{24,16},{28,20},{1,25},{... | collective-permute-start | bytes 294920 | tf_op jit(solution)/shard_map/ppermute | solution.py:402
  34.1 10.7 %collective-permute-start.3 = (bf16[4,384,128]{2,1,0:T(8,128)(2,1)S(1)}, bf16[4,384,128]{2,1,0:T(8,128)(2,1)S(1)}, u32[]{:S(2)}, u32[]{:S(2)}) collective-permute-start(bf16[4,384,128]{2,1,0:T(8,128)(2,1)S(1)} %pad_maximum_fusion.3.rest_0_), channel_id=1, source_target_pairs={{0,4},{4,0},{8,12},{12,8},{16,20},{20,16},{24,28},{28,24},{1,5},{5... | collective-permute-start | bytes 1179656 | tf_op jit(solution)/shard_map/ppermute | solution.py:407
  35.7 28.2 %all-to-all-start = ((bf16[8,48,512]{2,1,0:T(8,128)(2,1)}), bf16[8,48,512]{2,1,0:T(8,128)(2,1)}, u32[]{:S(2)}, u32[]{:S(2)}) async-start(bf16[8,48,512]{2,1,0:T(8,128)(2,1)} %get-tuple-element.17), calls=%async_computation | async-start | bytes 786432 | tf_op jit(solution)/shard_map/all_to_all | solution.py:456
  39.8 22.4 %collective-permute-start.12 = (bf16[384,512]{1,0:T(8,128)(2,1)}, bf16[384,512]{1,0:T(8,128)(2,1)S(1)}, u32[]{:S(2)}, u32[]{:S(2)}) collective-permute-start(bf16[384,512]{1,0:T(8,128)(2,1)} %bitcast.29), channel_id=1, source_target_pairs={{0,2},{1,3},{2,0},{3,1},{4,6},{5,7},{6,4},{7,5},{8,10},{9,11},{10,... | collective-permute-start | bytes 1179656 | tf_op jit(solution)/shard_map/ppermute | solution.py:377
  62.2 14.3 %collective-permute-start.4 = (bf16[2,96,2048]{2,1,0:T(8,128)(2,1)}, bf16[2,96,2048]{2,1,0:T(8,128)(2,1)}, u32[]{:S(2)}, u32[]{:S(2)}) collective-permute-start(bf16[2,96,2048]{2,1,0:T(8,128)(2,1)} %get-tuple-element.15), channel_id=1, source_target_pairs={{0,1},{1,0},{2,3},{3,2},{4,5},{5,4},{6,7},{7,6},{8,9},{9,8},{10,11... | collective-permute-start | bytes 2359304 | tf_op jit(solution)/shard_map/ppermute | solution.py:372
  63.3 16.0 %collective-permute-start.13 = (bf16[2,384,512]{2,1,0:T(8,128)(2,1)S(1)}, bf16[2,384,512]{2,1,0:T(8,128)(2,1)S(1)}, u32[]{:S(2)}, u32[]{:S(2)}) collective-permute-start(bf16[2,384,512]{2,1,0:T(8,128)(2,1)S(1)} %pad_maximum_fusion.2.refs_0_), channel_id=1, source_target_pairs={{0,1},{1,0},{2,3},{3,2},{4,5},{5,4},{6,7},{7,6},{8,9},{9,8},{10,11... | collective-permute-start | bytes 2359304 | tf_op jit(solution)/shard_map/ppermute | solution.py:372
  63.9 11.4 %collective-permute-start.8 = (bf16[384,512]{1,0:T(8,128)(2,1)}, bf16[384,512]{1,0:T(8,128)(2,1)}, u32[]{:S(2)}, u32[]{:S(2)}) collective-permute-start(bf16[384,512]{1,0:T(8,128)(2,1)} %bitcast.23), channel_id=1, source_target_pairs={{0,2},{1,3},{2,0},{3,1},{4,6},{5,7},{6,4},{7,5},{8,10},{9,11},{10,... | collective-permute-start | bytes 1179656 | tf_op jit(solution)/shard_map/ppermute | solution.py:377
  76.5 14.2 %collective-permute-start.9 = (bf16[2,384,512]{2,1,0:T(8,128)(2,1)S(1)}, bf16[2,384,512]{2,1,0:T(8,128)(2,1)S(1)}, u32[]{:S(2)}, u32[]{:S(2)}) collective-permute-start(bf16[2,384,512]{2,1,0:T(8,128)(2,1)S(1)} %pad_maximum_fusion.1.refs_0_), channel_id=1, source_target_pairs={{0,1},{1,0},{2,3},{3,2},{4,5},{5,4},{6,7},{7,6},{8,9},{9,8},{10,11... | collective-permute-start | bytes 2359304 | tf_op jit(solution)/shard_map/ppermute | solution.py:372
  77.7 11.7 %collective-permute-start.5 = (bf16[96,2048]{1,0:T(8,128)(2,1)S(1)}, bf16[96,2048]{1,0:T(8,128)(2,1)S(1)}, u32[]{:S(2)}, u32[]{:S(2)}) collective-permute-start(bf16[96,2048]{1,0:T(8,128)(2,1)S(1)} %fusion.2), channel_id=1, source_target_pairs={{0,2},{1,3},{2,0},{3,1},{4,6},{5,7},{6,4},{7,5},{8,10},{9,11},{10,... | collective-permute-start | bytes 1179656 | tf_op jit(solution)/shard_map/ppermute | solution.py:377
  89.1 12.6 %collective-permute-start.14 = (bf16[2,384,512]{2,1,0:T(8,128)(2,1)S(1)}, bf16[2,384,512]{2,1,0:T(8,128)(2,1)S(1)}, u32[]{:S(2)}, u32[]{:S(2)}) collective-permute-start(bf16[2,384,512]{2,1,0:T(8,128)(2,1)S(1)} %get-tuple-element.22), channel_id=1, source_target_pairs={{0,1},{1,0},{2,3},{3,2},{4,5},{5,4},{6,7},{7,6},{8,9},{9,8},{10,11... | collective-permute-start | bytes 2359304 | tf_op jit(solution)/shard_map/ppermute | solution.py:372
  101.4 21.4 %collective-permute-start.10 = (bf16[2,384,512]{2,1,0:T(8,128)(2,1)}, bf16[2,384,512]{2,1,0:T(8,128)(2,1)}, u32[]{:S(2)}, u32[]{:S(2)}) collective-permute-start(bf16[2,384,512]{2,1,0:T(8,128)(2,1)} %get-tuple-element.19), channel_id=1, source_target_pairs={{0,1},{1,0},{2,3},{3,2},{4,5},{5,4},{6,7},{7,6},{8,9},{9,8},{10,11... | collective-permute-start | bytes 2359304 | tf_op jit(solution)/shard_map/ppermute | solution.py:372
  101.8 12.1 %collective-permute-start.15 = (bf16[384,512]{1,0:T(8,128)(2,1)S(1)}, bf16[384,512]{1,0:T(8,128)(2,1)S(1)}, u32[]{:S(2)}, u32[]{:S(2)}) collective-permute-start(bf16[384,512]{1,0:T(8,128)(2,1)S(1)} %fusion.4), channel_id=1, source_target_pairs={{0,2},{1,3},{2,0},{3,1},{4,6},{5,7},{6,4},{7,5},{8,10},{9,11},{10,... | collective-permute-start | bytes 1179656 | tf_op jit(solution)/shard_map/ppermute | solution.py:377
  104.2 21.0 %collective-permute-start.6 = (bf16[96,2048]{1,0:T(8,128)(2,1)S(1)}, bf16[96,2048]{1,0:T(8,128)(2,1)S(1)}, u32[]{:S(2)}, u32[]{:S(2)}) collective-permute-start(bf16[96,2048]{1,0:T(8,128)(2,1)S(1)} %multiply_convert_fusion), channel_id=1, source_target_pairs={{0,2},{1,3},{2,0},{3,1},{4,6},{5,7},{6,4},{7,5},{8,10},{9,11},{10,... | collective-permute-start | bytes 1179656 | tf_op jit(solution)/shard_map/ppermute | solution.py:377
  114.8 20.6 %all-to-all-start.3 = ((bf16[8,48,512]{2,1,0:T(8,128)(2,1)}), bf16[8,48,512]{2,1,0:T(8,128)(2,1)S(1)}, u32[]{:S(2)}, u32[]{:S(2)}) async-start(bf16[8,48,512]{2,1,0:T(8,128)(2,1)} %bitcast.33), calls=%async_computation.3 | async-start | bytes 786432 | tf_op jit(solution)/shard_map/all_to_all | solution.py:481
  124.1 9.4 %collective-permute-start.11 = (bf16[384,512]{1,0:T(8,128)(2,1)S(1)}, bf16[384,512]{1,0:T(8,128)(2,1)S(1)}, u32[]{:S(2)}, u32[]{:S(2)}) collective-permute-start(bf16[384,512]{1,0:T(8,128)(2,1)S(1)} %fusion.3), channel_id=1, source_target_pairs={{0,2},{1,3},{2,0},{3,1},{4,6},{5,7},{6,4},{7,5},{8,10},{9,11},{10,... | collective-permute-start | bytes 1179656 | tf_op jit(solution)/shard_map/ppermute | solution.py:377
  126.4 17.8 %collective-permute-start.7 = (bf16[2,96,2048]{2,1,0:T(8,128)(2,1)}, bf16[2,96,2048]{2,1,0:T(8,128)(2,1)}, u32[]{:S(2)}, u32[]{:S(2)}) collective-permute-start(bf16[2,96,2048]{2,1,0:T(8,128)(2,1)} %get-tuple-element.29), channel_id=1, source_target_pairs={{0,1},{1,0},{2,3},{3,2},{4,5},{5,4},{6,7},{7,6},{8,9},{9,8},{10,11... | collective-permute-start | bytes 2359304 | tf_op jit(solution)/shard_map/ppermute | solution.py:372
  131.4 10.0 %collective-permute-start.16 = (bf16[2,256,512]{2,1,0:T(8,128)(2,1)S(1)}, bf16[2,256,512]{2,1,0:T(8,128)(2,1)}, u32[]{:S(2)}, u32[]{:S(2)}) collective-permute-start(bf16[2,256,512]{2,1,0:T(8,128)(2,1)S(1)} %get-tuple-element.25), channel_id=1, source_target_pairs={{0,1},{1,0},{2,3},{3,2},{4,5},{5,4},{6,7},{7,6},{8,9},{9,8},{10,11... | collective-permute-start | bytes 1572872 | tf_op jit(solution)/shard_map/ppermute | solution.py:372
  135.3 16.4 %all-to-all-start.1 = ((bf16[8,48,512]{2,1,0:T(8,128)(2,1)}), bf16[8,48,512]{2,1,0:T(8,128)(2,1)S(1)}, u32[]{:S(2)}, u32[]{:S(2)}) async-start(bf16[8,48,512]{2,1,0:T(8,128)(2,1)} %bitcast.27), calls=%async_computation.1 | async-start | bytes 786432 | tf_op jit(solution)/shard_map/all_to_all | solution.py:481
  142.5 7.8 %collective-permute-start.17 = (bf16[256,512]{1,0:T(8,128)(2,1)S(1)}, bf16[256,512]{1,0:T(8,128)(2,1)S(1)}, u32[]{:S(2)}, u32[]{:S(2)}) collective-permute-start(bf16[256,512]{1,0:T(8,128)(2,1)S(1)} %get-tuple-element.26), channel_id=1, source_target_pairs={{0,2},{1,3},{2,0},{3,1},{4,6},{5,7},{6,4},{7,5},{8,10},{9,11},{10,... | collective-permute-start | bytes 786440 | tf_op jit(solution)/shard_map/ppermute | solution.py:377
  (14 other events, 113.3 us)

commit v2 on v0

v2 whole, which is shorter than its diff:
```python
import functools
import math

import jax
import jax.numpy as jnp
import numpy as np
from jax import lax
from jax.experimental import pallas as pl
from jax.experimental.pallas import tpu as pltpu
from jax.sharding import PartitionSpec as P


HEADS = 16
KV_HEADS = 4
HEAD_DIM = 64
GRID_W = 64
EPSILON = 1e-06
ROUTED_SCALE = 2.5
LOG2E = 1.4426950408889634
BF = jnp.bfloat16
F32 = jnp.float32
VMEM = pl.BlockSpec(memory_space=pltpu.VMEM)
HBM = pl.BlockSpec(memory_space=pltpu.HBM)


def params(mib):
    return pltpu.CompilerParams(vmem_limit_bytes=mib * 1024 * 1024)


def cost(flops, bytes_accessed, exps=0):
    return pl.CostEstimate(
        flops=int(flops), bytes_accessed=int(bytes_accessed), transcendentals=int(exps)
    )


def in_hbm(arrays):
    return [pltpu.with_memory_space_constraint(a, pltpu.HBM) for a in arrays]


def fetch(sources, targets, sems):
    copies = [
        pltpu.make_async_copy(a, b, sems.at[i]) for i, (a, b) in enumerate(zip(sources, targets))
    ]
    for copy in copies:
        copy.start()
    return copies


def wait(copies):
    for copy in copies:
        copy.wait()


def room(arrays):
    return [pltpu.VMEM(a.shape, a.dtype) for a in arrays] + [
        pltpu.SemaphoreType.DMA((len(arrays),))
    ]


def dot(a, b, dims=((1,), (0,))):
    return lax.dot_general(a, b, (dims, ((), ())), preferred_element_type=F32)


def rotate_block(x, gain, table_ref, grid_rows, g):
    lane = lax.broadcasted_iota(jnp.int32, x.shape, 1)
    squares = x * x
    first = lane < HEAD_DIM
    sum_a = jnp.sum(jnp.where(first, squares, 0.0), axis=1, keepdims=True)
    sum_b = jnp.sum(jnp.where(first, 0.0, squares), axis=1, keepdims=True)
    mean = jnp.where(first, sum_a, sum_b) * (1.0 / HEAD_DIM)
    y = x * lax.rsqrt(mean + EPSILON) * gain
    by_row = lane % 32 < 16
    height = grid_rows + GRID_W
    cosine = jnp.where(by_row, table_ref[g : g + 1, :], table_ref[grid_rows:height, :])
    sine = jnp.where(
        by_row,
        table_ref[height + g : height + g + 1, :],
        table_ref[height + grid_rows : 2 * height, :],
    )
    swapped = jnp.where(lane % HEAD_DIM < 32, pltpu.roll(y, 96, 1), pltpu.roll(y, 32, 1))
    return y * cosine + swapped * sine


def key_kernel(
    heads, key_hbm, value_hbm, gain_hbm, inverse_hbm, out_ref, table_ref, key_ref, value_ref,
    gain_ref, inverse_ref, sems,
):
    kv_index = lax.axis_index("tp") * heads * KV_HEADS // HEADS
    cols = pl.ds(pl.multiple_of(kv_index // 2 * 128, 128), 128)
    copies = fetch(
        [inverse_hbm, gain_hbm, key_hbm.at[:, cols], value_hbm.at[:, cols]],
        [inverse_ref, gain_ref, key_ref, value_ref],
        sems,
    )
    wait(copies[:1])
    local_rows = key_ref.shape[0]
    grid_rows = local_rows // GRID_W
    height = grid_rows + GRID_W
    index = lax.broadcasted_iota(jnp.int32, (height, 128), 0)
    place = jnp.where(
        index < grid_rows, lax.axis_index("ep") * grid_rows + index, index - grid_rows
    )
    angle = place.astype(F32) * inverse_ref[...]
    lanes = lax.broadcasted_iota(jnp.int32, (height, 128), 1)
    table_ref[:height, :] = jnp.cos(angle)
    sine = jnp.sin(angle)
    table_ref[height:, :] = jnp.where(lanes % HEAD_DIM < HEAD_DIM // 2, -sine, sine)
    odd = kv_index % 2 == 1
    wait(copies[1:])
    gain = jnp.concatenate([gain_ref[...]] * 2, axis=1)
    lane = lax.broadcasted_iota(jnp.int32, (GRID_W, 128), 1)
    for g in range(grid_rows):
        rows = slice(g * GRID_W, (g + 1) * GRID_W)
        keys = key_ref[rows, :].astype(F32)
        values = value_ref[rows, :].astype(F32)
        turned = rotate_block(keys, gain, table_ref, grid_rows, g)
        turned = jnp.where(odd, pltpu.roll(turned, 64, 1), turned)
        values = jnp.where(odd, values, pltpu.roll(values, 64, 1))
        out_ref[rows, :] = jnp.where(lane < HEAD_DIM, turned, values).astype(BF)


def prepare_keys(key_rows, value_rows, gain, heads):
    local_rows = key_rows.shape[0]
    height = local_rows // GRID_W + GRID_W
    quarter = HEAD_DIM // 4
    inverse = 10000.0 ** (-np.arange(quarter, dtype=np.float32) / quarter)
    inverse = jnp.asarray(np.tile(inverse, 128 // quarter)[None, :], F32)
    args = (key_rows, value_rows, gain[None, :], inverse)
    return pl.pallas_call(
        functools.partial(key_kernel, heads),
        in_specs=[HBM] * 4,
        out_specs=[VMEM] * 2,
        out_shape=[
            jax.ShapeDtypeStruct((local_rows, 128), BF),
            jax.ShapeDtypeStruct((2 * height, 128), F32),
        ],
        scratch_shapes=[pltpu.VMEM((local_rows, 128), BF)] * 2 + room(args[2:])[:2]
        + [pltpu.SemaphoreType.DMA((4,))],
        compiler_params=params(8),
        cost_estimate=cost(1e9, 3e5),
        name="keys",
    )(*in_hbm(args))


def attention_kernel(heads, tile, chunk, n_kv, q_hbm, gain_hbm, table_hbm, *rest):
    kv_refs = rest[:n_kv]
    att_ref, qs_ref, sa_ref, sb_ref, o_ref, kt_ref, q_ref, gain_ref, table_ref, sems = rest[n_kv:]
    copies = fetch([q_hbm, gain_hbm, table_hbm], [q_ref, gain_ref, table_ref], sems)
    local_rows = q_ref.shape[0]
    grid_rows = local_rows // GRID_W
    blocks = [ref.at[b] for ref in kv_refs for b in range(ref.shape[0])]
    for i, ref in enumerate(blocks):
        kt_ref[:, i * local_rows : (i + 1) * local_rows] = ref[...].astype(F32).T.astype(BF)
    keys = len(blocks) * local_rows
    wait(copies)
    lane = lax.broadcasted_iota(jnp.int32, (GRID_W, 128), 1)
    gain = jnp.concatenate([gain_ref[...]] * 2, axis=1)
    pairs = q_ref.shape[1] // 128
    for pair in range(pairs):
        for g in range(grid_rows):
            x = q_ref[g * GRID_W : (g + 1) * GRID_W, pair * 128 : (pair + 1) * 128].astype(F32)
            turned = rotate_block(x, gain, table_ref, grid_rows, g)
            turned = turned.astype(BF).astype(F32) * HEAD_DIM ** (-0.5)
            for k in range(min(2, heads - 2 * pair)):
                own = turned if k == 0 else pltpu.roll(turned, 64, 1)
                start = (2 * pair + k) * local_rows + g * GRID_W
                qs_ref[start : start + GRID_W, :] = jnp.where(lane < HEAD_DIM, own, 0.0).astype(BF)

    def score(q, s_ref, at, peak):
        s = dot(q, kt_ref[:, at : at + chunk]) * LOG2E
        s_ref[:, at : at + chunk] = s
        for c in range(0, chunk, 128):
            part = s[:, c : c + 128]
            peak = part if peak is None else jnp.maximum(peak, part)
        return peak

    tiles = heads * local_rows // tile
    buffers = (sa_ref, sb_ref)
    peak = None
    for at in range(0, keys, chunk):
        peak = score(qs_ref[:tile, :], sa_ref, at, peak)
    peak = jnp.max(peak, axis=1, keepdims=True)
    for i in range(tiles):
        begin = i * tile
        total = jnp.zeros((tile, 128), F32)
        accum = jnp.zeros((tile, 128), F32)
        next_peak = None
        for at in range(0, keys, chunk):
            if i + 1 < tiles:
                q = qs_ref[begin + tile : begin + 2 * tile, :]
                next_peak = score(q, buffers[(i + 1) % 2], at, next_peak)
            e = jnp.exp2(buffers[i % 2][:, at : at + chunk] - peak)
            for c in range(0, chunk, 128):
                total = total + e[:, c : c + 128]
            e = e.astype(BF)
            for c in range(0, chunk, local_rows):
                accum = accum + dot(e[:, c : c + local_rows], blocks[(at + c) // local_rows][...])
        o_ref[begin : begin + tile, :] = accum / jnp.sum(total, axis=1, keepdims=True)
        if i + 1 < tiles:
            peak = jnp.max(next_peak, axis=1, keepdims=True)
    wide = lax.broadcasted_iota(jnp.int32, (local_rows, 128), 1)
    for pair in range(pairs):
        start = 2 * pair * local_rows
        low = pltpu.roll(o_ref[start : start + local_rows, :], 64, 1)
        if heads > 2 * pair + 1:
            high = o_ref[start + local_rows : start + 2 * local_rows, :]
        else:
            high = jnp.zeros((local_rows, 128), F32)
        att_ref[:, pair * 128 : (pair + 1) * 128] = jnp.where(wide < HEAD_DIM, low, high).astype(BF)


def attention(query_rows, kv_list, gain, table):
    local_rows, width = query_rows.shape
    heads = width // HEAD_DIM
    if width % 128:
        query_rows = jnp.pad(query_rows, ((0, 0), (0, 64)))
    keys = sum(k.shape[0] * k.shape[1] for k in kv_list)
    chunk = 2 * local_rows if keys % (2 * local_rows) == 0 else local_rows
    tile = 256 if heads * local_rows % 256 == 0 else 128
    args = (query_rows, gain[None, :], table)
    attended = pl.pallas_call(
        functools.partial(attention_kernel, heads, tile, chunk, len(kv_list)),
        in_specs=[HBM] * 3 + [VMEM] * len(kv_list),
        out_specs=VMEM,
        out_shape=jax.ShapeDtypeStruct(query_rows.shape, BF),
        scratch_shapes=[
            pltpu.VMEM((heads * local_rows, 128), BF),
            pltpu.VMEM((tile, keys), F32),
            pltpu.VMEM((tile, keys), F32),
            pltpu.VMEM((heads * local_rows, 128), F32),
            pltpu.VMEM((128, keys), BF),
        ]
        + room(args),
        compiler_params=params(24),
        cost_estimate=cost(8e9, 2e6, heads * local_rows * keys),
        name="attention",
    )(*in_hbm(args), *kv_list)
    return attended[:, :width]


def project_kernel(counts, block, *refs):
    att_refs, rest = refs[: len(counts)], refs[len(counts) :]
    w_refs = []
    for count in counts:
        w_refs.append(rest[:count])
        rest = rest[count:]
    gain_ref, out_ref, sum_ref = rest
    rows, model = out_ref.shape
    squares = jnp.zeros((rows, 128), F32)
    for at in range(0, model, block):
        total = None
        for a, parts in zip(att_refs, w_refs):
            part, row = None, 0
            for w in parts:
                term = dot(a[:, row : row + w.shape[0]], w[:, at : at + block])
                part = term if part is None else part + term
                row += w.shape[0]
            part = part.astype(BF).astype(F32)
            total = part if total is None else total + part
        sum_ref[:, at : at + block] = total
        for c in range(0, block, 128):
            squares = squares + total[:, c : c + 128] * total[:, c : c + 128]
    mean = jnp.sum(squares, axis=1, keepdims=True) * (1.0 / model)
    scale = lax.rsqrt(mean + EPSILON)
    for at in range(0, model, block):
        cols = slice(at, at + block)
        out_ref[:, cols] = (sum_ref[:, cols] * scale * gain_ref[:, cols]).astype(BF)


def project(att_list, w_list, gain):
    rows, model = att_list[0].shape[0], w_list[0][0].shape[1]
    args = (*att_list, *(w for parts in w_list for w in parts), gain[None, :])
    return pl.pallas_call(
        functools.partial(project_kernel, [len(w) for w in w_list], min(256, model)),
        in_specs=[VMEM] * len(args),
        out_specs=VMEM,
        out_shape=jax.ShapeDtypeStruct((rows, model), BF),
        scratch_shapes=[pltpu.VMEM((rows, model), F32)],
        compiler_params=params(32),
        cost_estimate=cost(2e9, 6e6),
        name="project",
    )(*args)


def route_kernel(
    experts, cap, ids_hbm, score_hbm, x_hbm, gain_hbm, normed_ref, plan_hbm, out_hbm, plan_ref,
    out_ref, idst_ref, score_ref, x_ref, gain_ref, sems, out_sems,
):
    copies = fetch(
        [ids_hbm, score_hbm, gain_hbm, x_hbm], [idst_ref, score_ref, gain_ref, x_ref], sems
    )
    wait(copies[:2])
    top, rows = idst_ref.shape
    names = lax.broadcasted_iota(jnp.int32, (experts, rows), 0)
    hits = [idst_ref[k : k + 1, :] == names for k in range(top)]
    named = functools.reduce(jnp.logical_or, hits)
    r0 = lax.broadcasted_iota(jnp.int32, (rows, rows), 0)
    r1 = lax.broadcasted_iota(jnp.int32, (rows, rows), 1)
    above = jnp.where(r0 < r1, 1.0, 0.0).astype(BF)
    count = dot(jnp.where(named, 1.0, 0.0).astype(BF), above)
    scores = [score_ref[k : k + 1, :] for k in range(top)]
    score_sum = functools.reduce(jnp.add, scores)
    lines = []
    for k in range(top):
        rank = jnp.sum(jnp.where(hits[k], count, 0.0), axis=0, keepdims=True)
        lines.append((idst_ref[k : k + 1, :] * cap).astype(F32) + rank)
    lines += [s / score_sum * ROUTED_SCALE for s in scores]
    lines += [jnp.zeros((8 - 2 * top, rows), F32)]
    plan_ref[...] = jnp.concatenate(lines, axis=0).T
    sent = [pltpu.make_async_copy(plan_ref, plan_hbm, out_sems.at[0])]
    sent[0].start()
    wait(copies[2:])
    x = x_ref[...].astype(F32)
    mean = jnp.mean(x * x, axis=1, keepdims=True)
    normed_ref[...] = (x * lax.rsqrt(mean + EPSILON) * gain_ref[...]).astype(BF)
    place = jnp.where(named, count.astype(jnp.int32), -1)
    width = out_ref.shape[2]
    lane = lax.axis_index("tp")
    own = normed_ref[:, pl.ds(pl.multiple_of(lane * width, 128), width)]
    slots = lax.broadcasted_iota(jnp.int32, (cap, rows), 0)
    for e in range(experts):
        pick = jnp.where(place[e : e + 1, :] == slots, 1.0, 0.0).astype(BF)
        out_ref[e] = dot(pick, own).astype(BF)
        sent.append(pltpu.make_async_copy(out_ref.at[e], out_hbm.at[e], out_sems.at[1 + e]))
        sent[-1].start()
    wait(sent)


def route(expert_ids, gate_score, expert_input, gain, experts, cap, width):
    rows = expert_ids.shape[0]
    args = (expert_ids.T, gate_score.T, expert_input, gain[None, :])
    outs = [
        jax.ShapeDtypeStruct(expert_input.shape, BF),
        jax.ShapeDtypeStruct((rows, 8), F32),
        jax.ShapeDtypeStruct((experts, cap, width), BF),
    ]
    return pl.pallas_call(
        functools.partial(route_kernel, experts, cap),
        in_specs=[HBM] * 4,
        out_specs=[VMEM, HBM, HBM],
        out_shape=outs[:1] + [pltpu.HBM(a.shape, a.dtype) for a in outs[1:]],
        scratch_shapes=room(outs[1:])[:2]
        + room(args)
        + [pltpu.SemaphoreType.DMA((experts + 1,))],
        compiler_params=params(16),
        cost_estimate=cost(1e9, 4e6),
        name="route",
    )(*in_hbm(args))


def loads_of(hidden):
    return 2 if hidden % 512 == 0 else 1


def mlp_kernel(n_x, halves, offsets, early, late, chunk, *refs):
    x_refs, refs = refs[:n_x], refs[n_x:]
    if late:
        partial_ref, refs = refs[0], refs[1:]
    gate_hbm, up_hbm, refs = refs[0], refs[1], refs[2:]
    if early:
        out_ref, gate_ref, up_ref, sems = refs
    else:
        down_hbm, send_ref, keep_ref, gate_ref, up_ref, sems, h_ref, down_ref = refs
    lane = lax.axis_index("tp")
    chip, side = lane // 2, lane % 2
    hidden = gate_ref.shape[1]
    block = min(256, hidden // loads_of(hidden))
    rows, row = [], 0
    for ref, offset in zip(x_refs, offsets):
        size = ref.shape[1]
        begin = 0
        if offset is not None:
            source = 2 * lax.rem(chip + halves - offset[0], halves)
            source = source + (side if offset[1] == 0 else 1 - side)
            begin = pl.multiple_of(source * size, 128)
        rows.append((pl.ds(begin, size), slice(row, row + size)))
        row += size
    loads = loads_of(hidden)
    load = hidden // loads
    groups = []
    for at in range(0, hidden, load):
        cols = slice(at, at + load)
        groups.append(
            [
                (w_hbm.at[0, there, cols], w_ref.at[here, cols])
                for w_hbm, w_ref in ((gate_hbm, gate_ref), (up_hbm, up_ref))
                for there, here in rows
            ]
        )
    if not early:
        width = send_ref.shape[2]
        goals = [(1 - side, step, send_ref) for step in range(halves)]
        goals += [(side, step, keep_ref) for step in range(halves)]
        groups.append([])
        for i, (core, step, unused) in enumerate(goals):
            goal = 2 * lax.rem(chip + step, halves) + core
            begin = pl.multiple_of(goal * width, 128)
            groups[-1].append((down_hbm.at[0, :, pl.ds(begin, width)], down_ref.at[i]))
    number = 0
    for i, group in enumerate(groups):
        groups[i] = [
            pltpu.make_async_copy(x, y, sems.at[number + j]) for j, (x, y) in enumerate(group)
        ]
        number += len(group)

    def start(i):
        for copy in groups[i] if i < len(groups) else ():
            copy.start()

    start(0)
    if loads > 1:
        start(1)

    def product(w_ref, cols):
        total = None
        for ref, (unused, here) in zip(x_refs, rows):
            term = dot(ref[...], w_ref[here, cols])
            total = term if total is None else total + term
        return total

    for at in range(0, hidden, block):
        cols = slice(at, at + block)
        if at % load == 0:
            wait(groups[at // load])
            start(at // load + min(2, loads))
        gate = product(gate_ref, cols)
        up = product(up_ref, cols)
        if late:
            taken = slice(chunk * gate.shape[0], (chunk + 1) * gate.shape[0])
            gate = gate + partial_ref[0, taken, cols]
            up = up + partial_ref[1, taken, cols]
        if early:
            out_ref[0, :, cols] = gate
            out_ref[1, :, cols] = up
        else:
            h_ref[:, cols] = (gate / (1.0 + jnp.exp(-gate)) * up).astype(BF)
    if early:
        return
    inner = min(256, width)
    wait(groups[-1])
    for i, (unused, step, out) in enumerate(goals):
        for at in range(0, width, inner):
            cols = slice(at, at + inner)
            out[step, :, cols] = dot(h_ref[...], down_ref[i, :, cols]).astype(BF)


def mlp(x_list, offsets, weights, halves, early=False, partial=None, chunk=0):
    rows = x_list[0].shape[0]
    model, hidden = weights[0].shape[1:]
    width = model // (2 * halves)
    depth = sum(x.shape[1] for x in x_list)
    n_copies = 2 * len(x_list) * loads_of(hidden)
    if early:
        weights = weights[:2]
        outs = [jax.ShapeDtypeStruct((2, rows, hidden), F32)]
    else:
        n_copies += 2 * halves
        outs = [jax.ShapeDtypeStruct((halves, rows, width), BF)] * 2
    scratch = [pltpu.VMEM((depth, hidden), BF)] * 2 + [pltpu.SemaphoreType.DMA((n_copies,))]
    if not early:
        scratch += [pltpu.VMEM((rows, hidden), BF), pltpu.VMEM((2 * halves, hidden, width), BF)]
    late = [] if partial is None else [partial]
    flops = 4 * rows * depth * hidden + (0 if early else 2 * rows * model * hidden)
    return pl.pallas_call(
        functools.partial(mlp_kernel, len(x_list), halves, offsets, early, bool(late), chunk),
        in_specs=[VMEM] * len(x_list + late) + [HBM] * len(weights),
        out_specs=[VMEM] * len(outs),
        out_shape=outs,
        scratch_shapes=scratch,
        compiler_params=params(24),
        cost_estimate=cost(flops, 6 * model * hidden),
    )(*x_list, *late, *in_hbm(weights))


def small_call(kernel, args, outs, scratch=()):
    return pl.pallas_call(
        kernel,
        in_specs=[VMEM] * len(args),
        out_specs=[HBM if isinstance(o, type(pltpu.HBM((8, 128), F32))) else VMEM for o in outs],
        out_shape=outs,
        scratch_shapes=list(scratch),
        compiler_params=params(4),
        cost_estimate=cost(1e8, 2e6),
    )(*args)


def split_kernel(in_ref, *outs):
    for i, out in enumerate(outs):
        out[...] = in_ref[i]


def split(x):
    shape = jax.ShapeDtypeStruct(x.shape[1:], x.dtype)
    return small_call(split_kernel, [x], [shape] * x.shape[0])


def stack_kernel(*refs):
    for i, ref in enumerate(refs[:-1]):
        refs[-1][i] = ref[...]


def stack(arrays):
    shape = jax.ShapeDtypeStruct((len(arrays), *arrays[0].shape), arrays[0].dtype)
    return small_call(stack_kernel, arrays, [shape])[0]


def add_kernel(a_ref, b_ref, *outs):
    for i, out in enumerate(outs):
        out[...] = (a_ref[1 + i].astype(F32) + b_ref[1 + i].astype(F32)).astype(BF)


def add_terms(keep, received):
    shape = jax.ShapeDtypeStruct(keep.shape[1:], BF)
    return small_call(add_kernel, [keep, received], [shape] * (keep.shape[0] - 1))


def finish_kernel(counts, *refs):
    refs, out_hbm, out_ref, sems = refs[:-3], refs[-3], refs[-2], refs[-1]
    width = out_ref.shape[2]
    blocks = out_ref.shape[0] // len(counts)
    copies = []
    for h, count in enumerate(counts):
        keep, received, others = refs[0], refs[1], refs[2:count]
        refs = refs[count:]
        total = keep[0].astype(F32) + received[0].astype(F32)
        for other in others:
            total = total + other[...].astype(F32)
        at = h * blocks
        out_ref[at : at + blocks] = total.astype(BF).reshape(blocks, out_ref.shape[1], width)
        copies.append(
            pltpu.make_async_copy(
                out_ref.at[at : at + blocks], out_hbm.at[at : at + blocks], sems.at[h]
            )
        )
        copies[-1].start()
    wait(copies)


def finish(groups, shape):
    return small_call(
        functools.partial(finish_kernel, [len(g) for g in groups]),
        [a for g in groups for a in g],
        [pltpu.HBM(shape, BF)],
        [pltpu.VMEM(shape, BF), pltpu.SemaphoreType.DMA((shape[0],))],
    )[0]


def combine_kernel(top, plan_hbm, slots_ref, keep_ref, received_ref, *refs):
    others, (out_ref, plan_ref, sems) = refs[:-3], refs[-3:]
    copies = fetch([plan_hbm], [plan_ref], sems)
    rows = plan_ref.shape[0]
    experts, cap, width = slots_ref.shape
    n = lax.broadcasted_iota(jnp.int32, (rows, experts * cap), 1)
    total = keep_ref[0].astype(F32) + received_ref[0].astype(F32)
    for other in others:
        total = total + other[...].astype(F32)
    wait(copies)
    for k in range(top):
        pick = jnp.where(n == plan_ref[:, k : k + 1].astype(jnp.int32), 1.0, 0.0).astype(BF)
        picked = dot(pick, slots_ref[...].reshape(experts * cap, width))
        total = total + picked * plan_ref[:, top + k : top + k + 1]
    out_ref[...] = total.astype(BF)


def combine(plan, top, slots, keep, received, others):
    rows = plan.shape[0]
    args = (slots, keep, received, *others)
    return pl.pallas_call(
        functools.partial(combine_kernel, top),
        in_specs=[HBM] + [VMEM] * len(args),
        out_specs=VMEM,
        out_shape=jax.ShapeDtypeStruct((rows, slots.shape[2]), BF),
        scratch_shapes=room([plan]),
        compiler_params=params(16),
        cost_estimate=cost(8e8, 2e6),
        name="combine",
    )(*in_hbm([plan]), *args)


def core_swap(x):
    n = lax.axis_size("tp")
    return lax.ppermute(x, "tp", [(i, i ^ 1) for i in range(n)])


def chip_shift(x, step):
    n = lax.axis_size("tp")
    return lax.ppermute(x, "tp", [(i, (i + 2 * step) % n) for i in range(n)])


def gather_lanes(x, halves):
    mine = [x] + [chip_shift(x, s) for s in range(1, halves)]
    other = [core_swap(m) for m in mine]
    offsets = [(s, 0) for s in range(halves)] + [(s, 1) for s in range(halves)]
    return mine + other, offsets


def scatter_chips(keep, received):
    terms = add_terms(keep, received)
    return [chip_shift(t, s + 1) for s, t in enumerate(terms)]


def ep_gather(x, axis_z, axis_x):
    n = lax.axis_size("ep")
    own = [x]
    for step in range(1, axis_z):
        own.append(lax.ppermute(x, "ep", [(i, (i + step * axis_x) % n) for i in range(n)]))
    stacked = stack(own)
    groups = [stacked]
    for step in range(1, axis_x):
        perm = [(i, i // axis_x * axis_x + (i + step) % axis_x) for i in range(n)]
        groups.append(lax.ppermute(stacked, "ep", perm))
    return groups


def exchange(x):
    return lax.all_to_all(x, "ep", 0, 0, tiled=True)


def body(
    x_size,
    query_rows,
    key_rows,
    value_rows,
    query_gain,
    key_gain,
    out_weight,
    mixer_gain,
    expert_input,
    expert_ids,
    gate_score,
    expert_gain,
    gate_weight,
    up_weight,
    down_weight,
    shared_gate,
    shared_up,
    shared_down,
):
    return whole_step(
        x_size,
        query_rows,
        key_rows,
        value_rows,
        query_gain,
        key_gain,
        out_weight,
        mixer_gain,
        expert_input,
        expert_ids,
        gate_score,
        expert_gain,
        gate_weight,
        up_weight,
        down_weight,
        shared_gate,
        shared_up,
        shared_down,
    )


def whole_step(
    x_size,
    query_rows,
    key_rows,
    value_rows,
    query_gain,
    key_gain,
    out_weight,
    mixer_gain,
    expert_input,
    expert_ids,
    gate_score,
    expert_gain,
    gate_weight,
    up_weight,
    down_weight,
    shared_gate,
    shared_up,
    shared_down,
):
    ep, tp = lax.axis_size("ep"), lax.axis_size("tp")
    halves = tp // 2
    heads = query_rows.shape[1] // HEAD_DIM
    assert tp > 2 and tp % 2 == 0 and heads <= HEADS // KV_HEADS and gate_weight.shape[0] == 1
    rows, top = expert_ids.shape
    width = expert_input.shape[1] // tp
    cap = 3 * rows * top // (2 * ep)
    chunks = 2
    size = ep * cap // chunks

    part = out_weight.shape[0] // 8 * 7
    parts = [out_weight[:part], out_weight[part:]]
    w_list = [[out_weight]]
    for step in range(1, halves):
        w_list.append([chip_shift(w, step) for w in parts])
    w_list += [[core_swap(w) for w in parts] for parts in w_list]

    normed, plan, outgoing = route(
        expert_ids, gate_score, expert_input, expert_gain, ep, cap, width
    )
    arrived = exchange(outgoing).reshape(chunks * size, width)

    shared = (shared_gate[None], shared_up[None], shared_down[None])
    sh_send, sh_keep = mlp([normed], [None], shared, halves)
    sh_received = core_swap(sh_send)
    sh_others = scatter_chips(sh_keep, sh_received)

    weights = [gate_weight, up_weight, down_weight]
    own_chip = [arrived, core_swap(arrived)]
    (partial,) = mlp(own_chip, [(0, 0), (0, 1)], weights, halves, True)
    results = []
    for h, x in enumerate(split(arrived.reshape(chunks, size, width))):
        mine = [chip_shift(x, s) for s in range(1, halves)]
        other = [core_swap(m) for m in mine]
        offsets = [(s, c) for c in range(2) for s in range(1, halves)]
        send, keep = mlp(mine + other, offsets, weights, halves, partial=partial, chunk=h)
        received = core_swap(send)
        results.append((keep, received, *scatter_chips(keep, received)))
    returned = exchange(finish(results, (ep, cap, width)))
    expert_out = combine(plan, top, returned, sh_keep, sh_received, sh_others)

    kv, table = prepare_keys(key_rows, value_rows, key_gain, heads)
    kv_list = ep_gather(kv, ep // x_size, x_size)
    attended = attention(query_rows, kv_list, query_gain, table)[:, : query_rows.shape[1]]
    att_list, _ = gather_lanes(attended, halves)
    mixer_out = project(att_list, w_list, mixer_gain)
    return (mixer_out, expert_out)


def solution(mesh):
    in_specs = (
        P("ep", "tp"),
        P("ep", None),
        P("ep", None),
        P(),
        P(),
        P("tp", None),
        P(),
        P("ep", None),
        P("ep", None),
        P("ep", None),
        P(),
        P("ep", None, "tp"),
        P("ep", None, "tp"),
        P("ep", "tp", None),
        P(None, "tp"),
        P(None, "tp"),
        P("tp", None),
    )
    out_specs = (P("ep", None), P("ep", "tp"))
    ep = mesh.shape["ep"]
    x_size = 2 ** (int(math.log2(ep)) // 2)
    return jax.shard_map(
        functools.partial(body, x_size),
        mesh=mesh,
        in_specs=in_specs,
        out_specs=out_specs,
        check_vma=False,
    )
```

time: 219 us -> 151 us (0.69)
  matrix products: 58.9 us -> 0 us
  Pallas kernels: 0 us -> 45 us
  blocking collectives: 61.6 us -> 27.4 us
  local copies, waits for them, and re-layouts: 25.5 us -> 1.63 us
  waiting for transfers between devices: 36 us -> 56.9 us
  other arithmetic: 17.9 us -> 0 us
  starting transfers between devices: 3.9 us -> 18.2 us
  between operations: 14.2 us -> 0.96 us
    dot_general x22 -> x0, matrix products: 58.9 us -> none  [the longest x8 19.6 us: step_block(): jnp.einsum('kgqs,skd->kgqd', exponent.astype(jnp.bfloat16), block_values,...]
    ppermute x0 -> x23, waiting for transfers between devices: none -> 56.9 us  [the longest x8 48 us: chip_shift(): return lax.ppermute(x, 'tp', [(i, (i + 2 * step) % n) for i in range(n)])]
    pallas_call x0 -> x15, Pallas kernels: none -> 45 us  [the longest x4 20.9 us: mlp(): pl.pallas_call(functools.partial(mlp_kernel, len(x_list), halves, offsets...]
    psum x1 -> x0, waiting for transfers between devices: 35.9 us -> none  [mixer_half(): lax.psum(partial_value.astype(jnp.bfloat16), 'tp').astype(jnp.float32)]
    all_gather x1 -> x0, blocking collectives: 34.3 us -> none  [mixer_half(): piece = lax.all_gather(stacked, 'ep', axis=0, tiled=True)]
    ppermute x0 -> x23, starting transfers between devices: none -> 14.5 us  [the longest x8 9.46 us: chip_shift(): return lax.ppermute(x, 'tp', [(i, (i + 2 * step) % n) for i in range(n)])]
    dynamic_slice x18 -> x0, local copies, waits for them, and re-layouts: 9.34 us -> none  [the longest x16 8.26 us: mixer_half(): carry, unused = lax.scan(step_block, carry, blocks)]
    reduce_sum x15 -> x0, other arithmetic: 8.17 us -> none  [the longest x8 3.24 us: step_block(): row_total = row_total * shrink + jnp.sum(exponent, axis=3)]
  transfers between devices with their start and end apart: 4 -> 24, of which waited for: 1 -> 10; matrix products, arithmetic and copies ran while one was open for 30% -> 1% of each run, Pallas kernels for 0% -> 27%
where the time goes in v2:
time: 151 us; the launch traced here: 150 us
  waiting for transfers between devices  56.9 us (38%)
  Pallas kernels  45 us (30%)
  blocking collectives  27.4 us (18%)
  starting transfers between devices  18.2 us (12%)
  local copies, waits for them, and re-layouts  1.63 us (1%)
    ppermute x8, waiting for transfers between devices, chip_shift(): return lax.ppermute(x, 'tp', [(i, (i + 2 * step) % n) for i in range(n)])  48 us
    all_to_all x1, blocking collectives, exchange(): return lax.all_to_all(x, 'ep', 0, 0, tiled=True)  27.4 us
    pallas_call x4, Pallas kernels, mlp(): pl.pallas_call(functools.partial(mlp_kernel, len(x_list), halves, offsets...  20.9 us
    ppermute x8, starting transfers between devices, chip_shift(): return lax.ppermute(x, 'tp', [(i, (i + 2 * step) % n) for i in range(n)])  9.46 us
    pallas_call x1, Pallas kernels, attention(): pl.pallas_call(functools.partial(attention_kernel, heads, tile, chunk, le...  9.23 us
    ppermute x3, waiting for transfers between devices, ep_gather(): lax.ppermute(x, 'ep', [(i, (i + step * axis_x) % n) for i in range(n)])  8.16 us
    pallas_call x1, Pallas kernels, project(): pl.pallas_call(functools.partial(project_kernel, [len(w) for w in w_list]...  5.6 us
    all_to_all x1, starting transfers between devices, exchange(): return lax.all_to_all(x, 'ep', 0, 0, tiled=True)  3.74 us
  transfers between devices with their start and end apart: 24, of which 10 were waited for; matrix products, arithmetic and copies ran while one was open for 1% of the time, Pallas kernels for 27%

profile of v2, /device:TPU:0, one launch (start us, length us, event | category | flops | bytes accessed | tf_op | source)
XLA Modules:
  0.0 150.1 jit_solution(13975641908961096539)
XLA Ops:
  0.6 3.0 %route.1 = (bf16[256,2048]{1,0:T(8,128)(2,1)S(1)}, f32[256,8]{1,0:T(8,128)}, bf16[8,96,512]{2,1,0:T(8,128)(2,1)}) custom-call(s32[2,256]{1,0:T(2,128)} %bitcast.19, f32[2,256]{1,0:T(2,128)} %bitcast.20, bf16[256,2048]{1,0:T(8,128)(2,1)} %x_hbm.1, f32[1,2048]{1,0:T(1,128)} %bitcast.18), custom_call_target="tpu_custom_call" | custom-call | flops 1000000000 | bytes 4000000 | tf_op jit(solution)/shard_map/route/pallas_call | solution.py:337
  3.6 27.4 %all_to_all.10 = bf16[8,96,512]{2,1,0:T(8,128)(2,1)S(1)} all-to-all(bf16[8,96,512]{2,1,0:T(8,128)(2,1)} %get-tuple-element.18), channel_id=1, replica_groups=mesh['ep'=8,'tp'=4] {'ep'}, dimensions={0} | all-to-all | bytes 1572864 | tf_op jit(solution)/shard_map/all_to_all | solution.py:616
  31.1 1.6 %collective-permute-start.17 = (bf16[384,512]{1,0:T(8,128)(2,1)S(1)}, bf16[384,512]{1,0:T(8,128)(2,1)S(1)}, u32[]{:S(2)}, u32[]{:S(2)}) collective-permute-start(bf16[384,512]{1,0:T(8,128)(2,1)S(1)} %get-tuple-element.22), channel_id=1, source_target_pairs={{0,2},{1,3},{2,0},{3,1},{4,6},{5,7},{6,4},{7,5},{8,10},{9,11},{10,... | collective-permute-start | bytes 1179656 | tf_op jit(solution)/shard_map/ppermute | solution.py:587
  33.2 10.0 %collective-permute-done.17.refs_0_ = bf16[384,512]{1,0:T(8,128)(2,1)S(1)} collective-permute-done((bf16[384,512]{1,0:T(8,128)(2,1)S(1)}, bf16[384,512]{1,0:T(8,128)(2,1)S(1)}, u32[]{:S(2)}, u32[]{:S(2)}) %collective-permute-start.17) | collective-permute-done | bytes 393248 | tf_op jit(solution)/shard_map/ppermute | solution.py:587
  43.1 8.0 %collective-permute-done.12.refs_0_ = bf16[384,512]{1,0:T(8,128)(2,1)S(1)} collective-permute-done((bf16[384,512]{1,0:T(8,128)(2,1)S(1)}, bf16[384,512]{1,0:T(8,128)(2,1)S(1)}, u32[]{:S(2)}, u32[]{:S(2)}) %collective-permute-start.12) | collective-permute-done | bytes 393248 | tf_op jit(solution)/shard_map/ppermute | solution.py:587
  51.1 5.2 %shard_map.187.refs_2_ = f32[2,768,1024]{2,1,0:T(8,128)S(1)} custom-call(bf16[768,512]{1,0:T(8,128)(2,1)S(1)} %bitcast.13, bf16[768,512]{1,0:T(8,128)(2,1)S(1)} %collective-permute-done.14.refs_1_, bf16[1,2048,1024]{2,1,0:T(8,128)(2,1)} %refs_3_.5, bf16[1,2048,1024]{2,1,0:T(8,128)(2,1)} %refs_4_.5), custom_call_target="tpu_custom_call" | custom-call | flops 3221225472 | bytes 12582912 | tf_op jit(solution)/shard_map/pallas_call | solution.py:464
  56.3 5.9 %shard_map.190 = (bf16[2,384,512]{2,1,0:T(8,128)(2,1)S(1)}, bf16[2,384,512]{2,1,0:T(8,128)(2,1)S(1)}) custom-call(bf16[384,512]{1,0:T(8,128)(2,1)S(1)} %collective-permute-done.17.refs_0_, bf16[384,512]{1,0:T(8,128)(2,1)S(1)} %collective-permute-done.18.refs_1_, f32[2,768,1024]{2,1,0:T(8,128)S(1)} %shard_map.187.refs_2_, bf16[1,2048,1024]{2,1,0:T(8,128)(2,1)} %refs_3_.5, ...), custom_call_target="tpu_custom_call" | custom-call | flops 3221225472 | bytes 12582912 | tf_op jit(solution)/shard_map/pallas_call | solution.py:464
  62.8 5.8 %shard_map.188 = (bf16[2,384,512]{2,1,0:T(8,128)(2,1)S(1)}, bf16[2,384,512]{2,1,0:T(8,128)(2,1)S(1)}) custom-call(bf16[384,512]{1,0:T(8,128)(2,1)S(1)} %collective-permute-done.12.refs_0_, bf16[384,512]{1,0:T(8,128)(2,1)S(1)} %collective-permute-done.13.refs_1_, f32[2,768,1024]{2,1,0:T(8,128)S(1)} %shard_map.187.refs_2_, bf16[1,2048,1024]{2,1,0:T(8,128)(2,1)} %refs_3_.5, ...), custom_call_target="tpu_custom_call" | custom-call | flops 3221225472 | bytes 12582912 | tf_op jit(solution)/shard_map/pallas_call | solution.py:464
  69.7 1.6 %collective-permute-start.7 = (bf16[224,2048]{1,0:T(8,128)(2,1)}, bf16[224,2048]{1,0:T(8,128)(2,1)}, u32[]{:S(2)}, u32[]{:S(2)}) collective-permute-start(bf16[224,2048]{1,0:T(8,128)(2,1)} %slice.6), channel_id=1, source_target_pairs={{0,2},{1,3},{2,0},{3,1},{4,6},{5,7},{6,4},{7,5},{8,10},{9,11},{10,... | collective-permute-start | bytes 2752520 | tf_op jit(solution)/shard_map/ppermute | solution.py:587
  71.2 1.9 %keys.1 = (bf16[384,128]{1,0:T(8,128)(2,1)S(1)}, f32[140,128]{1,0:T(8,128)S(1)}) custom-call(bf16[384,256]{1,0:T(8,128)(2,1)} %key_hbm.1, bf16[384,256]{1,0:T(8,128)(2,1)} %value_hbm.1, f32[1,64]{1,0:T(1,128)} %bitcast.21, f32[1,128]{1,0:T(1,128)} %constant.2.clone.inverse_hbm), custom_call_target="tpu_custom_call" | custom-call | flops 1000000000 | bytes 300000 | tf_op jit(solution)/shard_map/keys/pallas_call | solution.py:129
  75.6 1.6 %collective-permute-start.16 = (bf16[384,512]{1,0:T(8,128)(2,1)S(1)}, bf16[384,512]{1,0:T(8,128)(2,1)S(1)}, u32[]{:S(2)}, u32[]{:S(2)}) collective-permute-start(bf16[384,512]{1,0:T(8,128)(2,1)S(1)} %shard_map.189), channel_id=1, source_target_pairs={{0,2},{1,3},{2,0},{3,1},{4,6},{5,7},{6,4},{7,5},{8,10},{9,11},{10,... | collective-permute-start | bytes 1179656 | tf_op jit(solution)/shard_map/ppermute | solution.py:587
  77.8 3.0 %collective-permute-done.refs_1_ = bf16[384,128]{1,0:T(8,128)(2,1)S(1)} collective-permute-done((bf16[384,128]{1,0:T(8,128)(2,1)S(1)}, bf16[384,128]{1,0:T(8,128)(2,1)S(1)}, u32[]{:S(2)}, u32[]{:S(2)}) %collective-permute-start) | collective-permute-done | bytes 98336 | tf_op jit(solution)/shard_map/ppermute | solution.py:606
  80.8 4.0 %collective-permute-done.1.refs_2_ = bf16[384,128]{1,0:T(8,128)(2,1)S(1)} collective-permute-done((bf16[384,128]{1,0:T(8,128)(2,1)S(1)}, bf16[384,128]{1,0:T(8,128)(2,1)S(1)}, u32[]{:S(2)}, u32[]{:S(2)}) %collective-permute-start.1) | collective-permute-done | bytes 98336 | tf_op jit(solution)/shard_map/ppermute | solution.py:606
  86.7 1.5 collective-permute-start.3
  88.2 13.3 %collective-permute-done.20.refs_5_ = bf16[384,512]{1,0:T(8,128)(2,1)S(1)} collective-permute-done((bf16[384,512]{1,0:T(8,128)(2,1)S(1)}, bf16[384,512]{1,0:T(8,128)(2,1)S(1)}, u32[]{:S(2)}, u32[]{:S(2)}) %collective-permute-start.20) | collective-permute-done | bytes 393248 | tf_op jit(solution)/shard_map/ppermute | solution.py:587
  101.5 7.9 %collective-permute-done.16.refs_2_ = bf16[384,512]{1,0:T(8,128)(2,1)S(1)} collective-permute-done((bf16[384,512]{1,0:T(8,128)(2,1)S(1)}, bf16[384,512]{1,0:T(8,128)(2,1)S(1)}, u32[]{:S(2)}, u32[]{:S(2)}) %collective-permute-start.16) | collective-permute-done | bytes 393248 | tf_op jit(solution)/shard_map/ppermute | solution.py:587
  110.6 3.7 %all-to-all-start.1 = ((bf16[8,96,512]{2,1,0:T(8,128)(2,1)}), bf16[8,96,512]{2,1,0:T(8,128)(2,1)S(1)}, u32[]{:S(2)}, u32[]{:S(2)}) async-start(bf16[8,96,512]{2,1,0:T(8,128)(2,1)} %shard_map.192), calls=%async_computation.1 | async-start | bytes 1572864 | tf_op jit(solution)/shard_map/all_to_all | solution.py:616
  114.3 4.0 %shard_map.193 = (bf16[2,256,512]{2,1,0:T(8,128)(2,1)S(1)}, bf16[2,256,512]{2,1,0:T(8,128)(2,1)S(1)}) custom-call(bf16[256,2048]{1,0:T(8,128)(2,1)S(1)} %get-tuple-element.25.refs_0_, bf16[1,2048,512]{2,1,0:T(8,128)(2,1)} %bitcast.15, bf16[1,2048,512]{2,1,0:T(8,128)(2,1)} %bitcast.16, bf16[1,512,2048]{2,1,0:T(8,128)(2,1)} %bitcast.17), custom_call_target="tpu_custom_call" | custom-call | flops 1610612736 | bytes 6291456 | tf_op jit(solution)/shard_map/pallas_call | solution.py:464
  118.9 9.2 %attention.1.refs_0_ = bf16[384,256]{1,0:T(8,128)(2,1)S(1)} custom-call(bf16[384,256]{1,0:T(8,128)(2,1)} %q_hbm.1, f32[1,64]{1,0:T(1,128)} %bitcast.22, f32[140,128]{1,0:T(8,128)} %copy-done.2, bf16[4,384,128]{2,1,0:T(8,128)(2,1)} %shard_map.185.rest_0_, bf16[4,384,128]{2,1,0:T(8,128)(2,1)} %collective-permute-done.3.rest_1_), custom_call_target="tpu_custom_call" | custom-call | flops 8000000000 | bytes 2000000 | tf_op jit(solution)/shard_map/attention/pallas_call | solution.py:221
  128.2 1.6 %collective-permute-start.4 = (bf16[384,256]{1,0:T(8,128)(2,1)S(1)}, bf16[384,256]{1,0:T(8,128)(2,1)S(1)}, u32[]{:S(2)}, u32[]{:S(2)}) collective-permute-start(bf16[384,256]{1,0:T(8,128)(2,1)S(1)} %attention.1.refs_0_), channel_id=1, source_target_pairs={{0,2},{1,3},{2,0},{3,1},{4,6},{5,7},{6,4},{7,5},{8,10},{9,11},{10,... | collective-permute-start | bytes 589832 | tf_op jit(solution)/shard_map/ppermute | solution.py:587
  130.4 7.6 %collective-permute-done.8.refs_6_ = bf16[32,2048]{1,0:T(8,128)(2,1)S(1)} collective-permute-done((bf16[32,2048]{1,0:T(8,128)(2,1)S(1)}, bf16[32,2048]{1,0:T(8,128)(2,1)S(1)}, u32[]{:S(2)}, u32[]{:S(2)}) %collective-permute-start.8) | collective-permute-done | bytes 131104 | tf_op jit(solution)/shard_map/ppermute | solution.py:587
  139.3 1.5 collective-permute-start.22
  140.8 5.6 %project.1 = bf16[384,2048]{1,0:T(8,128)(2,1)} custom-call(bf16[384,256]{1,0:T(8,128)(2,1)S(1)} %attention.1.refs_0_, bf16[384,256]{1,0:T(8,128)(2,1)S(1)} %collective-permute-done.4.refs_1_, bf16[384,256]{1,0:T(8,128)(2,1)S(1)} %collective-permute-done.5.refs_2_, bf16[384,256]{1,0:T(8,128)(2,1)S(1)} %collective-permute-done.6.refs_3_, ...), custom_call_target="tpu_custom_call" | custom-call | flops 2000000000 | bytes 6000000 | tf_op jit(solution)/shard_map/project/pallas_call | solution.py:273
  147.7 2.2 %combine.1 = bf16[256,512]{1,0:T(8,128)(2,1)} custom-call(f32[256,8]{1,0:T(8,128)} %get-tuple-element.17.plan_hbm, bf16[8,96,512]{2,1,0:T(8,128)(2,1)S(1)} %all-to-all-done.1.slots_ref, bf16[2,256,512]{2,1,0:T(8,128)(2,1)S(1)} %get-tuple-element.26.a_ref.keep_ref, bf16[2,256,512]{2,1,0:T(8,128)(2,1)S(1)} %collective-permute-done.21.b_ref.received_ref, ...), custom_call_target="tpu_custom_call" | custom-call | flops 800000000 | bytes 2000000 | tf_op jit(solution)/shard_map/combine/pallas_call | solution.py:568
  (48 shorter events, 12.1 us)
Async XLA Ops:
  31.0 20.1 %collective-permute-start.14 = (bf16[768,512]{1,0:T(8,128)(2,1)S(1)}, bf16[768,512]{1,0:T(8,128)(2,1)S(1)}, u32[]{:S(2)}, u32[]{:S(2)}) collective-permute-start(bf16[768,512]{1,0:T(8,128)(2,1)S(1)} %bitcast.11), channel_id=1, source_target_pairs={{0,1},{1,0},{2,3},{3,2},{4,5},{5,4},{6,7},{7,6},{8,9},{9,8},{10,11... | collective-permute-start | bytes 2359304 | tf_op jit(solution)/shard_map/ppermute | solution.py:582
  31.1 12.1 %collective-permute-start.17 = (bf16[384,512]{1,0:T(8,128)(2,1)S(1)}, bf16[384,512]{1,0:T(8,128)(2,1)S(1)}, u32[]{:S(2)}, u32[]{:S(2)}) collective-permute-start(bf16[384,512]{1,0:T(8,128)(2,1)S(1)} %get-tuple-element.22), channel_id=1, source_target_pairs={{0,2},{1,3},{2,0},{3,1},{4,6},{5,7},{6,4},{7,5},{8,10},{9,11},{10,... | collective-permute-start | bytes 1179656 | tf_op jit(solution)/shard_map/ppermute | solution.py:587
  32.7 18.4 %collective-permute-start.12 = (bf16[384,512]{1,0:T(8,128)(2,1)S(1)}, bf16[384,512]{1,0:T(8,128)(2,1)S(1)}, u32[]{:S(2)}, u32[]{:S(2)}) collective-permute-start(bf16[384,512]{1,0:T(8,128)(2,1)S(1)} %get-tuple-element.19), channel_id=1, source_target_pairs={{0,2},{1,3},{2,0},{3,1},{4,6},{5,7},{6,4},{7,5},{8,10},{9,11},{10,... | collective-permute-start | bytes 1179656 | tf_op jit(solution)/shard_map/ppermute | solution.py:587
  43.1 13.2 %collective-permute-start.18 = (bf16[384,512]{1,0:T(8,128)(2,1)S(1)}, bf16[384,512]{1,0:T(8,128)(2,1)S(1)}, u32[]{:S(2)}, u32[]{:S(2)}) collective-permute-start(bf16[384,512]{1,0:T(8,128)(2,1)S(1)} %collective-permute-done.17.refs_0_), channel_id=1, source_target_pairs={{0,1},{1,0},{2,3},{3,2},{4,5},{5,4},{6,7},{7,6},{8,9},{9,8},{10,11... | collective-permute-start | bytes 1179656 | tf_op jit(solution)/shard_map/ppermute | solution.py:582
  51.1 11.7 %collective-permute-start.13 = (bf16[384,512]{1,0:T(8,128)(2,1)S(1)}, bf16[384,512]{1,0:T(8,128)(2,1)S(1)}, u32[]{:S(2)}, u32[]{:S(2)}) collective-permute-start(bf16[384,512]{1,0:T(8,128)(2,1)S(1)} %collective-permute-done.12.refs_0_), channel_id=1, source_target_pairs={{0,1},{1,0},{2,3},{3,2},{4,5},{5,4},{6,7},{7,6},{8,9},{9,8},{10,11... | collective-permute-start | bytes 1179656 | tf_op jit(solution)/shard_map/ppermute | solution.py:582
  62.2 12.6 %collective-permute-start.19 = (bf16[2,384,512]{2,1,0:T(8,128)(2,1)S(1)}, bf16[2,384,512]{2,1,0:T(8,128)(2,1)S(1)}, u32[]{:S(2)}, u32[]{:S(2)}) collective-permute-start(bf16[2,384,512]{2,1,0:T(8,128)(2,1)S(1)} %get-tuple-element.24), channel_id=1, source_target_pairs={{0,1},{1,0},{2,3},{3,2},{4,5},{5,4},{6,7},{7,6},{8,9},{9,8},{10,11... | collective-permute-start | bytes 2359304 | tf_op jit(solution)/shard_map/ppermute | solution.py:582
  68.6 6.9 %collective-permute-start.15 = (bf16[2,384,512]{2,1,0:T(8,128)(2,1)S(1)}, bf16[2,384,512]{2,1,0:T(8,128)(2,1)S(1)}, u32[]{:S(2)}, u32[]{:S(2)}) collective-permute-start(bf16[2,384,512]{2,1,0:T(8,128)(2,1)S(1)} %get-tuple-element.21), channel_id=1, source_target_pairs={{0,1},{1,0},{2,3},{3,2},{4,5},{5,4},{6,7},{7,6},{8,9},{9,8},{10,11... | collective-permute-start | bytes 2359304 | tf_op jit(solution)/shard_map/ppermute | solution.py:582
  69.7 48.8 %collective-permute-start.7 = (bf16[224,2048]{1,0:T(8,128)(2,1)}, bf16[224,2048]{1,0:T(8,128)(2,1)}, u32[]{:S(2)}, u32[]{:S(2)}) collective-permute-start(bf16[224,2048]{1,0:T(8,128)(2,1)} %slice.6), channel_id=1, source_target_pairs={{0,2},{1,3},{2,0},{3,1},{4,6},{5,7},{6,4},{7,5},{8,10},{9,11},{10,... | collective-permute-start | bytes 2752520 | tf_op jit(solution)/shard_map/ppermute | solution.py:587
  73.8 7.0 %collective-permute-start = (bf16[384,128]{1,0:T(8,128)(2,1)S(1)}, bf16[384,128]{1,0:T(8,128)(2,1)S(1)}, u32[]{:S(2)}, u32[]{:S(2)}) collective-permute-start(bf16[384,128]{1,0:T(8,128)(2,1)S(1)} %get-tuple-element.16.refs_0_), channel_id=1, source_target_pairs={{0,8},{4,12},{8,16},{12,20},{16,24},{20,28},{24,0},{28,4},{1,9},{5... | collective-permute-start | bytes 294920 | tf_op jit(solution)/shard_map/ppermute | solution.py:606
  74.9 26.6 %collective-permute-start.20 = (bf16[384,512]{1,0:T(8,128)(2,1)S(1)}, bf16[384,512]{1,0:T(8,128)(2,1)S(1)}, u32[]{:S(2)}, u32[]{:S(2)}) collective-permute-start(bf16[384,512]{1,0:T(8,128)(2,1)S(1)} %shard_map.191), channel_id=1, source_target_pairs={{0,2},{1,3},{2,0},{3,1},{4,6},{5,7},{6,4},{7,5},{8,10},{9,11},{10,... | collective-permute-start | bytes 1179656 | tf_op jit(solution)/shard_map/ppermute | solution.py:587
  75.6 33.9 %collective-permute-start.16 = (bf16[384,512]{1,0:T(8,128)(2,1)S(1)}, bf16[384,512]{1,0:T(8,128)(2,1)S(1)}, u32[]{:S(2)}, u32[]{:S(2)}) collective-permute-start(bf16[384,512]{1,0:T(8,128)(2,1)S(1)} %shard_map.189), channel_id=1, source_target_pairs={{0,2},{1,3},{2,0},{3,1},{4,6},{5,7},{6,4},{7,5},{8,10},{9,11},{10,... | collective-permute-start | bytes 1179656 | tf_op jit(solution)/shard_map/ppermute | solution.py:587
  77.2 7.6 %collective-permute-start.1 = (bf16[384,128]{1,0:T(8,128)(2,1)S(1)}, bf16[384,128]{1,0:T(8,128)(2,1)S(1)}, u32[]{:S(2)}, u32[]{:S(2)}) collective-permute-start(bf16[384,128]{1,0:T(8,128)(2,1)S(1)} %get-tuple-element.16.refs_0_), channel_id=1, source_target_pairs={{0,16},{4,20},{8,24},{12,28},{16,0},{20,4},{24,8},{28,12},{1,17},{... | collective-permute-start | bytes 294920 | tf_op jit(solution)/shard_map/ppermute | solution.py:606
  80.8 5.2 %collective-permute-start.2 = (bf16[384,128]{1,0:T(8,128)(2,1)S(1)}, bf16[384,128]{1,0:T(8,128)(2,1)S(1)}, u32[]{:S(2)}, u32[]{:S(2)}) collective-permute-start(bf16[384,128]{1,0:T(8,128)(2,1)S(1)} %get-tuple-element.16.refs_0_), channel_id=1, source_target_pairs={{0,24},{4,28},{8,0},{12,4},{16,8},{20,12},{24,16},{28,20},{1,25},{... | collective-permute-start | bytes 294920 | tf_op jit(solution)/shard_map/ppermute | solution.py:606
  86.7 32.2 %collective-permute-start.3 = (bf16[4,384,128]{2,1,0:T(8,128)(2,1)}, bf16[4,384,128]{2,1,0:T(8,128)(2,1)}, u32[]{:S(2)}, u32[]{:S(2)}) collective-permute-start(bf16[4,384,128]{2,1,0:T(8,128)(2,1)} %shard_map.185.rest_0_), channel_id=1, source_target_pairs={{0,4},{4,0},{8,12},{12,8},{16,20},{20,16},{24,28},{28,24},{1,5},{5... | collective-permute-start | bytes 1179656 | tf_op jit(solution)/shard_map/ppermute | solution.py:611
  88.2 52.6 %collective-permute-start.9 = (bf16[256,2048]{1,0:T(8,128)(2,1)S(1)}, bf16[256,2048]{1,0:T(8,128)(2,1)}, u32[]{:S(2)}, u32[]{:S(2)}) collective-permute-start(bf16[256,2048]{1,0:T(8,128)(2,1)S(1)} %copy-done), channel_id=1, source_target_pairs={{0,1},{1,0},{2,3},{3,2},{4,5},{5,4},{6,7},{7,6},{8,9},{9,8},{10,11... | collective-permute-start | bytes 3145736 | tf_op jit(solution)/shard_map/ppermute | solution.py:582
  110.6 37.1 %all-to-all-start.1 = ((bf16[8,96,512]{2,1,0:T(8,128)(2,1)}), bf16[8,96,512]{2,1,0:T(8,128)(2,1)S(1)}, u32[]{:S(2)}, u32[]{:S(2)}) async-start(bf16[8,96,512]{2,1,0:T(8,128)(2,1)} %shard_map.192), calls=%async_computation.1 | async-start | bytes 1572864 | tf_op jit(solution)/shard_map/all_to_all | solution.py:616
  118.4 19.6 %collective-permute-start.21 = (bf16[2,256,512]{2,1,0:T(8,128)(2,1)S(1)}, bf16[2,256,512]{2,1,0:T(8,128)(2,1)S(1)}, u32[]{:S(2)}, u32[]{:S(2)}) collective-permute-start(bf16[2,256,512]{2,1,0:T(8,128)(2,1)S(1)} %get-tuple-element.27), channel_id=1, source_target_pairs={{0,1},{1,0},{2,3},{3,2},{4,5},{5,4},{6,7},{7,6},{8,9},{9,8},{10,11... | collective-permute-start | bytes 1572872 | tf_op jit(solution)/shard_map/ppermute | solution.py:582
  118.4 22.4 %collective-permute-start.10 = (bf16[224,2048]{1,0:T(8,128)(2,1)}, bf16[224,2048]{1,0:T(8,128)(2,1)S(1)}, u32[]{:S(2)}, u32[]{:S(2)}) collective-permute-start(bf16[224,2048]{1,0:T(8,128)(2,1)} %collective-permute-done.7.refs_5_), channel_id=1, source_target_pairs={{0,1},{1,0},{2,3},{3,2},{4,5},{5,4},{6,7},{7,6},{8,9},{9,8},{10,11... | collective-permute-start | bytes 2752520 | tf_op jit(solution)/shard_map/ppermute | solution.py:582
  128.2 10.3 %collective-permute-start.4 = (bf16[384,256]{1,0:T(8,128)(2,1)S(1)}, bf16[384,256]{1,0:T(8,128)(2,1)S(1)}, u32[]{:S(2)}, u32[]{:S(2)}) collective-permute-start(bf16[384,256]{1,0:T(8,128)(2,1)S(1)} %attention.1.refs_0_), channel_id=1, source_target_pairs={{0,2},{1,3},{2,0},{3,1},{4,6},{5,7},{6,4},{7,5},{8,10},{9,11},{10,... | collective-permute-start | bytes 589832 | tf_op jit(solution)/shard_map/ppermute | solution.py:587
  129.8 8.2 %collective-permute-start.8 = (bf16[32,2048]{1,0:T(8,128)(2,1)S(1)}, bf16[32,2048]{1,0:T(8,128)(2,1)S(1)}, u32[]{:S(2)}, u32[]{:S(2)}) collective-permute-start(bf16[32,2048]{1,0:T(8,128)(2,1)S(1)} %slice.7), channel_id=1, source_target_pairs={{0,2},{1,3},{2,0},{3,1},{4,6},{5,7},{6,4},{7,5},{8,10},{9,11},{10,... | collective-permute-start | bytes 393224 | tf_op jit(solution)/shard_map/ppermute | solution.py:587
  138.0 1.3 collective-permute-start.11
  138.0 2.8 %collective-permute-start.5 = (bf16[384,256]{1,0:T(8,128)(2,1)S(1)}, bf16[384,256]{1,0:T(8,128)(2,1)S(1)}, u32[]{:S(2)}, u32[]{:S(2)}) collective-permute-start(bf16[384,256]{1,0:T(8,128)(2,1)S(1)} %attention.1.refs_0_), channel_id=1, source_target_pairs={{0,1},{1,0},{2,3},{3,2},{4,5},{5,4},{6,7},{7,6},{8,9},{9,8},{10,11... | collective-permute-start | bytes 589832 | tf_op jit(solution)/shard_map/ppermute | solution.py:582
  138.5 2.3 %collective-permute-start.6 = (bf16[384,256]{1,0:T(8,128)(2,1)S(1)}, bf16[384,256]{1,0:T(8,128)(2,1)S(1)}, u32[]{:S(2)}, u32[]{:S(2)}) collective-permute-start(bf16[384,256]{1,0:T(8,128)(2,1)S(1)} %collective-permute-done.4.refs_1_), channel_id=1, source_target_pairs={{0,1},{1,0},{2,3},{3,2},{4,5},{5,4},{6,7},{7,6},{8,9},{9,8},{10,11... | collective-permute-start | bytes 589832 | tf_op jit(solution)/shard_map/ppermute | solution.py:582
  139.3 8.4 %collective-permute-start.22 = (bf16[256,512]{1,0:T(8,128)(2,1)S(1)}, bf16[256,512]{1,0:T(8,128)(2,1)S(1)}, u32[]{:S(2)}, u32[]{:S(2)}) collective-permute-start(bf16[256,512]{1,0:T(8,128)(2,1)S(1)} %shard_map.194), channel_id=1, source_target_pairs={{0,2},{1,3},{2,0},{3,1},{4,6},{5,7},{6,4},{7,5},{8,10},{9,11},{10,... | collective-permute-start | bytes 786440 | tf_op jit(solution)/shard_map/ppermute | solution.py:587
  (3 other events, 29.0 us)

commit v3 on v2

--- a/solution.py
+++ b/solution.py
@@ -283,9 +283,10 @@
 
 
 def route_kernel(
-    experts, cap, ids_hbm, score_hbm, x_hbm, gain_hbm, normed_ref, plan_hbm, out_hbm, plan_ref,
-    out_ref, idst_ref, score_ref, x_ref, gain_ref, sems, out_sems,
+    experts, cap, ids_hbm, score_hbm, x_hbm, gain_hbm, normed_ref, plan_hbm, *refs
 ):
+    out_refs = refs[:experts]
+    plan_ref, place_ref, idst_ref, score_ref, x_ref, gain_ref, sems, out_sem = refs[experts:]
     copies = fetch(
         [ids_hbm, score_hbm, gain_hbm, x_hbm], [idst_ref, score_ref, gain_ref, x_ref], sems
     )
@@ -307,41 +308,36 @@
     lines += [s / score_sum * ROUTED_SCALE for s in scores]
     lines += [jnp.zeros((8 - 2 * top, rows), F32)]
     plan_ref[...] = jnp.concatenate(lines, axis=0).T
-    sent = [pltpu.make_async_copy(plan_ref, plan_hbm, out_sems.at[0])]
-    sent[0].start()
+    sent = pltpu.make_async_copy(plan_ref, plan_hbm, out_sem)
+    sent.start()
+    place_ref[...] = jnp.where(named, count.astype(jnp.int32), -1)
     wait(copies[2:])
     x = x_ref[...].astype(F32)
     mean = jnp.mean(x * x, axis=1, keepdims=True)
     normed_ref[...] = (x * lax.rsqrt(mean + EPSILON) * gain_ref[...]).astype(BF)
-    place = jnp.where(named, count.astype(jnp.int32), -1)
-    width = out_ref.shape[2]
-    lane = lax.axis_index("tp")
-    own = normed_ref[:, pl.ds(pl.multiple_of(lane * width, 128), width)]
+    width = out_refs[0].shape[1]
+    own = normed_ref[:, pl.ds(pl.multiple_of(lax.axis_index("tp") * width, 128), width)]
     slots = lax.broadcasted_iota(jnp.int32, (cap, rows), 0)
-    for e in range(experts):
-        pick = jnp.where(place[e : e + 1, :] == slots, 1.0, 0.0).astype(BF)
-        out_ref[e] = dot(pick, own).astype(BF)
-        sent.append(pltpu.make_async_copy(out_ref.at[e], out_hbm.at[e], out_sems.at[1 + e]))
-        sent[-1].start()
-    wait(sent)
+    me = lax.axis_index("ep")
+    for step, ref in enumerate(out_refs):
+        place = place_ref[pl.ds(me ^ step, 1), :]
+        ref[...] = dot(jnp.where(place == slots, 1.0, 0.0).astype(BF), own).astype(BF)
+    sent.wait()
 
 
 def route(expert_ids, gate_score, expert_input, gain, experts, cap, width):
     rows = expert_ids.shape[0]
     args = (expert_ids.T, gate_score.T, expert_input, gain[None, :])
-    outs = [
-        jax.ShapeDtypeStruct(expert_input.shape, BF),
-        jax.ShapeDtypeStruct((rows, 8), F32),
-        jax.ShapeDtypeStruct((experts, cap, width), BF),
-    ]
+    normed = jax.ShapeDtypeStruct(expert_input.shape, BF)
+    block = jax.ShapeDtypeStruct((cap, width), BF)
     return pl.pallas_call(
         functools.partial(route_kernel, experts, cap),
         in_specs=[HBM] * 4,
-        out_specs=[VMEM, HBM, HBM],
-        out_shape=outs[:1] + [pltpu.HBM(a.shape, a.dtype) for a in outs[1:]],
-        scratch_shapes=room(outs[1:])[:2]
+        out_specs=[VMEM, HBM] + [VMEM] * experts,
+        out_shape=[normed, pltpu.HBM((rows, 8), F32)] + [block] * experts,
+        scratch_shapes=[pltpu.VMEM((rows, 8), F32), pltpu.VMEM((experts, rows), jnp.int32)]
         + room(args)
-        + [pltpu.SemaphoreType.DMA((experts + 1,))],
+        + [pltpu.SemaphoreType.DMA],
         compiler_params=params(16),
         cost_estimate=cost(1e9, 4e6),
         name="route",
@@ -411,7 +407,7 @@
     if loads > 1:
         start(1)
 
-    def product(w_ref, cols):
+    def product(w_ref, cols, x_refs):
         total = None
         for ref, (unused, here) in zip(x_refs, rows):
             term = dot(ref[...], w_ref[here, cols])
@@ -423,16 +419,18 @@
         if at % load == 0:
             wait(groups[at // load])
             start(at // load + min(2, loads))
-        gate = product(gate_ref, cols)
-        up = product(up_ref, cols)
-        if late:
-            taken = slice(chunk * gate.shape[0], (chunk + 1) * gate.shape[0])
-            gate = gate + partial_ref[0, taken, cols]
-            up = up + partial_ref[1, taken, cols]
-        if early:
-            out_ref[0, :, cols] = gate
-            out_ref[1, :, cols] = up
-        else:
+        for h in range(0, n_x, len(offsets)):
+            gate = product(gate_ref, cols, x_refs[h : h + len(offsets)])
+            up = product(up_ref, cols, x_refs[h : h + len(offsets)])
+            if early:
+                taken = slice(h // len(offsets) * gate.shape[0], (h // len(offsets) + 1) * gate.shape[0])
+                out_ref[0, taken, cols] = gate
+                out_ref[1, taken, cols] = up
+                continue
+            if late:
+                taken = slice(chunk * gate.shape[0], (chunk + 1) * gate.shape[0])
+                gate = gate + partial_ref[0, taken, cols]
+                up = up + partial_ref[1, taken, cols]
             h_ref[:, cols] = (gate / (1.0 + jnp.exp(-gate)) * up).astype(BF)
     if early:
         return
@@ -448,11 +446,11 @@
     rows = x_list[0].shape[0]
     model, hidden = weights[0].shape[1:]
     width = model // (2 * halves)
-    depth = sum(x.shape[1] for x in x_list)
-    n_copies = 2 * len(x_list) * loads_of(hidden)
+    depth = sum(x.shape[1] for x in x_list[: len(offsets)])
+    n_copies = 2 * len(offsets) * loads_of(hidden)
     if early:
         weights = weights[:2]
-        outs = [jax.ShapeDtypeStruct((2, rows, hidden), F32)]
+        outs = [jax.ShapeDtypeStruct((2, len(x_list) // len(offsets) * rows, hidden), F32)]
     else:
         n_copies += 2 * halves
         outs = [jax.ShapeDtypeStruct((halves, rows, width), BF)] * 2
@@ -484,16 +482,6 @@
     )(*args)
 
 
-def split_kernel(in_ref, *outs):
-    for i, out in enumerate(outs):
-        out[...] = in_ref[i]
-
-
-def split(x):
-    shape = jax.ShapeDtypeStruct(x.shape[1:], x.dtype)
-    return small_call(split_kernel, [x], [shape] * x.shape[0])
-
-
 def stack_kernel(*refs):
     for i, ref in enumerate(refs[:-1]):
         refs[-1][i] = ref[...]
@@ -516,8 +504,9 @@
 
 def finish_kernel(counts, *refs):
     refs, out_hbm, out_ref, sems = refs[:-3], refs[-3], refs[-2], refs[-1]
-    width = out_ref.shape[2]
-    blocks = out_ref.shape[0] // len(counts)
+    ep, cap, width = out_ref.shape
+    blocks = ep // len(counts)
+    me = lax.axis_index("ep")
     copies = []
     for h, count in enumerate(counts):
         keep, received, others = refs[0], refs[1], refs[2:count]
@@ -525,14 +514,12 @@
         total = keep[0].astype(F32) + received[0].astype(F32)
         for other in others:
             total = total + other[...].astype(F32)
-        at = h * blocks
-        out_ref[at : at + blocks] = total.astype(BF).reshape(blocks, out_ref.shape[1], width)
-        copies.append(
-            pltpu.make_async_copy(
-                out_ref.at[at : at + blocks], out_hbm.at[at : at + blocks], sems.at[h]
+        out_ref[h * blocks : (h + 1) * blocks] = total.astype(BF).reshape(blocks, cap, width)
+        for step in range(h * blocks, (h + 1) * blocks):
+            copies.append(
+                pltpu.make_async_copy(out_ref.at[step], out_hbm.at[me ^ step], sems.at[step])
             )
-        )
-        copies[-1].start()
+            copies[-1].start()
     wait(copies)
 
 
@@ -545,15 +532,25 @@
     )[0]
 
 
-def combine_kernel(top, plan_hbm, slots_ref, keep_ref, received_ref, *refs):
-    others, (out_ref, plan_ref, sems) = refs[:-3], refs[-3:]
+def total_kernel(keep_ref, received_ref, *refs):
+    others, out_ref = refs[:-1], refs[-1]
+    total = keep_ref[0].astype(F32) + received_ref[0].astype(F32)
+    for other in others:
+        total = total + other[...].astype(F32)
+    out_ref[...] = total
+
+
+def add_all(keep, received, others):
+    shape = jax.ShapeDtypeStruct(keep.shape[1:], F32)
+    return small_call(total_kernel, [keep, received, *others], [shape])[0]
+
+
+def combine_kernel(top, plan_hbm, slots_ref, shared_ref, out_ref, plan_ref, sems):
     copies = fetch([plan_hbm], [plan_ref], sems)
     rows = plan_ref.shape[0]
     experts, cap, width = slots_ref.shape
     n = lax.broadcasted_iota(jnp.int32, (rows, experts * cap), 1)
-    total = keep_ref[0].astype(F32) + received_ref[0].astype(F32)
-    for other in others:
-        total = total + other[...].astype(F32)
+    total = shared_ref[...]
     wait(copies)
     for k in range(top):
         pick = jnp.where(n == plan_ref[:, k : k + 1].astype(jnp.int32), 1.0, 0.0).astype(BF)
@@ -562,9 +559,9 @@
     out_ref[...] = total.astype(BF)
 
 
-def combine(plan, top, slots, keep, received, others):
+def combine(plan, top, slots, shared):
     rows = plan.shape[0]
-    args = (slots, keep, received, *others)
+    args = (slots, shared)
     return pl.pallas_call(
         functools.partial(combine_kernel, top),
         in_specs=[HBM] + [VMEM] * len(args),
@@ -688,17 +685,22 @@
     chunks = 2
     size = ep * cap // chunks
 
-    part = out_weight.shape[0] // 8 * 7
-    parts = [out_weight[:part], out_weight[part:]]
+    eighth = out_weight.shape[0] // 8
+    ends = (0, 4 * eighth, 8 * eighth)
+    parts = [out_weight[i:j] for i, j in zip(ends, ends[1:])]
     w_list = [[out_weight]]
     for step in range(1, halves):
         w_list.append([chip_shift(w, step) for w in parts])
     w_list += [[core_swap(w) for w in parts] for parts in w_list]
 
-    normed, plan, outgoing = route(
+    normed, plan, *outgoing = route(
         expert_ids, gate_score, expert_input, expert_gain, ep, cap, width
     )
-    arrived = exchange(outgoing).reshape(chunks * size, width)
+    blocks = [outgoing[0]]
+    for step in range(1, ep):
+        blocks.append(lax.ppermute(outgoing[step], "ep", [(i, i ^ step) for i in range(ep)]))
+    part = ep // chunks
+    arrived = [stack(blocks[h * part : (h + 1) * part]).reshape(size, width) for h in range(chunks)]
 
     shared = (shared_gate[None], shared_up[None], shared_down[None])
     sh_send, sh_keep = mlp([normed], [None], shared, halves)
@@ -706,10 +708,10 @@
     sh_others = scatter_chips(sh_keep, sh_received)
 
     weights = [gate_weight, up_weight, down_weight]
-    own_chip = [arrived, core_swap(arrived)]
+    own_chip = [p for x in arrived for p in (x, core_swap(x))]
     (partial,) = mlp(own_chip, [(0, 0), (0, 1)], weights, halves, True)
     results = []
-    for h, x in enumerate(split(arrived.reshape(chunks, size, width))):
+    for h, x in enumerate(arrived):
         mine = [chip_shift(x, s) for s in range(1, halves)]
         other = [core_swap(m) for m in mine]
         offsets = [(s, c) for c in range(2) for s in range(1, halves)]
@@ -717,7 +719,8 @@
         received = core_swap(send)
         results.append((keep, received, *scatter_chips(keep, received)))
     returned = exchange(finish(results, (ep, cap, width)))
-    expert_out = combine(plan, top, returned, sh_keep, sh_received, sh_others)
+    shared_sum = add_all(sh_keep, sh_received, sh_others)
+    expert_out = combine(plan, top, returned, shared_sum)
 
     kv, table = prepare_keys(key_rows, value_rows, key_gain, heads)
     kv_list = ep_gather(kv, ep // x_size, x_size)

time: 151 us -> 151 us (level)
  blocking collectives: 27.4 us -> 0 us
  starting transfers between devices: 18.2 us -> 36 us
  waiting for transfers between devices: 56.9 us -> 68.2 us
    all_to_all x1 -> x0, blocking collectives: 27.4 us -> none  [exchange(): return lax.all_to_all(x, 'ep', 0, 0, tiled=True)]
    ppermute x0 -> x7, waiting for transfers between devices: none -> 15.2 us  [whole_step(): lax.ppermute(outgoing[step], 'ep', [(i, i ^ step) for i in range(ep)])]
    ppermute x0 -> x7, starting transfers between devices: none -> 14.2 us  [whole_step(): lax.ppermute(outgoing[step], 'ep', [(i, i ^ step) for i in range(ep)])]
    ppermute x3, waiting for transfers between devices: 8.16 us -> 0.01 us  [ep_gather(): lax.ppermute(x, 'ep', [(i, (i + step * axis_x) % n) for i in range(n)])]
    ppermute x3, starting transfers between devices: 1.7 us -> 6.86 us  [ep_gather(): lax.ppermute(x, 'ep', [(i, (i + step * axis_x) % n) for i in range(n)])]
    ppermute x8, waiting for transfers between devices: 48 us -> 51.9 us  [chip_shift(): return lax.ppermute(x, 'tp', [(i, (i + 2 * step) % n) for i in range(n)])]
  transfers between devices with their start and end apart: 24 -> 32, of which waited for: 10 -> 10; matrix products, arithmetic and copies ran while one was open for 1% -> 1% of each run, Pallas kernels for 27% -> 26%
where the time goes in v3:
time: 151 us; the launch traced here: 150 us
  waiting for transfers between devices  68.2 us (45%)
  Pallas kernels  43.9 us (29%)
  starting transfers between devices  36 us (24%)
    ppermute x8, waiting for transfers between devices, chip_shift(): return lax.ppermute(x, 'tp', [(i, (i + 2 * step) % n) for i in range(n)])  51.9 us
    pallas_call x4, Pallas kernels, mlp(): pl.pallas_call(functools.partial(mlp_kernel, len(x_list), halves, offsets...  21.5 us
    ppermute x7, waiting for transfers between devices, whole_step(): lax.ppermute(outgoing[step], 'ep', [(i, i ^ step) for i in range(ep)])  15.2 us
    ppermute x7, starting transfers between devices, whole_step(): lax.ppermute(outgoing[step], 'ep', [(i, i ^ step) for i in range(ep)])  14.2 us
    pallas_call x1, Pallas kernels, attention(): pl.pallas_call(functools.partial(attention_kernel, heads, tile, chunk, le...  9.12 us
    ppermute x8, starting transfers between devices, chip_shift(): return lax.ppermute(x, 'tp', [(i, (i + 2 * step) % n) for i in range(n)])  8.5 us
    ppermute x3, starting transfers between devices, ep_gather(): lax.ppermute(x, 'ep', [(i, (i + step * axis_x) % n) for i in range(n)])  6.86 us
    pallas_call x1, Pallas kernels, project(): pl.pallas_call(functools.partial(project_kernel, [len(w) for w in w_list]...  5.38 us
  transfers between devices with their start and end apart: 32, of which 10 were waited for; matrix products, arithmetic and copies ran while one was open for 1% of the time, Pallas kernels for 26%

profile of v3, /device:TPU:0, one launch (start us, length us, event | category | flops | bytes accessed | tf_op | source)
XLA Modules:
  0.0 150.1 jit_solution(15336244539397418435)
XLA Ops:
  0.6 2.2 %route.1 = (bf16[256,2048]{1,0:T(8,128)(2,1)S(1)}, f32[256,8]{1,0:T(8,128)}, bf16[96,512]{1,0:T(8,128)(2,1)S(1)}, bf16[96,512]{1,0:T(8,128)(2,1)S(1)}, bf16[96,5...) custom-call(s32[2,256]{1,0:T(2,128)} %bitcast.22, ...), custom_call_target="tpu_custom_call" | custom-call | flops 1000000000 | bytes 4000000 | tf_op jit(solution)/shard_map/route/pallas_call | solution.py:333
  2.9 4.1 %collective-permute-start.18 = (bf16[96,512]{1,0:T(8,128)(2,1)S(1)}, bf16[96,512]{1,0:T(8,128)(2,1)S(1)}, u32[]{:S(2)}, u32[]{:S(2)}) collective-permute-start(bf16[96,512]{1,0:T(8,128)(2,1)S(1)} %get-tuple-element.27), channel_id=1, source_target_pairs={{0,16},{4,20},{8,24},{12,28},{16,0},{20,4},{24,8},{28,12},{1,17},{... | collective-permute-start | bytes 294920 | tf_op jit(solution)/shard_map/ppermute | solution.py:701
  8.3 3.6 %collective-permute-start.20 = (bf16[96,512]{1,0:T(8,128)(2,1)S(1)}, bf16[96,512]{1,0:T(8,128)(2,1)S(1)}, u32[]{:S(2)}, u32[]{:S(2)}) collective-permute-start(bf16[96,512]{1,0:T(8,128)(2,1)S(1)} %get-tuple-element.29), channel_id=1, source_target_pairs={{0,24},{4,28},{8,16},{12,20},{16,8},{20,12},{24,0},{28,4},{1,25},{... | collective-permute-start | bytes 294920 | tf_op jit(solution)/shard_map/ppermute | solution.py:701
  11.9 7.2 %collective-permute-done.18.refs_0_ = bf16[96,512]{1,0:T(8,128)(2,1)S(1)} collective-permute-done((bf16[96,512]{1,0:T(8,128)(2,1)S(1)}, bf16[96,512]{1,0:T(8,128)(2,1)S(1)}, u32[]{:S(2)}, u32[]{:S(2)}) %collective-permute-start.18) | collective-permute-done | bytes 98336 | tf_op jit(solution)/shard_map/ppermute | solution.py:701
  19.1 3.2 %collective-permute-done.19.refs_1_ = bf16[96,512]{1,0:T(8,128)(2,1)S(1)} collective-permute-done((bf16[96,512]{1,0:T(8,128)(2,1)S(1)}, bf16[96,512]{1,0:T(8,128)(2,1)S(1)}, u32[]{:S(2)}, u32[]{:S(2)}) %collective-permute-start.19) | collective-permute-done | bytes 98336 | tf_op jit(solution)/shard_map/ppermute | solution.py:701
  22.3 1.6 %collective-permute-start.25 = (bf16[384,512]{1,0:T(8,128)(2,1)S(1)}, bf16[384,512]{1,0:T(8,128)(2,1)S(1)}, u32[]{:S(2)}, u32[]{:S(2)}) collective-permute-start(bf16[384,512]{1,0:T(8,128)(2,1)S(1)} %bitcast.11), channel_id=1, source_target_pairs={{0,2},{1,3},{2,0},{3,1},{4,6},{5,7},{6,4},{7,5},{8,10},{9,11},{10,... | collective-permute-start | bytes 1179656 | tf_op jit(solution)/shard_map/ppermute | solution.py:584
  24.5 3.9 %collective-permute-start.13 = (bf16[96,512]{1,0:T(8,128)(2,1)S(1)}, bf16[96,512]{1,0:T(8,128)(2,1)S(1)}, u32[]{:S(2)}, u32[]{:S(2)}) collective-permute-start(bf16[96,512]{1,0:T(8,128)(2,1)S(1)} %get-tuple-element.25), channel_id=1, source_target_pairs={{0,8},{4,12},{8,0},{12,4},{16,24},{20,28},{24,16},{28,20},{1,9},{5... | collective-permute-start | bytes 294920 | tf_op jit(solution)/shard_map/ppermute | solution.py:701
  29.2 2.6 %collective-permute-done.13.refs_2_ = bf16[96,512]{1,0:T(8,128)(2,1)S(1)} collective-permute-done((bf16[96,512]{1,0:T(8,128)(2,1)S(1)}, bf16[96,512]{1,0:T(8,128)(2,1)S(1)}, u32[]{:S(2)}, u32[]{:S(2)}) %collective-permute-start.13) | collective-permute-done | bytes 98336 | tf_op jit(solution)/shard_map/ppermute | solution.py:701
  31.8 2.1 %collective-permute-done.14.refs_3_ = bf16[96,512]{1,0:T(8,128)(2,1)S(1)} collective-permute-done((bf16[96,512]{1,0:T(8,128)(2,1)S(1)}, bf16[96,512]{1,0:T(8,128)(2,1)S(1)}, u32[]{:S(2)}, u32[]{:S(2)}) %collective-permute-start.14) | collective-permute-done | bytes 98336 | tf_op jit(solution)/shard_map/ppermute | solution.py:701
  35.0 8.8 %collective-permute-done.15.refs_0_ = bf16[384,512]{1,0:T(8,128)(2,1)S(1)} collective-permute-done((bf16[384,512]{1,0:T(8,128)(2,1)S(1)}, bf16[384,512]{1,0:T(8,128)(2,1)S(1)}, u32[]{:S(2)}, u32[]{:S(2)}) %collective-permute-start.15) | collective-permute-done | bytes 393248 | tf_op jit(solution)/shard_map/ppermute | solution.py:584
  43.8 5.2 %shard_map.188.refs_2_ = f32[2,768,1024]{2,1,0:T(8,128)S(1)} custom-call(bf16[384,512]{1,0:T(8,128)(2,1)S(1)} %bitcast.16, bf16[384,512]{1,0:T(8,128)(2,1)S(1)} %collective-permute-done.17.refs_1_, bf16[384,512]{1,0:T(8,128)(2,1)S(1)} %bitcast.13, bf16[384,512]{1,0:T(8,128)(2,1)S(1)} %collective-permute-done.22.refs_3_, bf16[1,2048,1024]{2,1,0:T(8,128)(2,1)} %refs_3_.3, ...), custom_call_target="tpu_custom_call" | custom-call | flops 1610612736 | bytes 12582912 | tf_op jit(solution)/shard_map/pallas_call | solution.py:462
  49.0 5.9 %shard_map.191 = (bf16[2,384,512]{2,1,0:T(8,128)(2,1)S(1)}, bf16[2,384,512]{2,1,0:T(8,128)(2,1)S(1)}) custom-call(bf16[384,512]{1,0:T(8,128)(2,1)S(1)} %collective-permute-done.25.refs_0_, bf16[384,512]{1,0:T(8,128)(2,1)S(1)} %collective-permute-done.26.refs_1_, f32[2,768,1024]{2,1,0:T(8,128)S(1)} %shard_map.188.refs_2_, bf16[1,2048,1024]{2,1,0:T(8,128)(2,1)} %refs_3_.3, ...), custom_call_target="tpu_custom_call" | custom-call | flops 3221225472 | bytes 12582912 | tf_op jit(solution)/shard_map/pallas_call | solution.py:462
  55.4 5.8 %shard_map.189 = (bf16[2,384,512]{2,1,0:T(8,128)(2,1)S(1)}, bf16[2,384,512]{2,1,0:T(8,128)(2,1)S(1)}) custom-call(bf16[384,512]{1,0:T(8,128)(2,1)S(1)} %collective-permute-done.15.refs_0_, bf16[384,512]{1,0:T(8,128)(2,1)S(1)} %collective-permute-done.16.refs_1_, f32[2,768,1024]{2,1,0:T(8,128)S(1)} %shard_map.188.refs_2_, bf16[1,2048,1024]{2,1,0:T(8,128)(2,1)} %refs_3_.3, ...), custom_call_target="tpu_custom_call" | custom-call | flops 3221225472 | bytes 12582912 | tf_op jit(solution)/shard_map/pallas_call | solution.py:462
  61.4 1.9 %keys.1 = (bf16[384,128]{1,0:T(8,128)(2,1)S(1)}, f32[140,128]{1,0:T(8,128)S(1)}) custom-call(bf16[384,256]{1,0:T(8,128)(2,1)} %key_hbm.1, bf16[384,256]{1,0:T(8,128)(2,1)} %value_hbm.1, f32[1,64]{1,0:T(1,128)} %bitcast.24, f32[1,128]{1,0:T(1,128)} %constant.2.clone.inverse_hbm), custom_call_target="tpu_custom_call" | custom-call | flops 1000000000 | bytes 300000 | tf_op jit(solution)/shard_map/keys/pallas_call | solution.py:129
  64.4 3.4 %collective-permute-start.1 = (bf16[384,128]{1,0:T(8,128)(2,1)S(1)}, bf16[384,128]{1,0:T(8,128)(2,1)S(1)}, u32[]{:S(2)}, u32[]{:S(2)}) collective-permute-start(bf16[384,128]{1,0:T(8,128)(2,1)S(1)} %get-tuple-element.21.refs_0_), channel_id=1, source_target_pairs={{0,16},{4,20},{8,24},{12,28},{16,0},{20,4},{24,8},{28,12},{1,17},{... | collective-permute-start | bytes 294920 | tf_op jit(solution)/shard_map/ppermute | solution.py:603
  67.8 2.4 %collective-permute-start.2 = (bf16[384,128]{1,0:T(8,128)(2,1)S(1)}, bf16[384,128]{1,0:T(8,128)(2,1)S(1)}, u32[]{:S(2)}, u32[]{:S(2)}) collective-permute-start(bf16[384,128]{1,0:T(8,128)(2,1)S(1)} %get-tuple-element.21.refs_0_), channel_id=1, source_target_pairs={{0,24},{4,28},{8,0},{12,4},{16,8},{20,12},{24,16},{28,20},{1,25},{... | collective-permute-start | bytes 294920 | tf_op jit(solution)/shard_map/ppermute | solution.py:603
  70.1 4.6 %shard_map.194 = (bf16[2,256,512]{2,1,0:T(8,128)(2,1)}, bf16[2,256,512]{2,1,0:T(8,128)(2,1)S(1)}) custom-call(bf16[256,2048]{1,0:T(8,128)(2,1)S(1)} %get-tuple-element.35.refs_0_, bf16[1,2048,512]{2,1,0:T(8,128)(2,1)} %bitcast.18, bf16[1,2048,512]{2,1,0:T(8,128)(2,1)} %bitcast.19, bf16[1,512,2048]{2,1,0:T(8,128)(2,1)} %bitcast.20), custom_call_target="tpu_custom_call" | custom-call | flops 1610612736 | bytes 6291456 | tf_op jit(solution)/shard_map/pallas_call | solution.py:462
  80.3 6.7 %collective-permute-done.28.refs_5_ = bf16[384,512]{1,0:T(8,128)(2,1)S(1)} collective-permute-done((bf16[384,512]{1,0:T(8,128)(2,1)S(1)}, bf16[384,512]{1,0:T(8,128)(2,1)S(1)}, u32[]{:S(2)}, u32[]{:S(2)}) %collective-permute-start.28) | collective-permute-done | bytes 393248 | tf_op jit(solution)/shard_map/ppermute | solution.py:584
  87.6 29.9 %collective-permute-done.24.refs_2_ = bf16[384,512]{1,0:T(8,128)(2,1)S(1)} collective-permute-done((bf16[384,512]{1,0:T(8,128)(2,1)S(1)}, bf16[384,512]{1,0:T(8,128)(2,1)S(1)}, u32[]{:S(2)}, u32[]{:S(2)}) %collective-permute-start.24) | collective-permute-done | bytes 393248 | tf_op jit(solution)/shard_map/ppermute | solution.py:584
  118.5 3.6 %all-to-all-start = ((bf16[8,96,512]{2,1,0:T(8,128)(2,1)}), bf16[8,96,512]{2,1,0:T(8,128)(2,1)S(1)}, u32[]{:S(2)}, u32[]{:S(2)}) async-start(bf16[8,96,512]{2,1,0:T(8,128)(2,1)} %shard_map.193), calls=%async_computation | async-start | bytes 1572864 | tf_op jit(solution)/shard_map/all_to_all | solution.py:613
  124.4 9.1 %attention.1.refs_0_ = bf16[384,256]{1,0:T(8,128)(2,1)S(1)} custom-call(bf16[384,256]{1,0:T(8,128)(2,1)} %q_hbm.1, f32[1,64]{1,0:T(1,128)} %bitcast.25, f32[140,128]{1,0:T(8,128)} %copy-done.2, bf16[4,384,128]{2,1,0:T(8,128)(2,1)S(1)} %shard_map.185.rest_0_, bf16[4,384,128]{2,1,0:T(8,128)(2,1)} %collective-permute-done.3.rest_1_), custom_call_target="tpu_custom_call" | custom-call | flops 8000000000 | bytes 2000000 | tf_op jit(solution)/shard_map/attention/pallas_call | solution.py:221
  134.1 6.5 %collective-permute-done.4.refs_1_ = bf16[384,256]{1,0:T(8,128)(2,1)S(1)} collective-permute-done((bf16[384,256]{1,0:T(8,128)(2,1)S(1)}, bf16[384,256]{1,0:T(8,128)(2,1)S(1)}, u32[]{:S(2)}, u32[]{:S(2)}) %collective-permute-start.4) | collective-permute-done | bytes 196640 | tf_op jit(solution)/shard_map/ppermute | solution.py:584
  142.3 5.4 %project.1 = bf16[384,2048]{1,0:T(8,128)(2,1)} custom-call(bf16[384,256]{1,0:T(8,128)(2,1)S(1)} %attention.1.refs_0_, bf16[384,256]{1,0:T(8,128)(2,1)S(1)} %collective-permute-done.4.refs_1_, bf16[384,256]{1,0:T(8,128)(2,1)S(1)} %collective-permute-done.5.refs_2_, bf16[384,256]{1,0:T(8,128)(2,1)S(1)} %collective-permute-done.6.refs_3_, ...), custom_call_target="tpu_custom_call" | custom-call | flops 2000000000 | bytes 6000000 | tf_op jit(solution)/shard_map/project/pallas_call | solution.py:273
  147.7 2.2 %combine.1 = bf16[256,512]{1,0:T(8,128)(2,1)} custom-call(f32[256,8]{1,0:T(8,128)} %get-tuple-element.22.plan_hbm, bf16[8,96,512]{2,1,0:T(8,128)(2,1)S(1)} %all-to-all-done.slots_ref, f32[256,512]{1,0:T(8,128)S(1)} %shard_map.196.shared_ref), custom_call_target="tpu_custom_call" | custom-call | flops 800000000 | bytes 2000000 | tf_op jit(solution)/shard_map/combine/pallas_call | solution.py:565
  (64 shorter events, 17.2 us)
Async XLA Ops:
  2.9 16.2 %collective-permute-start.18 = (bf16[96,512]{1,0:T(8,128)(2,1)S(1)}, bf16[96,512]{1,0:T(8,128)(2,1)S(1)}, u32[]{:S(2)}, u32[]{:S(2)}) collective-permute-start(bf16[96,512]{1,0:T(8,128)(2,1)S(1)} %get-tuple-element.27), channel_id=1, source_target_pairs={{0,16},{4,20},{8,24},{12,28},{16,0},{20,4},{24,8},{28,12},{1,17},{... | collective-permute-start | bytes 294920 | tf_op jit(solution)/shard_map/ppermute | solution.py:701
  7.0 15.3 %collective-permute-start.19 = (bf16[96,512]{1,0:T(8,128)(2,1)S(1)}, bf16[96,512]{1,0:T(8,128)(2,1)S(1)}, u32[]{:S(2)}, u32[]{:S(2)}) collective-permute-start(bf16[96,512]{1,0:T(8,128)(2,1)S(1)} %get-tuple-element.28), channel_id=1, source_target_pairs={{0,20},{4,16},{8,28},{12,24},{16,4},{20,0},{24,12},{28,8},{1,21},{... | collective-permute-start | bytes 294920 | tf_op jit(solution)/shard_map/ppermute | solution.py:701
  8.3 14.0 %collective-permute-start.20 = (bf16[96,512]{1,0:T(8,128)(2,1)S(1)}, bf16[96,512]{1,0:T(8,128)(2,1)S(1)}, u32[]{:S(2)}, u32[]{:S(2)}) collective-permute-start(bf16[96,512]{1,0:T(8,128)(2,1)S(1)} %get-tuple-element.29), channel_id=1, source_target_pairs={{0,24},{4,28},{8,16},{12,20},{16,8},{20,12},{24,0},{28,4},{1,25},{... | collective-permute-start | bytes 294920 | tf_op jit(solution)/shard_map/ppermute | solution.py:701
  11.9 10.4 %collective-permute-start.21 = (bf16[96,512]{1,0:T(8,128)(2,1)S(1)}, bf16[96,512]{1,0:T(8,128)(2,1)S(1)}, u32[]{:S(2)}, u32[]{:S(2)}) collective-permute-start(bf16[96,512]{1,0:T(8,128)(2,1)S(1)} %get-tuple-element.30), channel_id=1, source_target_pairs={{0,28},{4,24},{8,20},{12,16},{16,12},{20,8},{24,4},{28,0},{1,29},{... | collective-permute-start | bytes 294920 | tf_op jit(solution)/shard_map/ppermute | solution.py:701
  22.3 12.7 %collective-permute-start.25 = (bf16[384,512]{1,0:T(8,128)(2,1)S(1)}, bf16[384,512]{1,0:T(8,128)(2,1)S(1)}, u32[]{:S(2)}, u32[]{:S(2)}) collective-permute-start(bf16[384,512]{1,0:T(8,128)(2,1)S(1)} %bitcast.11), channel_id=1, source_target_pairs={{0,2},{1,3},{2,0},{3,1},{4,6},{5,7},{6,4},{7,5},{8,10},{9,11},{10,... | collective-permute-start | bytes 1179656 | tf_op jit(solution)/shard_map/ppermute | solution.py:584
  33.9 9.8 %collective-permute-start.15 = (bf16[384,512]{1,0:T(8,128)(2,1)S(1)}, bf16[384,512]{1,0:T(8,128)(2,1)S(1)}, u32[]{:S(2)}, u32[]{:S(2)}) collective-permute-start(bf16[384,512]{1,0:T(8,128)(2,1)S(1)} %bitcast.14), channel_id=1, source_target_pairs={{0,2},{1,3},{2,0},{3,1},{4,6},{5,7},{6,4},{7,5},{8,10},{9,11},{10,... | collective-permute-start | bytes 1179656 | tf_op jit(solution)/shard_map/ppermute | solution.py:584
  35.0 14.0 %collective-permute-start.26 = (bf16[384,512]{1,0:T(8,128)(2,1)S(1)}, bf16[384,512]{1,0:T(8,128)(2,1)S(1)}, u32[]{:S(2)}, u32[]{:S(2)}) collective-permute-start(bf16[384,512]{1,0:T(8,128)(2,1)S(1)} %collective-permute-done.25.refs_0_), channel_id=1, source_target_pairs={{0,1},{1,0},{2,3},{3,2},{4,5},{5,4},{6,7},{7,6},{8,9},{9,8},{10,11... | collective-permute-start | bytes 1179656 | tf_op jit(solution)/shard_map/ppermute | solution.py:579
  43.8 11.7 %collective-permute-start.16 = (bf16[384,512]{1,0:T(8,128)(2,1)S(1)}, bf16[384,512]{1,0:T(8,128)(2,1)S(1)}, u32[]{:S(2)}, u32[]{:S(2)}) collective-permute-start(bf16[384,512]{1,0:T(8,128)(2,1)S(1)} %collective-permute-done.15.refs_0_), channel_id=1, source_target_pairs={{0,1},{1,0},{2,3},{3,2},{4,5},{5,4},{6,7},{7,6},{8,9},{9,8},{10,11... | collective-permute-start | bytes 1179656 | tf_op jit(solution)/shard_map/ppermute | solution.py:579
  54.9 19.8 %collective-permute-start.27 = (bf16[2,384,512]{2,1,0:T(8,128)(2,1)S(1)}, bf16[2,384,512]{2,1,0:T(8,128)(2,1)S(1)}, u32[]{:S(2)}, u32[]{:S(2)}) collective-permute-start(bf16[2,384,512]{2,1,0:T(8,128)(2,1)S(1)} %get-tuple-element.34), channel_id=1, source_target_pairs={{0,1},{1,0},{2,3},{3,2},{4,5},{5,4},{6,7},{7,6},{8,9},{9,8},{10,11... | collective-permute-start | bytes 2359304 | tf_op jit(solution)/shard_map/ppermute | solution.py:579
  61.3 16.8 %collective-permute-start.23 = (bf16[2,384,512]{2,1,0:T(8,128)(2,1)S(1)}, bf16[2,384,512]{2,1,0:T(8,128)(2,1)S(1)}, u32[]{:S(2)}, u32[]{:S(2)}) collective-permute-start(bf16[2,384,512]{2,1,0:T(8,128)(2,1)S(1)} %get-tuple-element.32), channel_id=1, source_target_pairs={{0,1},{1,0},{2,3},{3,2},{4,5},{5,4},{6,7},{7,6},{8,9},{9,8},{10,11... | collective-permute-start | bytes 2359304 | tf_op jit(solution)/shard_map/ppermute | solution.py:579
  63.3 11.7 %collective-permute-start = (bf16[384,128]{1,0:T(8,128)(2,1)S(1)}, bf16[384,128]{1,0:T(8,128)(2,1)S(1)}, u32[]{:S(2)}, u32[]{:S(2)}) collective-permute-start(bf16[384,128]{1,0:T(8,128)(2,1)S(1)} %get-tuple-element.21.refs_0_), channel_id=1, source_target_pairs={{0,8},{4,12},{8,16},{12,20},{16,24},{20,28},{24,0},{28,4},{1,9},{5... | collective-permute-start | bytes 294920 | tf_op jit(solution)/shard_map/ppermute | solution.py:603
  64.4 13.2 %collective-permute-start.1 = (bf16[384,128]{1,0:T(8,128)(2,1)S(1)}, bf16[384,128]{1,0:T(8,128)(2,1)S(1)}, u32[]{:S(2)}, u32[]{:S(2)}) collective-permute-start(bf16[384,128]{1,0:T(8,128)(2,1)S(1)} %get-tuple-element.21.refs_0_), channel_id=1, source_target_pairs={{0,16},{4,20},{8,24},{12,28},{16,0},{20,4},{24,8},{28,12},{1,17},{... | collective-permute-start | bytes 294920 | tf_op jit(solution)/shard_map/ppermute | solution.py:603
  67.8 12.0 %collective-permute-start.2 = (bf16[384,128]{1,0:T(8,128)(2,1)S(1)}, bf16[384,128]{1,0:T(8,128)(2,1)S(1)}, u32[]{:S(2)}, u32[]{:S(2)}) collective-permute-start(bf16[384,128]{1,0:T(8,128)(2,1)S(1)} %get-tuple-element.21.refs_0_), channel_id=1, source_target_pairs={{0,24},{4,28},{8,0},{12,4},{16,8},{20,12},{24,16},{28,20},{1,25},{... | collective-permute-start | bytes 294920 | tf_op jit(solution)/shard_map/ppermute | solution.py:603
  74.8 47.4 %collective-permute-start.29 = (bf16[2,256,512]{2,1,0:T(8,128)(2,1)}, bf16[2,256,512]{2,1,0:T(8,128)(2,1)S(1)}, u32[]{:S(2)}, u32[]{:S(2)}) collective-permute-start(bf16[2,256,512]{2,1,0:T(8,128)(2,1)} %get-tuple-element.37), channel_id=1, source_target_pairs={{0,1},{1,0},{2,3},{3,2},{4,5},{5,4},{6,7},{7,6},{8,9},{9,8},{10,11... | collective-permute-start | bytes 1572872 | tf_op jit(solution)/shard_map/ppermute | solution.py:579
  75.0 12.1 %collective-permute-start.28 = (bf16[384,512]{1,0:T(8,128)(2,1)S(1)}, bf16[384,512]{1,0:T(8,128)(2,1)S(1)}, u32[]{:S(2)}, u32[]{:S(2)}) collective-permute-start(bf16[384,512]{1,0:T(8,128)(2,1)S(1)} %shard_map.192), channel_id=1, source_target_pairs={{0,2},{1,3},{2,0},{3,1},{4,6},{5,7},{6,4},{7,5},{8,10},{9,11},{10,... | collective-permute-start | bytes 1179656 | tf_op jit(solution)/shard_map/ppermute | solution.py:584
  77.6 46.3 %collective-permute-start.7 = (bf16[128,2048]{1,0:T(8,128)(2,1)}, bf16[128,2048]{1,0:T(8,128)(2,1)}, u32[]{:S(2)}, u32[]{:S(2)}) collective-permute-start(bf16[128,2048]{1,0:T(8,128)(2,1)} %get-tuple-element.39), channel_id=1, source_target_pairs={{0,2},{1,3},{2,0},{3,1},{4,6},{5,7},{6,4},{7,5},{8,10},{9,11},{10,... | collective-permute-start | bytes 1572872 | tf_op jit(solution)/shard_map/ppermute | solution.py:584
  78.1 46.0 %collective-permute-start.8 = (bf16[128,2048]{1,0:T(8,128)(2,1)}, bf16[128,2048]{1,0:T(8,128)(2,1)}, u32[]{:S(2)}, u32[]{:S(2)}) collective-permute-start(bf16[128,2048]{1,0:T(8,128)(2,1)} %get-tuple-element.38), channel_id=1, source_target_pairs={{0,2},{1,3},{2,0},{3,1},{4,6},{5,7},{6,4},{7,5},{8,10},{9,11},{10,... | collective-permute-start | bytes 1572872 | tf_op jit(solution)/shard_map/ppermute | solution.py:584
  79.7 37.7 %collective-permute-start.24 = (bf16[384,512]{1,0:T(8,128)(2,1)S(1)}, bf16[384,512]{1,0:T(8,128)(2,1)S(1)}, u32[]{:S(2)}, u32[]{:S(2)}) collective-permute-start(bf16[384,512]{1,0:T(8,128)(2,1)S(1)} %shard_map.190), channel_id=1, source_target_pairs={{0,2},{1,3},{2,0},{3,1},{4,6},{5,7},{6,4},{7,5},{8,10},{9,11},{10,... | collective-permute-start | bytes 1179656 | tf_op jit(solution)/shard_map/ppermute | solution.py:584
  87.0 37.4 %collective-permute-start.3 = (bf16[4,384,128]{2,1,0:T(8,128)(2,1)S(1)}, bf16[4,384,128]{2,1,0:T(8,128)(2,1)}, u32[]{:S(2)}, u32[]{:S(2)}) collective-permute-start(bf16[4,384,128]{2,1,0:T(8,128)(2,1)S(1)} %shard_map.185.rest_0_), channel_id=1, source_target_pairs={{0,4},{4,0},{8,12},{12,8},{16,20},{20,16},{24,28},{28,24},{1,5},{5... | collective-permute-start | bytes 1179656 | tf_op jit(solution)/shard_map/ppermute | solution.py:608
  118.5 29.2 %all-to-all-start = ((bf16[8,96,512]{2,1,0:T(8,128)(2,1)}), bf16[8,96,512]{2,1,0:T(8,128)(2,1)S(1)}, u32[]{:S(2)}, u32[]{:S(2)}) async-start(bf16[8,96,512]{2,1,0:T(8,128)(2,1)} %shard_map.193), calls=%async_computation | async-start | bytes 1572864 | tf_op jit(solution)/shard_map/all_to_all | solution.py:613
  122.1 20.2 %collective-permute-start.9 = (bf16[256,2048]{1,0:T(8,128)(2,1)S(1)}, bf16[256,2048]{1,0:T(8,128)(2,1)S(1)}, u32[]{:S(2)}, u32[]{:S(2)}) collective-permute-start(bf16[256,2048]{1,0:T(8,128)(2,1)S(1)} %copy-done), channel_id=1, source_target_pairs={{0,1},{1,0},{2,3},{3,2},{4,5},{5,4},{6,7},{7,6},{8,9},{9,8},{10,11... | collective-permute-start | bytes 3145736 | tf_op jit(solution)/shard_map/ppermute | solution.py:579
  122.3 18.3 %collective-permute-start.30 = (bf16[256,512]{1,0:T(8,128)(2,1)S(1)}, bf16[256,512]{1,0:T(8,128)(2,1)S(1)}, u32[]{:S(2)}, u32[]{:S(2)}) collective-permute-start(bf16[256,512]{1,0:T(8,128)(2,1)S(1)} %shard_map.195), channel_id=1, source_target_pairs={{0,2},{1,3},{2,0},{3,1},{4,6},{5,7},{6,4},{7,5},{8,10},{9,11},{10,... | collective-permute-start | bytes 786440 | tf_op jit(solution)/shard_map/ppermute | solution.py:584
  123.9 18.5 %collective-permute-start.10 = (bf16[128,2048]{1,0:T(8,128)(2,1)}, bf16[128,2048]{1,0:T(8,128)(2,1)S(1)}, u32[]{:S(2)}, u32[]{:S(2)}) collective-permute-start(bf16[128,2048]{1,0:T(8,128)(2,1)} %collective-permute-done.7.refs_5_), channel_id=1, source_target_pairs={{0,1},{1,0},{2,3},{3,2},{4,5},{5,4},{6,7},{7,6},{8,9},{9,8},{10,11... | collective-permute-start | bytes 1572872 | tf_op jit(solution)/shard_map/ppermute | solution.py:579
  124.1 18.3 %collective-permute-start.11 = (bf16[128,2048]{1,0:T(8,128)(2,1)}, bf16[128,2048]{1,0:T(8,128)(2,1)S(1)}, u32[]{:S(2)}, u32[]{:S(2)}) collective-permute-start(bf16[128,2048]{1,0:T(8,128)(2,1)} %collective-permute-done.8.refs_6_), channel_id=1, source_target_pairs={{0,1},{1,0},{2,3},{3,2},{4,5},{5,4},{6,7},{7,6},{8,9},{9,8},{10,11... | collective-permute-start | bytes 1572872 | tf_op jit(solution)/shard_map/ppermute | solution.py:579
  (11 other events, 83.0 us)

commit v4 on v3

--- a/solution.py
+++ b/solution.py
@@ -532,26 +532,25 @@
     )[0]
 
 
-def total_kernel(keep_ref, received_ref, *refs):
-    others, out_ref = refs[:-1], refs[-1]
+def total_kernel(plan_ref, keep_ref, received_ref, *refs):
+    others, (out_ref, kept_ref) = refs[:-2], refs[-2:]
+    kept_ref[...] = plan_ref[...]
     total = keep_ref[0].astype(F32) + received_ref[0].astype(F32)
     for other in others:
         total = total + other[...].astype(F32)
     out_ref[...] = total
 
 
-def add_all(keep, received, others):
-    shape = jax.ShapeDtypeStruct(keep.shape[1:], F32)
-    return small_call(total_kernel, [keep, received, *others], [shape])[0]
-
-
-def combine_kernel(top, plan_hbm, slots_ref, shared_ref, out_ref, plan_ref, sems):
-    copies = fetch([plan_hbm], [plan_ref], sems)
+def add_all(plan, keep, received, others):
+    outs = [jax.ShapeDtypeStruct(keep.shape[1:], F32), jax.ShapeDtypeStruct(plan.shape, F32)]
+    return small_call(total_kernel, [plan, keep, received, *others], outs)
+
+
+def combine_kernel(top, plan_ref, slots_ref, shared_ref, out_ref):
     rows = plan_ref.shape[0]
     experts, cap, width = slots_ref.shape
     n = lax.broadcasted_iota(jnp.int32, (rows, experts * cap), 1)
     total = shared_ref[...]
-    wait(copies)
     for k in range(top):
         pick = jnp.where(n == plan_ref[:, k : k + 1].astype(jnp.int32), 1.0, 0.0).astype(BF)
         picked = dot(pick, slots_ref[...].reshape(experts * cap, width))
@@ -561,17 +560,16 @@
 
 def combine(plan, top, slots, shared):
     rows = plan.shape[0]
-    args = (slots, shared)
+    args = (plan, slots, shared)
     return pl.pallas_call(
         functools.partial(combine_kernel, top),
-        in_specs=[HBM] + [VMEM] * len(args),
+        in_specs=[VMEM] * len(args),
         out_specs=VMEM,
         out_shape=jax.ShapeDtypeStruct((rows, slots.shape[2]), BF),
-        scratch_shapes=room([plan]),
         compiler_params=params(16),
         cost_estimate=cost(8e8, 2e6),
         name="combine",
-    )(*in_hbm([plan]), *args)
+    )(*args)
 
 
 def core_swap(x):
@@ -686,7 +684,7 @@
     size = ep * cap // chunks
 
     eighth = out_weight.shape[0] // 8
-    ends = (0, 4 * eighth, 8 * eighth)
+    ends = (0, 5 * eighth, 8 * eighth)
     parts = [out_weight[i:j] for i, j in zip(ends, ends[1:])]
     w_list = [[out_weight]]
     for step in range(1, halves):
@@ -719,7 +717,7 @@
         received = core_swap(send)
         results.append((keep, received, *scatter_chips(keep, received)))
     returned = exchange(finish(results, (ep, cap, width)))
-    shared_sum = add_all(sh_keep, sh_received, sh_others)
+    shared_sum, plan = add_all(plan, sh_keep, sh_received, sh_others)
     expert_out = combine(plan, top, returned, shared_sum)
 
     kv, table = prepare_keys(key_rows, value_rows, key_gain, heads)

time: 151 us -> 137 us (0.907)
  waiting for transfers between devices: 68.2 us -> 55.4 us
    ppermute x8, waiting for transfers between devices: 51.9 us -> 38.7 us  [chip_shift(): return lax.ppermute(x, 'tp', [(i, (i + 2 * step) % n) for i in range(n)])]
  transfers between devices with their start and end apart: 32 -> 32, of which waited for: 10 -> 11; matrix products, arithmetic and copies ran while one was open for 1% -> 1% of each run, Pallas kernels for 26% -> 29%
where the time goes in v4:
time: 137 us
  waiting for transfers between devices  55.4 us (40%)
  Pallas kernels  42.9 us (31%)
  starting transfers between devices  37.1 us (27%)
    ppermute x8, waiting for transfers between devices, chip_shift(): return lax.ppermute(x, 'tp', [(i, (i + 2 * step) % n) for i in range(n)])  38.7 us
    pallas_call x4, Pallas kernels, mlp(): pl.pallas_call(functools.partial(mlp_kernel, len(x_list), halves, offsets...  21.4 us
    ppermute x7, waiting for transfers between devices, whole_step(): lax.ppermute(outgoing[step], 'ep', [(i, i ^ step) for i in range(ep)])  15.2 us
    ppermute x7, starting transfers between devices, whole_step(): lax.ppermute(outgoing[step], 'ep', [(i, i ^ step) for i in range(ep)])  14.2 us
    pallas_call x1, Pallas kernels, attention(): pl.pallas_call(functools.partial(attention_kernel, heads, tile, chunk, le...  9.14 us
    ppermute x8, starting transfers between devices, chip_shift(): return lax.ppermute(x, 'tp', [(i, (i + 2 * step) % n) for i in range(n)])  9.03 us
    ppermute x3, starting transfers between devices, ep_gather(): lax.ppermute(x, 'ep', [(i, (i + step * axis_x) % n) for i in range(n)])  7.58 us
    pallas_call x1, Pallas kernels, project(): pl.pallas_call(functools.partial(project_kernel, [len(w) for w in w_list]...  5.35 us
  transfers between devices with their start and end apart: 32, of which 11 were waited for; matrix products, arithmetic and copies ran while one was open for 1% of the time, Pallas kernels for 29%

profile of v4, /device:TPU:0, one launch (start us, length us, event | category | flops | bytes accessed | tf_op | source)
XLA Modules:
  0.0 137.1 jit_solution(4606440148843024402)
XLA Ops:
  0.6 2.2 %route.1 = (bf16[256,2048]{1,0:T(8,128)(2,1)S(1)}, f32[256,8]{1,0:T(8,128)}, bf16[96,512]{1,0:T(8,128)(2,1)S(1)}, bf16[96,512]{1,0:T(8,128)(2,1)S(1)}, bf16[96,5...) custom-call(s32[2,256]{1,0:T(2,128)} %bitcast.22, ...), custom_call_target="tpu_custom_call" | custom-call | flops 1000000000 | bytes 4000000 | tf_op jit(solution)/shard_map/route/pallas_call | solution.py:333
  2.9 4.1 %collective-permute-start.20 = (bf16[96,512]{1,0:T(8,128)(2,1)S(1)}, bf16[96,512]{1,0:T(8,128)(2,1)S(1)}, u32[]{:S(2)}, u32[]{:S(2)}) collective-permute-start(bf16[96,512]{1,0:T(8,128)(2,1)S(1)} %get-tuple-element.33), channel_id=1, source_target_pairs={{0,16},{4,20},{8,24},{12,28},{16,0},{20,4},{24,8},{28,12},{1,17},{... | collective-permute-start | bytes 294920 | tf_op jit(solution)/shard_map/ppermute | solution.py:699
  8.3 3.6 %collective-permute-start.22 = (bf16[96,512]{1,0:T(8,128)(2,1)S(1)}, bf16[96,512]{1,0:T(8,128)(2,1)S(1)}, u32[]{:S(2)}, u32[]{:S(2)}) collective-permute-start(bf16[96,512]{1,0:T(8,128)(2,1)S(1)} %get-tuple-element.35), channel_id=1, source_target_pairs={{0,24},{4,28},{8,16},{12,20},{16,8},{20,12},{24,0},{28,4},{1,25},{... | collective-permute-start | bytes 294920 | tf_op jit(solution)/shard_map/ppermute | solution.py:699
  11.9 7.2 %collective-permute-done.20.refs_0_ = bf16[96,512]{1,0:T(8,128)(2,1)S(1)} collective-permute-done((bf16[96,512]{1,0:T(8,128)(2,1)S(1)}, bf16[96,512]{1,0:T(8,128)(2,1)S(1)}, u32[]{:S(2)}, u32[]{:S(2)}) %collective-permute-start.20) | collective-permute-done | bytes 98336 | tf_op jit(solution)/shard_map/ppermute | solution.py:699
  19.1 3.2 %collective-permute-done.21.refs_1_ = bf16[96,512]{1,0:T(8,128)(2,1)S(1)} collective-permute-done((bf16[96,512]{1,0:T(8,128)(2,1)S(1)}, bf16[96,512]{1,0:T(8,128)(2,1)S(1)}, u32[]{:S(2)}, u32[]{:S(2)}) %collective-permute-start.21) | collective-permute-done | bytes 98336 | tf_op jit(solution)/shard_map/ppermute | solution.py:699
  22.3 1.6 %collective-permute-start.27 = (bf16[384,512]{1,0:T(8,128)(2,1)S(1)}, bf16[384,512]{1,0:T(8,128)(2,1)S(1)}, u32[]{:S(2)}, u32[]{:S(2)}) collective-permute-start(bf16[384,512]{1,0:T(8,128)(2,1)S(1)} %bitcast.11), channel_id=1, source_target_pairs={{0,2},{1,3},{2,0},{3,1},{4,6},{5,7},{6,4},{7,5},{8,10},{9,11},{10,... | collective-permute-start | bytes 1179656 | tf_op jit(solution)/shard_map/ppermute | solution.py:582
  24.5 3.9 %collective-permute-start.15 = (bf16[96,512]{1,0:T(8,128)(2,1)S(1)}, bf16[96,512]{1,0:T(8,128)(2,1)S(1)}, u32[]{:S(2)}, u32[]{:S(2)}) collective-permute-start(bf16[96,512]{1,0:T(8,128)(2,1)S(1)} %get-tuple-element.31), channel_id=1, source_target_pairs={{0,8},{4,12},{8,0},{12,4},{16,24},{20,28},{24,16},{28,20},{1,9},{5... | collective-permute-start | bytes 294920 | tf_op jit(solution)/shard_map/ppermute | solution.py:699
  29.2 2.6 %collective-permute-done.15.refs_2_ = bf16[96,512]{1,0:T(8,128)(2,1)S(1)} collective-permute-done((bf16[96,512]{1,0:T(8,128)(2,1)S(1)}, bf16[96,512]{1,0:T(8,128)(2,1)S(1)}, u32[]{:S(2)}, u32[]{:S(2)}) %collective-permute-start.15) | collective-permute-done | bytes 98336 | tf_op jit(solution)/shard_map/ppermute | solution.py:699
  31.8 2.1 %collective-permute-done.16.refs_3_ = bf16[96,512]{1,0:T(8,128)(2,1)S(1)} collective-permute-done((bf16[96,512]{1,0:T(8,128)(2,1)S(1)}, bf16[96,512]{1,0:T(8,128)(2,1)S(1)}, u32[]{:S(2)}, u32[]{:S(2)}) %collective-permute-start.16) | collective-permute-done | bytes 98336 | tf_op jit(solution)/shard_map/ppermute | solution.py:699
  35.0 8.8 %collective-permute-done.17.refs_0_ = bf16[384,512]{1,0:T(8,128)(2,1)S(1)} collective-permute-done((bf16[384,512]{1,0:T(8,128)(2,1)S(1)}, bf16[384,512]{1,0:T(8,128)(2,1)S(1)}, u32[]{:S(2)}, u32[]{:S(2)}) %collective-permute-start.17) | collective-permute-done | bytes 393248 | tf_op jit(solution)/shard_map/ppermute | solution.py:582
  43.8 5.2 %shard_map.191.refs_2_ = f32[2,768,1024]{2,1,0:T(8,128)S(1)} custom-call(bf16[384,512]{1,0:T(8,128)(2,1)S(1)} %bitcast.16, bf16[384,512]{1,0:T(8,128)(2,1)S(1)} %collective-permute-done.19.refs_1_, bf16[384,512]{1,0:T(8,128)(2,1)S(1)} %bitcast.13, bf16[384,512]{1,0:T(8,128)(2,1)S(1)} %collective-permute-done.24.refs_3_, bf16[1,2048,1024]{2,1,0:T(8,128)(2,1)} %refs_3_.3, ...), custom_call_target="tpu_custom_call" | custom-call | flops 1610612736 | bytes 12582912 | tf_op jit(solution)/shard_map/pallas_call | solution.py:462
  49.0 5.9 %shard_map.194 = (bf16[2,384,512]{2,1,0:T(8,128)(2,1)S(1)}, bf16[2,384,512]{2,1,0:T(8,128)(2,1)S(1)}) custom-call(bf16[384,512]{1,0:T(8,128)(2,1)S(1)} %collective-permute-done.27.refs_0_, bf16[384,512]{1,0:T(8,128)(2,1)S(1)} %collective-permute-done.28.refs_1_, f32[2,768,1024]{2,1,0:T(8,128)S(1)} %shard_map.191.refs_2_, bf16[1,2048,1024]{2,1,0:T(8,128)(2,1)} %refs_3_.3, ...), custom_call_target="tpu_custom_call" | custom-call | flops 3221225472 | bytes 12582912 | tf_op jit(solution)/shard_map/pallas_call | solution.py:462
  55.4 5.8 %shard_map.192 = (bf16[2,384,512]{2,1,0:T(8,128)(2,1)S(1)}, bf16[2,384,512]{2,1,0:T(8,128)(2,1)S(1)}) custom-call(bf16[384,512]{1,0:T(8,128)(2,1)S(1)} %collective-permute-done.17.refs_0_, bf16[384,512]{1,0:T(8,128)(2,1)S(1)} %collective-permute-done.18.refs_1_, f32[2,768,1024]{2,1,0:T(8,128)S(1)} %shard_map.191.refs_2_, bf16[1,2048,1024]{2,1,0:T(8,128)(2,1)} %refs_3_.3, ...), custom_call_target="tpu_custom_call" | custom-call | flops 3221225472 | bytes 12582912 | tf_op jit(solution)/shard_map/pallas_call | solution.py:462
  61.4 1.9 %keys.1 = (bf16[384,128]{1,0:T(8,128)(2,1)S(1)}, f32[140,128]{1,0:T(8,128)S(1)}) custom-call(bf16[384,256]{1,0:T(8,128)(2,1)} %key_hbm.1, bf16[384,256]{1,0:T(8,128)(2,1)} %value_hbm.1, f32[1,64]{1,0:T(1,128)} %bitcast.24, f32[1,128]{1,0:T(1,128)} %constant.2.clone.inverse_hbm), custom_call_target="tpu_custom_call" | custom-call | flops 1000000000 | bytes 300000 | tf_op jit(solution)/shard_map/keys/pallas_call | solution.py:129
  64.6 3.4 %collective-permute-start.1 = (bf16[384,128]{1,0:T(8,128)(2,1)S(1)}, bf16[384,128]{1,0:T(8,128)(2,1)S(1)}, u32[]{:S(2)}, u32[]{:S(2)}) collective-permute-start(bf16[384,128]{1,0:T(8,128)(2,1)S(1)} %get-tuple-element.23.refs_0_), channel_id=1, source_target_pairs={{0,16},{4,20},{8,24},{12,28},{16,0},{20,4},{24,8},{28,12},{1,17},{... | collective-permute-start | bytes 294920 | tf_op jit(solution)/shard_map/ppermute | solution.py:601
  69.9 4.5 %shard_map.186 = (bf16[2,256,512]{2,1,0:T(8,128)(2,1)}, bf16[2,256,512]{2,1,0:T(8,128)(2,1)S(1)}) custom-call(bf16[256,2048]{1,0:T(8,128)(2,1)S(1)} %get-tuple-element.25.refs_0_, bf16[1,2048,512]{2,1,0:T(8,128)(2,1)} %bitcast.18, bf16[1,2048,512]{2,1,0:T(8,128)(2,1)} %bitcast.19, bf16[1,512,2048]{2,1,0:T(8,128)(2,1)} %bitcast.20), custom_call_target="tpu_custom_call" | custom-call | flops 1610612736 | bytes 6291456 | tf_op jit(solution)/shard_map/pallas_call | solution.py:462
  74.6 2.9 %collective-permute-start.2 = (bf16[384,128]{1,0:T(8,128)(2,1)S(1)}, bf16[384,128]{1,0:T(8,128)(2,1)S(1)}, u32[]{:S(2)}, u32[]{:S(2)}) collective-permute-start(bf16[384,128]{1,0:T(8,128)(2,1)S(1)} %get-tuple-element.23.refs_0_), channel_id=1, source_target_pairs={{0,24},{4,28},{8,0},{12,4},{16,8},{20,12},{24,16},{28,20},{1,25},{... | collective-permute-start | bytes 294920 | tf_op jit(solution)/shard_map/ppermute | solution.py:601
  78.2 1.6 %collective-permute-start.26 = (bf16[384,512]{1,0:T(8,128)(2,1)S(1)}, bf16[384,512]{1,0:T(8,128)(2,1)S(1)}, u32[]{:S(2)}, u32[]{:S(2)}) collective-permute-start(bf16[384,512]{1,0:T(8,128)(2,1)S(1)} %shard_map.193), channel_id=1, source_target_pairs={{0,2},{1,3},{2,0},{3,1},{4,6},{5,7},{6,4},{7,5},{8,10},{9,11},{10,... | collective-permute-start | bytes 1179656 | tf_op jit(solution)/shard_map/ppermute | solution.py:582
  80.8 14.3 %collective-permute-done.30.refs_5_ = bf16[384,512]{1,0:T(8,128)(2,1)S(1)} collective-permute-done((bf16[384,512]{1,0:T(8,128)(2,1)S(1)}, bf16[384,512]{1,0:T(8,128)(2,1)S(1)}, u32[]{:S(2)}, u32[]{:S(2)}) %collective-permute-start.30) | collective-permute-done | bytes 393248 | tf_op jit(solution)/shard_map/ppermute | solution.py:582
  95.1 7.4 %collective-permute-done.26.refs_2_ = bf16[384,512]{1,0:T(8,128)(2,1)S(1)} collective-permute-done((bf16[384,512]{1,0:T(8,128)(2,1)S(1)}, bf16[384,512]{1,0:T(8,128)(2,1)S(1)}, u32[]{:S(2)}, u32[]{:S(2)}) %collective-permute-start.26) | collective-permute-done | bytes 393248 | tf_op jit(solution)/shard_map/ppermute | solution.py:582
  103.6 3.6 %all-to-all-start = ((bf16[8,96,512]{2,1,0:T(8,128)(2,1)}), bf16[8,96,512]{2,1,0:T(8,128)(2,1)S(1)}, u32[]{:S(2)}, u32[]{:S(2)}) async-start(bf16[8,96,512]{2,1,0:T(8,128)(2,1)} %shard_map.196), calls=%async_computation | async-start | bytes 1572864 | tf_op jit(solution)/shard_map/all_to_all | solution.py:611
  109.6 9.1 %attention.1.refs_0_ = bf16[384,256]{1,0:T(8,128)(2,1)S(1)} custom-call(bf16[384,256]{1,0:T(8,128)(2,1)} %q_hbm.1, f32[1,64]{1,0:T(1,128)} %bitcast.25, f32[140,128]{1,0:T(8,128)} %copy-done.3, bf16[4,384,128]{2,1,0:T(8,128)(2,1)S(1)} %shard_map.185.rest_0_, bf16[4,384,128]{2,1,0:T(8,128)(2,1)} %collective-permute-done.3.rest_1_), custom_call_target="tpu_custom_call" | custom-call | flops 8000000000 | bytes 2000000 | tf_op jit(solution)/shard_map/attention/pallas_call | solution.py:221
  120.5 8.2 %collective-permute-done.4.refs_1_ = bf16[384,256]{1,0:T(8,128)(2,1)S(1)} collective-permute-done((bf16[384,256]{1,0:T(8,128)(2,1)S(1)}, bf16[384,256]{1,0:T(8,128)(2,1)S(1)}, u32[]{:S(2)}, u32[]{:S(2)}) %collective-permute-start.4) | collective-permute-done | bytes 196640 | tf_op jit(solution)/shard_map/ppermute | solution.py:582
  130.4 5.3 %project.1 = bf16[384,2048]{1,0:T(8,128)(2,1)} custom-call(bf16[384,256]{1,0:T(8,128)(2,1)S(1)} %attention.1.refs_0_, bf16[384,256]{1,0:T(8,128)(2,1)S(1)} %collective-permute-done.4.refs_1_, bf16[384,256]{1,0:T(8,128)(2,1)S(1)} %collective-permute-done.5.refs_2_, bf16[384,256]{1,0:T(8,128)(2,1)S(1)} %collective-permute-done.6.refs_3_, ...), custom_call_target="tpu_custom_call" | custom-call | flops 2000000000 | bytes 6000000 | tf_op jit(solution)/shard_map/project/pallas_call | solution.py:273
  (67 shorter events, 17.6 us)
Async XLA Ops:
  2.9 16.2 %collective-permute-start.20 = (bf16[96,512]{1,0:T(8,128)(2,1)S(1)}, bf16[96,512]{1,0:T(8,128)(2,1)S(1)}, u32[]{:S(2)}, u32[]{:S(2)}) collective-permute-start(bf16[96,512]{1,0:T(8,128)(2,1)S(1)} %get-tuple-element.33), channel_id=1, source_target_pairs={{0,16},{4,20},{8,24},{12,28},{16,0},{20,4},{24,8},{28,12},{1,17},{... | collective-permute-start | bytes 294920 | tf_op jit(solution)/shard_map/ppermute | solution.py:699
  7.0 15.3 %collective-permute-start.21 = (bf16[96,512]{1,0:T(8,128)(2,1)S(1)}, bf16[96,512]{1,0:T(8,128)(2,1)S(1)}, u32[]{:S(2)}, u32[]{:S(2)}) collective-permute-start(bf16[96,512]{1,0:T(8,128)(2,1)S(1)} %get-tuple-element.34), channel_id=1, source_target_pairs={{0,20},{4,16},{8,28},{12,24},{16,4},{20,0},{24,12},{28,8},{1,21},{... | collective-permute-start | bytes 294920 | tf_op jit(solution)/shard_map/ppermute | solution.py:699
  8.3 14.0 %collective-permute-start.22 = (bf16[96,512]{1,0:T(8,128)(2,1)S(1)}, bf16[96,512]{1,0:T(8,128)(2,1)S(1)}, u32[]{:S(2)}, u32[]{:S(2)}) collective-permute-start(bf16[96,512]{1,0:T(8,128)(2,1)S(1)} %get-tuple-element.35), channel_id=1, source_target_pairs={{0,24},{4,28},{8,16},{12,20},{16,8},{20,12},{24,0},{28,4},{1,25},{... | collective-permute-start | bytes 294920 | tf_op jit(solution)/shard_map/ppermute | solution.py:699
  11.9 10.4 %collective-permute-start.23 = (bf16[96,512]{1,0:T(8,128)(2,1)S(1)}, bf16[96,512]{1,0:T(8,128)(2,1)S(1)}, u32[]{:S(2)}, u32[]{:S(2)}) collective-permute-start(bf16[96,512]{1,0:T(8,128)(2,1)S(1)} %get-tuple-element.36), channel_id=1, source_target_pairs={{0,28},{4,24},{8,20},{12,16},{16,12},{20,8},{24,4},{28,0},{1,29},{... | collective-permute-start | bytes 294920 | tf_op jit(solution)/shard_map/ppermute | solution.py:699
  22.3 12.7 %collective-permute-start.27 = (bf16[384,512]{1,0:T(8,128)(2,1)S(1)}, bf16[384,512]{1,0:T(8,128)(2,1)S(1)}, u32[]{:S(2)}, u32[]{:S(2)}) collective-permute-start(bf16[384,512]{1,0:T(8,128)(2,1)S(1)} %bitcast.11), channel_id=1, source_target_pairs={{0,2},{1,3},{2,0},{3,1},{4,6},{5,7},{6,4},{7,5},{8,10},{9,11},{10,... | collective-permute-start | bytes 1179656 | tf_op jit(solution)/shard_map/ppermute | solution.py:582
  33.9 9.8 %collective-permute-start.17 = (bf16[384,512]{1,0:T(8,128)(2,1)S(1)}, bf16[384,512]{1,0:T(8,128)(2,1)S(1)}, u32[]{:S(2)}, u32[]{:S(2)}) collective-permute-start(bf16[384,512]{1,0:T(8,128)(2,1)S(1)} %bitcast.14), channel_id=1, source_target_pairs={{0,2},{1,3},{2,0},{3,1},{4,6},{5,7},{6,4},{7,5},{8,10},{9,11},{10,... | collective-permute-start | bytes 1179656 | tf_op jit(solution)/shard_map/ppermute | solution.py:582
  35.0 14.0 %collective-permute-start.28 = (bf16[384,512]{1,0:T(8,128)(2,1)S(1)}, bf16[384,512]{1,0:T(8,128)(2,1)S(1)}, u32[]{:S(2)}, u32[]{:S(2)}) collective-permute-start(bf16[384,512]{1,0:T(8,128)(2,1)S(1)} %collective-permute-done.27.refs_0_), channel_id=1, source_target_pairs={{0,1},{1,0},{2,3},{3,2},{4,5},{5,4},{6,7},{7,6},{8,9},{9,8},{10,11... | collective-permute-start | bytes 1179656 | tf_op jit(solution)/shard_map/ppermute | solution.py:577
  43.8 11.7 %collective-permute-start.18 = (bf16[384,512]{1,0:T(8,128)(2,1)S(1)}, bf16[384,512]{1,0:T(8,128)(2,1)S(1)}, u32[]{:S(2)}, u32[]{:S(2)}) collective-permute-start(bf16[384,512]{1,0:T(8,128)(2,1)S(1)} %collective-permute-done.17.refs_0_), channel_id=1, source_target_pairs={{0,1},{1,0},{2,3},{3,2},{4,5},{5,4},{6,7},{7,6},{8,9},{9,8},{10,11... | collective-permute-start | bytes 1179656 | tf_op jit(solution)/shard_map/ppermute | solution.py:577
  54.9 19.5 %collective-permute-start.29 = (bf16[2,384,512]{2,1,0:T(8,128)(2,1)S(1)}, bf16[2,384,512]{2,1,0:T(8,128)(2,1)S(1)}, u32[]{:S(2)}, u32[]{:S(2)}) collective-permute-start(bf16[2,384,512]{2,1,0:T(8,128)(2,1)S(1)} %get-tuple-element.40), channel_id=1, source_target_pairs={{0,1},{1,0},{2,3},{3,2},{4,5},{5,4},{6,7},{7,6},{8,9},{9,8},{10,11... | collective-permute-start | bytes 2359304 | tf_op jit(solution)/shard_map/ppermute | solution.py:577
  61.3 13.3 %collective-permute-start.25 = (bf16[2,384,512]{2,1,0:T(8,128)(2,1)S(1)}, bf16[2,384,512]{2,1,0:T(8,128)(2,1)S(1)}, u32[]{:S(2)}, u32[]{:S(2)}) collective-permute-start(bf16[2,384,512]{2,1,0:T(8,128)(2,1)S(1)} %get-tuple-element.38), channel_id=1, source_target_pairs={{0,1},{1,0},{2,3},{3,2},{4,5},{5,4},{6,7},{7,6},{8,9},{9,8},{10,11... | collective-permute-start | bytes 2359304 | tf_op jit(solution)/shard_map/ppermute | solution.py:577
  63.3 14.4 %collective-permute-start = (bf16[384,128]{1,0:T(8,128)(2,1)S(1)}, bf16[384,128]{1,0:T(8,128)(2,1)S(1)}, u32[]{:S(2)}, u32[]{:S(2)}) collective-permute-start(bf16[384,128]{1,0:T(8,128)(2,1)S(1)} %get-tuple-element.23.refs_0_), channel_id=1, source_target_pairs={{0,8},{4,12},{8,16},{12,20},{16,24},{20,28},{24,0},{28,4},{1,9},{5... | collective-permute-start | bytes 294920 | tf_op jit(solution)/shard_map/ppermute | solution.py:601
  64.6 13.6 %collective-permute-start.1 = (bf16[384,128]{1,0:T(8,128)(2,1)S(1)}, bf16[384,128]{1,0:T(8,128)(2,1)S(1)}, u32[]{:S(2)}, u32[]{:S(2)}) collective-permute-start(bf16[384,128]{1,0:T(8,128)(2,1)S(1)} %get-tuple-element.23.refs_0_), channel_id=1, source_target_pairs={{0,16},{4,20},{8,24},{12,28},{16,0},{20,4},{24,8},{28,12},{1,17},{... | collective-permute-start | bytes 294920 | tf_op jit(solution)/shard_map/ppermute | solution.py:601
  68.9 40.7 %collective-permute-start.7 = (bf16[160,2048]{1,0:T(8,128)(2,1)}, bf16[160,2048]{1,0:T(8,128)(2,1)}, u32[]{:S(2)}, u32[]{:S(2)}) collective-permute-start(bf16[160,2048]{1,0:T(8,128)(2,1)} %slice.6), channel_id=1, source_target_pairs={{0,2},{1,3},{2,0},{3,1},{4,6},{5,7},{6,4},{7,5},{8,10},{9,11},{10,... | collective-permute-start | bytes 1966088 | tf_op jit(solution)/shard_map/ppermute | solution.py:582
  74.5 34.4 %collective-permute-start.12 = (bf16[2,256,512]{2,1,0:T(8,128)(2,1)}, bf16[2,256,512]{2,1,0:T(8,128)(2,1)S(1)}, u32[]{:S(2)}, u32[]{:S(2)}) collective-permute-start(bf16[2,256,512]{2,1,0:T(8,128)(2,1)} %get-tuple-element.27), channel_id=1, source_target_pairs={{0,1},{1,0},{2,3},{3,2},{4,5},{5,4},{6,7},{7,6},{8,9},{9,8},{10,11... | collective-permute-start | bytes 1572872 | tf_op jit(solution)/shard_map/ppermute | solution.py:577
  77.7 17.4 %collective-permute-start.30 = (bf16[384,512]{1,0:T(8,128)(2,1)S(1)}, bf16[384,512]{1,0:T(8,128)(2,1)S(1)}, u32[]{:S(2)}, u32[]{:S(2)}) collective-permute-start(bf16[384,512]{1,0:T(8,128)(2,1)S(1)} %shard_map.195), channel_id=1, source_target_pairs={{0,2},{1,3},{2,0},{3,1},{4,6},{5,7},{6,4},{7,5},{8,10},{9,11},{10,... | collective-permute-start | bytes 1179656 | tf_op jit(solution)/shard_map/ppermute | solution.py:582
  78.2 24.3 %collective-permute-start.26 = (bf16[384,512]{1,0:T(8,128)(2,1)S(1)}, bf16[384,512]{1,0:T(8,128)(2,1)S(1)}, u32[]{:S(2)}, u32[]{:S(2)}) collective-permute-start(bf16[384,512]{1,0:T(8,128)(2,1)S(1)} %shard_map.193), channel_id=1, source_target_pairs={{0,2},{1,3},{2,0},{3,1},{4,6},{5,7},{6,4},{7,5},{8,10},{9,11},{10,... | collective-permute-start | bytes 1179656 | tf_op jit(solution)/shard_map/ppermute | solution.py:582
  80.1 29.4 %collective-permute-start.3 = (bf16[4,384,128]{2,1,0:T(8,128)(2,1)S(1)}, bf16[4,384,128]{2,1,0:T(8,128)(2,1)}, u32[]{:S(2)}, u32[]{:S(2)}) collective-permute-start(bf16[4,384,128]{2,1,0:T(8,128)(2,1)S(1)} %shard_map.185.rest_0_), channel_id=1, source_target_pairs={{0,4},{4,0},{8,12},{12,8},{16,20},{20,16},{24,28},{28,24},{1,5},{5... | collective-permute-start | bytes 1179656 | tf_op jit(solution)/shard_map/ppermute | solution.py:606
  103.6 32.2 %all-to-all-start = ((bf16[8,96,512]{2,1,0:T(8,128)(2,1)}), bf16[8,96,512]{2,1,0:T(8,128)(2,1)S(1)}, u32[]{:S(2)}, u32[]{:S(2)}) async-start(bf16[8,96,512]{2,1,0:T(8,128)(2,1)} %shard_map.196), calls=%async_computation | async-start | bytes 1572864 | tf_op jit(solution)/shard_map/all_to_all | solution.py:611
  107.2 23.2 %collective-permute-start.9 = (bf16[256,2048]{1,0:T(8,128)(2,1)S(1)}, bf16[256,2048]{1,0:T(8,128)(2,1)S(1)}, u32[]{:S(2)}, u32[]{:S(2)}) collective-permute-start(bf16[256,2048]{1,0:T(8,128)(2,1)S(1)} %copy-done), channel_id=1, source_target_pairs={{0,1},{1,0},{2,3},{3,2},{4,5},{5,4},{6,7},{7,6},{8,9},{9,8},{10,11... | collective-permute-start | bytes 3145736 | tf_op jit(solution)/shard_map/ppermute | solution.py:577
  107.3 13.0 %collective-permute-start.8 = (bf16[96,2048]{1,0:T(8,128)(2,1)S(1)}, bf16[96,2048]{1,0:T(8,128)(2,1)S(1)}, u32[]{:S(2)}, u32[]{:S(2)}) collective-permute-start(bf16[96,2048]{1,0:T(8,128)(2,1)S(1)} %slice.7), channel_id=1, source_target_pairs={{0,2},{1,3},{2,0},{3,1},{4,6},{5,7},{6,4},{7,5},{8,10},{9,11},{10,... | collective-permute-start | bytes 1179656 | tf_op jit(solution)/shard_map/ppermute | solution.py:582
  108.9 19.8 %collective-permute-start.13 = (bf16[256,512]{1,0:T(8,128)(2,1)S(1)}, bf16[256,512]{1,0:T(8,128)(2,1)S(1)}, u32[]{:S(2)}, u32[]{:S(2)}) collective-permute-start(bf16[256,512]{1,0:T(8,128)(2,1)S(1)} %shard_map.187), channel_id=1, source_target_pairs={{0,2},{1,3},{2,0},{3,1},{4,6},{5,7},{6,4},{7,5},{8,10},{9,11},{10,... | collective-permute-start | bytes 786440 | tf_op jit(solution)/shard_map/ppermute | solution.py:582
  109.5 20.9 %collective-permute-start.10 = (bf16[160,2048]{1,0:T(8,128)(2,1)}, bf16[160,2048]{1,0:T(8,128)(2,1)S(1)}, u32[]{:S(2)}, u32[]{:S(2)}) collective-permute-start(bf16[160,2048]{1,0:T(8,128)(2,1)} %collective-permute-done.7.refs_5_), channel_id=1, source_target_pairs={{0,1},{1,0},{2,3},{3,2},{4,5},{5,4},{6,7},{7,6},{8,9},{9,8},{10,11... | collective-permute-start | bytes 1966088 | tf_op jit(solution)/shard_map/ppermute | solution.py:577
  118.7 10.0 %collective-permute-start.4 = (bf16[384,256]{1,0:T(8,128)(2,1)S(1)}, bf16[384,256]{1,0:T(8,128)(2,1)S(1)}, u32[]{:S(2)}, u32[]{:S(2)}) collective-permute-start(bf16[384,256]{1,0:T(8,128)(2,1)S(1)} %attention.1.refs_0_), channel_id=1, source_target_pairs={{0,2},{1,3},{2,0},{3,1},{4,6},{5,7},{6,4},{7,5},{8,10},{9,11},{10,... | collective-permute-start | bytes 589832 | tf_op jit(solution)/shard_map/ppermute | solution.py:582
  120.3 9.9 %collective-permute-start.11 = (bf16[96,2048]{1,0:T(8,128)(2,1)S(1)}, bf16[96,2048]{1,0:T(8,128)(2,1)S(1)}, u32[]{:S(2)}, u32[]{:S(2)}) collective-permute-start(bf16[96,2048]{1,0:T(8,128)(2,1)S(1)} %collective-permute-done.8.refs_6_), channel_id=1, source_target_pairs={{0,1},{1,0},{2,3},{3,2},{4,5},{5,4},{6,7},{7,6},{8,9},{9,8},{10,11... | collective-permute-start | bytes 1179656 | tf_op jit(solution)/shard_map/ppermute | solution.py:577
  (12 other events, 110.2 us)
